TPU v7x, 512 devices: a whole 4x4x16 slice. The times are simulated.
512 devices in a mesh: ep: 32 (over z, core), tp: 16 (over y, x).
Axes of the slice: x: 4, y: 4, z: 16, core: 2. Of those that a mesh axis runs over, the one named last changes fastest.
Arguments:
- resid: bfloat16 [256, 2048], P('ep', 'tp'), may hold values from -6 to 6
- attn_gain: float32 [2048], replicated, may hold values from 0.1 to 1.9
- w_query: bfloat16 [2048, 1024], P(None, 'tp'), may hold values from -0.125 to 0.125
- w_key: bfloat16 [2048, 1024], P(None, 'tp'), may hold values from -0.125 to 0.125
- w_value: bfloat16 [2048, 1024], P(None, 'tp'), may hold values from -0.125 to 0.125
- key_cache: bfloat16 [256, 16, 64, 1024], P('ep', 'tp'), may hold values from -6 to 6
- value_cache: bfloat16 [256, 16, 64, 1024], P('ep', 'tp'), may hold values from -19 to 19
- key_bias: float32 [256, 16, 1024], P('ep', 'tp'), may hold values from -10.2 to 0
- lengths: int32 [256], P('ep'), may hold values from 1 to 1024
- mix_gain: float32 [1024], P('tp'), may hold values from 0.1 to 1.9
- w_out: bfloat16 [1024, 2048], P('tp'), may hold values from -0.1875 to 0.1875
- ffn_gain: float32 [2048], replicated, may hold values from 0.1 to 1.9
- route_experts: int32 [256, 4], P('ep'), may hold values from 0 to 31, all different within a row; in each aligned block of 8 rows (0 to 7, 8 to 15, ...) at most 3 rows name the same one
- route_weights: float32 [256, 4], P('ep'), may hold values from 0.05 to 1
- w_gate: bfloat16 [32, 2048, 2048], P('ep', None, 'tp'), may hold values from -0.3125 to 0.3125
- w_up: bfloat16 [32, 2048, 2048], P('ep', None, 'tp'), may hold values from -0.3125 to 0.3125
- w_down: bfloat16 [32, 2048, 2048], P('ep', 'tp'), may hold values from -0.0546875 to 0.0546875
Outputs:
- mixed: bfloat16 [256, 2048], P('ep', 'tp')
- new_keys: bfloat16 [256, 1024], P('ep', 'tp')
- new_values: bfloat16 [256, 1024], P('ep', 'tp')
Inputs may be any that keep to these rules, and one draw needn't show every extreme that they name: `route_experts`: each row names 4 different experts. Within the rows of one device (aligned blocks of 8 rows) no expert is named more than 3 times, a bound that some block reaches.
All inputs are finite; a program needn't handle non-finite values.
Results may differ from a plain program's by a relative error of at most 0.018.
Values may be sent and summed in bfloat16 or wider, within the bound.
No kernel may reach another device: no remote copies, remote signals or barrier semaphores. Data moves between devices by JAX's collectives and lax.ppermute only.
A program may use at most 64 MiB of HBM per device.

v0:
```python
import functools

import jax
import jax.numpy as jnp
from jax import lax
from jax.sharding import Mesh
from jax.sharding import PartitionSpec as P

TP = ("tp_0", "tp_1")


eps = 1e-06
limit = 7.0
alpha = 1.702


def cut_along(x, dim, size):
    before, after = (x.shape[:dim], x.shape[dim + 1 :])
    return jnp.moveaxis(x.reshape(*before, size, -1, *after), dim, 0)


def sum_at_owner(x, axis, dim):
    size = lax.axis_size(axis)
    parts = lax.all_to_all(cut_along(x, dim, size), axis, 0, 0, tiled=True)
    return jnp.sum(parts.astype(jnp.float32), axis=0)


def in_order(parts, dim):
    parts = jnp.moveaxis(parts, 0, dim)
    shape = parts.shape
    return parts.reshape(*shape[:dim], shape[dim] * shape[dim + 1], *shape[dim + 2 :])


def from_everyone(x, axis):
    size = lax.axis_size(axis)
    return lax.all_to_all(jnp.broadcast_to(x[None], (size, *x.shape)), axis, 0, 0, tiled=True)


def gather_directly(x, axis, dim):
    return in_order(from_everyone(x, axis), dim)


def over_axes(x, axes):
    return functools.reduce(lax.psum, axes, x)


def taken_together(x, axis):
    return from_everyone(x, axis).astype(jnp.float32).sum(axis=0)


def expert_block(inputs, gate_shard, up_shard, down_shard):
    gate = jnp.minimum(jnp.dot(inputs, gate_shard, preferred_element_type=jnp.float32), limit)
    upper = jnp.clip(jnp.dot(inputs, up_shard, preferred_element_type=jnp.float32), -limit, limit)
    active = ((upper + 1.0) * gate * jax.nn.sigmoid(alpha * gate)).astype(jnp.bfloat16)
    partial_out = jnp.dot(active, down_shard, preferred_element_type=jnp.float32)
    return sum_at_owner(partial_out.astype(jnp.bfloat16), TP, 1).astype(jnp.bfloat16)


def stick_heads(query, key_cache, value_cache, key_bias, lengths):
    sequences, heads, width, cache = key_cache.shape
    head_query = query.reshape(sequences, heads, width)
    scores = (
        jnp.einsum("bhd,bhds->bhs", head_query, key_cache, preferred_element_type=jnp.float32)
        * width ** (-0.5)
        + key_bias
    )
    live = lax.broadcasted_iota(jnp.int32, (sequences, 1, cache), 2) < lengths[:, None, None]
    log_keep = jnp.where(live, jax.nn.log_sigmoid(-scores), 0.0)
    after = lax.cumsum(log_keep, axis=2, reverse=True) - log_keep
    weights = jnp.where(live, jnp.exp(jax.nn.log_sigmoid(scores) + after), 0.0).astype(jnp.bfloat16)
    attended = jnp.einsum("bhs,bhds->bhd", weights, value_cache, preferred_element_type=jnp.float32)
    return attended.reshape(sequences, heads * width)


def body(
    resid,
    attn_gain,
    w_query,
    w_key,
    w_value,
    key_cache,
    value_cache,
    key_bias,
    lengths,
    mix_gain,
    w_out,
    ffn_gain,
    route_experts,
    route_weights,
    w_gate,
    w_up,
    w_down,
):
    whole = gather_directly(resid, TP, 1).astype(jnp.float32)
    model_width = whole.shape[1]
    normed_in = (
        whole * lax.rsqrt(jnp.mean(whole * whole, axis=1, keepdims=True) + eps) * attn_gain
    ).astype(jnp.bfloat16)
    query = jnp.dot(normed_in, w_query, preferred_element_type=jnp.float32).astype(jnp.bfloat16)
    new_keys = jnp.dot(normed_in, w_key, preferred_element_type=jnp.float32).astype(jnp.bfloat16)
    new_values = jnp.dot(normed_in, w_value, preferred_element_type=jnp.float32).astype(
        jnp.bfloat16
    )
    attended = stick_heads(query, key_cache, value_cache, key_bias, lengths)
    channels = attended.shape[1] * lax.axis_size(TP)
    head_total = over_axes(jnp.sum(attended * attended, axis=1), TP)
    normed_heads = (attended * lax.rsqrt(head_total / channels + eps)[:, None] * mix_gain).astype(
        jnp.bfloat16
    )
    partial_branch = jnp.dot(normed_heads, w_out, preferred_element_type=jnp.float32)
    shard_width = resid.shape[1]
    offset = lax.axis_index(TP) * shard_width
    middle = whole + taken_together(partial_branch.astype(jnp.bfloat16), TP).astype(jnp.float32)
    normed_mid = (
        middle * lax.rsqrt(jnp.mean(middle * middle, axis=1, keepdims=True) + eps) * ffn_gain
    ).astype(jnp.bfloat16)
    middle_own = lax.dynamic_slice_in_dim(middle, offset, shard_width, 1)
    sequences, top = route_experts.shape
    share = route_weights / jnp.sum(route_weights, axis=1, keepdims=True)
    groups = lax.axis_size("ep")
    experts_all = w_gate.shape[0] * groups
    capacity = max(2, min(sequences, 3 * sequences * top // experts_all))
    gate_shard = w_gate[0]
    up_shard = w_up[0]
    down_shard = w_down[0]
    count = sequences * top
    position = lax.broadcasted_iota(jnp.int32, (count, count), 0)
    later = position > position.T
    chosen = route_experts.reshape(-1)
    earlier = (chosen[:, None] == chosen[None, :]) & later
    rank = jnp.sum(earlier.astype(jnp.int32), axis=1)
    target = chosen * capacity + rank
    slots_total = experts_all * capacity
    slot_iota = lax.broadcasted_iota(jnp.int32, (slots_total, sequences, top), 0)
    dispatch = jnp.any(slot_iota == target.reshape(sequences, top)[None], axis=2).astype(
        jnp.bfloat16
    )
    outgoing = jnp.dot(dispatch, normed_mid, preferred_element_type=jnp.float32).astype(
        jnp.bfloat16
    )
    outgoing = outgoing.reshape(experts_all, capacity, model_width)
    arrived = lax.all_to_all(outgoing, "ep", split_axis=0, concat_axis=0, tiled=True)
    sources, items, width = arrived.shape
    result = expert_block(arrived.reshape(sources * items, width), gate_shard, up_shard, down_shard)
    returned = lax.all_to_all(
        result.reshape(sources, items, -1), "ep", split_axis=0, concat_axis=0, tiled=True
    )
    picker = (target[:, None] == lax.broadcasted_iota(jnp.int32, (count, slots_total), 1)).astype(
        jnp.bfloat16
    )
    picked = jnp.dot(
        picker, returned.reshape(slots_total, -1), preferred_element_type=jnp.float32
    ).reshape(sequences, top, -1)
    mixture = jnp.sum(share[:, :, None] * picked, axis=1)
    mixed = (middle_own + mixture).astype(jnp.bfloat16)
    return (mixed, new_keys, new_values)


def solution(mesh):
    torus = Mesh(mesh.devices.reshape(mesh.shape["ep"], 4, 4), ("ep", "tp_0", "tp_1"))
    in_specs = (
        P("ep", TP),
        P(),
        P(None, TP),
        P(None, TP),
        P(None, TP),
        P("ep", TP, None, None),
        P("ep", TP, None, None),
        P("ep", TP, None),
        P("ep"),
        P(TP),
        P(TP, None),
        P(),
        P("ep", None),
        P("ep", None),
        P("ep", None, TP),
        P("ep", None, TP),
        P("ep", TP, None),
    )
    out_specs = (P("ep", TP), P("ep", TP), P("ep", TP))
    return jax.shard_map(body, mesh=torus, in_specs=in_specs, out_specs=out_specs, check_vma=False)
```

profile of v0, /device:TPU:1, one launch (start us, length us, event | category | flops | bytes accessed | tf_op | source)
XLA Modules:
  0.0 150.7 jit_solution(17181071740203797541)
XLA Ops:
  0.7 0.8 broadcast_in_dim.6
  1.5 13.8 %all_to_all.25 = bf16[16,8,128]{2,1,0:T(8,128)(2,1)S(1)} all-to-all(bf16[16,8,128]{2,1,0:T(8,128)(2,1)S(1)} %broadcast_in_dim.6), channel_id=1, replica_groups=mesh['ep'=32,'tp_0'=4,'tp_1'=4] {'tp_0','tp_1'}, dimensions={0} | all-to-all | bytes 65536 | tf_op jit(solution)/shard_map/all_to_all | solution.py:36
  15.4 0.5 copy-done.19
  16.0 1.2 fusion.6
  17.4 0.7 copy-done.5
  18.4 9.9 %reduce-window.6 = f32[8,1,8,128]{3,2,1,0:T(8,128)S(1)} reduce-window(f32[8,1,8,128]{3,2,1,0:T(8,128)S(1)} %bitcast.86, f32[]{:T(128)} %constant.18.clone.1), window={size=1x1x1x128 pad=0_0x0_0x0_0x0_127}, to_apply=%region_1.2 | reduce-window | flops 1040384 | bytes 65540 | tf_op jit(solution)/shard_map/reduce-window
  28.7 0.6 fusion.7
  29.4 6.9 %psum.14 = f32[8]{0:T(128)S(1)} all-reduce(f32[8]{0:T(128)S(1)} %multiply_reduce_fusion), channel_id=1, replica_groups=mesh['ep'=32,'tp_0'=4,'tp_1'=4] {'tp_0'}, use_global_device_ids=true, to_apply=%region_4.5 | all-reduce | flops 8 | bytes 64 | tf_op jit(solution)/shard_map/psum | solution.py:44
  36.3 6.9 %psum.15 = f32[8]{0:T(128)S(1)} all-reduce(f32[8]{0:T(128)S(1)} %psum.14), channel_id=1, replica_groups=mesh['ep'=32,'tp_0'=4,'tp_1'=4] {'tp_1'}, use_global_device_ids=true, to_apply=%region_5.6 | all-reduce | flops 8 | bytes 64 | tf_op jit(solution)/shard_map/psum | solution.py:44
  43.2 0.6 copy-done.14
  44.0 0.9 broadcast_in_dim.7
  44.9 3.7 %all-to-all-start.1 = ((bf16[16,8,2048]{2,1,0:T(8,128)(2,1)}), bf16[16,8,2048]{2,1,0:T(8,128)(2,1)S(1)}, u32[]{:S(2)}, u32[]{:S(2)}) async-start(bf16[16,8,2048]{2,1,0:T(8,128)(2,1)} %broadcast_in_dim.7), calls=%async_computation.1 | async-start | bytes 1048576 | tf_op jit(solution)/shard_map/all_to_all | solution.py:36
  49.2 8.3 %all-to-all-done.1 = bf16[16,8,2048]{2,1,0:T(8,128)(2,1)S(1)} async-done(((bf16[16,8,2048]{2,1,0:T(8,128)(2,1)}), bf16[16,8,2048]{2,1,0:T(8,128)(2,1)S(1)}, u32[]{:S(2)}, u32[]{:S(2)}) %all-to-all-start.1) | async-done | bytes 524320 | tf_op jit(solution)/shard_map/all_to_all | solution.py:36
  57.8 0.7 copy-done.6
  58.8 1.0 reshape.177
  59.8 22.7 %all-to-all-start.2 = ((bf16[32,3,2048]{2,1,0:T(4,128)(2,1)}), bf16[32,3,2048]{2,1,0:T(4,128)(2,1)S(1)}, u32[]{:S(2)}, u32[]{:S(2)}) async-start(bf16[32,3,2048]{2,1,0:T(4,128)(2,1)} %reshape.177), calls=%async_computation.2 | async-start | bytes 1048576 | tf_op jit(solution)/shard_map/all_to_all | solution.py:142
  82.5 0.5 reduce_sum.82
  83.0 33.0 %all-to-all-done.2 = bf16[32,3,2048]{2,1,0:T(4,128)(2,1)S(1)} async-done(((bf16[32,3,2048]{2,1,0:T(4,128)(2,1)}), bf16[32,3,2048]{2,1,0:T(4,128)(2,1)S(1)}, u32[]{:S(2)}, u32[]{:S(2)}) %all-to-all-start.2) | async-done | bytes 393248 | tf_op jit(solution)/shard_map/all_to_all | solution.py:142
  116.0 0.3 reshape.178
  116.6 0.4 copy-done.2
  117.0 0.4 copy-done.1
  117.4 0.5 fusion
  117.9 0.8 copy.52
  118.7 3.7 %all-to-all-start.3 = ((bf16[16,96,128]{2,1,0:T(8,128)(2,1)}), bf16[16,96,128]{2,1,0:T(8,128)(2,1)S(1)}, u32[]{:S(2)}, u32[]{:S(2)}) async-start(bf16[16,96,128]{2,1,0:T(8,128)(2,1)} %bitcast.85), calls=%async_computation.3 | async-start | bytes 786432 | tf_op jit(solution)/shard_map/all_to_all | solution.py:24
  122.5 0.6 copy-done.20
  123.1 0.8 convolution_convert_fusion.4
  123.9 7.9 %all-to-all-done.3 = bf16[16,96,128]{2,1,0:T(8,128)(2,1)S(1)} async-done(((bf16[16,96,128]{2,1,0:T(8,128)(2,1)}), bf16[16,96,128]{2,1,0:T(8,128)(2,1)S(1)}, u32[]{:S(2)}, u32[]{:S(2)}) %all-to-all-start.3) | async-done | bytes 393248 | tf_op jit(solution)/shard_map/all_to_all | solution.py:24
  131.9 0.6 reshape.180
  132.5 5.1 %all-to-all-start.4 = ((bf16[32,3,128]{2,1,0:T(4,128)(2,1)}), bf16[32,3,128]{2,1,0:T(4,128)(2,1)S(1)}, u32[]{:S(2)}, u32[]{:S(2)}) async-start(bf16[32,3,128]{2,1,0:T(4,128)(2,1)} %reshape.180), calls=%async_computation.4 | async-start | bytes 65536 | tf_op jit(solution)/shard_map/all_to_all | solution.py:145
  137.6 0.8 convolution_convert_fusion.3
  138.5 11.4 %all-to-all-done.4 = bf16[32,3,128]{2,1,0:T(4,128)(2,1)S(1)} async-done(((bf16[32,3,128]{2,1,0:T(4,128)(2,1)}), bf16[32,3,128]{2,1,0:T(4,128)(2,1)S(1)}, u32[]{:S(2)}, u32[]{:S(2)}) %all-to-all-start.4) | async-done | bytes 24608 | tf_op jit(solution)/shard_map/all_to_all | solution.py:145
  150.1 0.6 add_convert_fusion
  (64 shorter events, 3.1 us)
Async XLA Ops:
  0.6 16.5 %copy-start = (bf16[8,1,64,1024]{3,2,1,0:T(8,128)(2,1)S(1)}, bf16[8,1,64,1024]{3,2,1,0:T(8,128)(2,1)}, u32[]{:S(2)}) copy-start(bf16[8,1,64,1024]{3,2,1,0:T(8,128)(2,1)} %param.22) | copy-start | bytes 3145732
  0.6 28.0 %copy-start.15 = (bf16[8,1,64,1024]{3,2,1,0:T(8,128)(2,1)S(1)}, bf16[8,1,64,1024]{3,2,1,0:T(8,128)(2,1)}, u32[]{:S(2)}) copy-start(bf16[8,1,64,1024]{3,2,1,0:T(8,128)(2,1)} %param.23) | copy-start | bytes 3145732
  15.4 0.5 copy-start.19
  17.4 0.8 copy-start.5
  17.4 0.8 copy-start.13
  28.7 14.5 %copy-start.4 = (bf16[64,2048]{1,0:T(8,128)(2,1)S(1)}, bf16[64,2048]{1,0:T(8,128)(2,1)}, u32[]{:S(2)}) copy-start(bf16[64,2048]{1,0:T(8,128)(2,1)} %param.27) | copy-start | bytes 786436
  43.1 0.7 copy-start.14
  44.9 3.7 %copy-start.11 = (s32[8,4]{0,1:T(4,128)S(1)}, s32[8,4]{0,1:T(4,128)}, u32[]{:S(2)}) copy-start(s32[8,4]{0,1:T(4,128)} %param.29) | copy-start | bytes 388
  44.9 12.7 %all-to-all-start.1 = ((bf16[16,8,2048]{2,1,0:T(8,128)(2,1)}), bf16[16,8,2048]{2,1,0:T(8,128)(2,1)S(1)}, u32[]{:S(2)}, u32[]{:S(2)}) async-start(bf16[16,8,2048]{2,1,0:T(8,128)(2,1)} %broadcast_in_dim.7), calls=%async_computation.1 | async-start | bytes 1048576 | tf_op jit(solution)/shard_map/all_to_all | solution.py:36
  49.1 8.5 %copy-start.7 = (s32[8,4]{0,1:T(4,128)}, s32[8,4]{0,1:T(4,128)S(1)}, u32[]{:S(2)}) copy-start(s32[8,4]{0,1:T(4,128)S(1)} %copy.40) | copy-start | bytes 388
  57.7 0.7 copy-start.6
  59.8 22.7 %copy-start.9 = (f32[8,4]{0,1:T(4,128)S(1)}, f32[8,4]{0,1:T(4,128)}, u32[]{:S(2)}) copy-start(f32[8,4]{0,1:T(4,128)} %param.30) | copy-start | bytes 388
  59.8 56.2 %all-to-all-start.2 = ((bf16[32,3,2048]{2,1,0:T(4,128)(2,1)}), bf16[32,3,2048]{2,1,0:T(4,128)(2,1)S(1)}, u32[]{:S(2)}, u32[]{:S(2)}) async-start(bf16[32,3,2048]{2,1,0:T(4,128)(2,1)} %reshape.177), calls=%async_computation.2 | async-start | bytes 1048576 | tf_op jit(solution)/shard_map/all_to_all | solution.py:142
  82.5 33.9 %copy-start.3 = (bf16[1,2048,128]{2,1,0:T(8,128)(2,1)S(1)}, bf16[1,2048,128]{2,1,0:T(8,128)(2,1)}, u32[]{:S(2)}) copy-start(bf16[1,2048,128]{2,1,0:T(8,128)(2,1)} %param.31) | copy-start | bytes 1572868
  116.0 1.0 copy-start.2
  116.3 1.1 copy-start.1
  118.7 3.7 %copy-start.10 = (f32[8,4]{0,1:T(4,128)S(1)}, f32[8,4]{0,1:T(4,128)}, u32[]{:S(2)}) copy-start(f32[8,4]{0,1:T(4,128)} %param.30) | copy-start | bytes 388
  118.7 3.7 %copy-start.12 = (f32[8]{0:T(128)S(1)}, f32[8]{0:T(128)}, u32[]{:S(2)}) copy-start(f32[8]{0:T(128)} %reduce_sum.82) | copy-start | bytes 100
  118.7 3.8 %copy-start.16 = (bf16[2048,64]{0,1:T(8,128)(2,1)S(1)}, bf16[2048,64]{0,1:T(8,128)(2,1)}, u32[]{:S(2)}) copy-start(bf16[2048,64]{0,1:T(8,128)(2,1)} %param.20) | copy-start | bytes 786436
  118.7 3.8 %copy-start.18 = (f32[2048]{0:T(1024)S(1)}, f32[2048]{0:T(1024)}, u32[]{:S(2)}) copy-start(f32[2048]{0:T(1024)} %param.18) | copy-start | bytes 24580
  118.7 13.1 %all-to-all-start.3 = ((bf16[16,96,128]{2,1,0:T(8,128)(2,1)}), bf16[16,96,128]{2,1,0:T(8,128)(2,1)S(1)}, u32[]{:S(2)}, u32[]{:S(2)}) async-start(bf16[16,96,128]{2,1,0:T(8,128)(2,1)} %bitcast.85), calls=%async_computation.3 | async-start | bytes 786432 | tf_op jit(solution)/shard_map/all_to_all | solution.py:24
  122.5 0.7 copy-start.20
  123.9 13.7 %copy-start.17 = (bf16[2048,64]{0,1:T(8,128)(2,1)S(1)}, bf16[2048,64]{0,1:T(8,128)(2,1)}, u32[]{:S(2)}) copy-start(bf16[2048,64]{0,1:T(8,128)(2,1)} %param.21) | copy-start | bytes 786436
  132.5 17.4 %all-to-all-start.4 = ((bf16[32,3,128]{2,1,0:T(4,128)(2,1)}), bf16[32,3,128]{2,1,0:T(4,128)(2,1)S(1)}, u32[]{:S(2)}, u32[]{:S(2)}) async-start(bf16[32,3,128]{2,1,0:T(4,128)(2,1)} %reshape.180), calls=%async_computation.4 | async-start | bytes 65536 | tf_op jit(solution)/shard_map/all_to_all | solution.py:145
  138.5 11.5 %copy-start.8 = (s32[8,4]{0,1:T(4,128)S(1)}, s32[8,4]{0,1:T(4,128)}, u32[]{:S(2)}) copy-start(s32[8,4]{0,1:T(4,128)} %copy-done.7) | copy-start | bytes 388
where the time goes:
time: 151 us
  waiting for transfers between devices  60.6 us (40%)
  starting transfers between devices  35.2 us (23%)
  blocking collectives  27.6 us (18%)
  other arithmetic  12.2 us (8%)
  local copies, waits for them, and re-layouts  9.13 us (6%)
  matrix products  5.08 us (3%)
    all_to_all x1, waiting for transfers between devices, body(): lax.all_to_all(outgoing, 'ep', split_axis=0, concat_axis=0, tiled=True)  33 us
    all_to_all x1, starting transfers between devices, body(): lax.all_to_all(outgoing, 'ep', split_axis=0, concat_axis=0, tiled=True)  22.7 us
    all_to_all x1, blocking collectives, from_everyone(): lax.all_to_all(jnp.broadcast_to(x[None], (size, *x.shape)), axis, 0, 0, t...  13.8 us
    psum x2, blocking collectives, over_axes(): return functools.reduce(lax.psum, axes, x)  13.8 us
    all_to_all x1, waiting for transfers between devices, body(): lax.all_to_all(result.reshape(sources, items, -1), 'ep', split_axis=0, co...  11.4 us
    another operation x2, other arithmetic  10.1 us
    all_to_all x1, waiting for transfers between devices, from_everyone(): lax.all_to_all(jnp.broadcast_to(x[None], (size, *x.shape)), axis, 0, 0, t...  8.34 us
    all_to_all x1, waiting for transfers between devices, sum_at_owner(): parts = lax.all_to_all(cut_along(x, dim, size), axis, 0, 0, tiled=True)  7.89 us
  transfers between devices with their start and end apart: 4, of which 4 were waited for; matrix products, arithmetic and copies ran while one was open for 2% of the time, Pallas kernels for 0%

commit v1 on v0

v1 whole, which is shorter than its diff:
```python
import jax
import jax.numpy as jnp
from jax import lax
from jax.experimental import pallas as pl
from jax.experimental.pallas import tpu as pltpu
from jax.sharding import Mesh
from jax.sharding import PartitionSpec as P

TP = ("tp_0", "tp_1")

eps = 1e-06
limit = 7.0
alpha = 1.702
LANES = 128
SLOTS = 4
CAP = 3


def from_everyone(x, axis):
    size = lax.axis_size(axis)
    return lax.all_to_all(jnp.broadcast_to(x[None], (size, *x.shape)), axis, 0, 0, tiled=True)


def attend_kernel(lengths_ref, parts_ref, gain_ref, wq_ref, key_ref, value_ref, bias_ref,
                  mix_ref, wout_ref, normed_ref, out_ref):
    blocks, rows, lanes = parts_ref.shape
    heads = key_ref.shape[2]
    cache = key_ref.shape[3]
    xs = [parts_ref[t].astype(jnp.float32) for t in range(blocks)]
    total = xs[0] * xs[0]
    for x in xs[1:]:
        total = total + x * x
    width = blocks * lanes
    scale = lax.rsqrt(jnp.sum(total, axis=1, keepdims=True) / width + eps)
    normed = jnp.concatenate(
        [(xs[t] * scale * gain_ref[t : t + 1, :]).astype(jnp.bfloat16) for t in range(blocks)],
        axis=1,
    )
    normed_ref[...] = normed
    query = jnp.dot(normed, wq_ref[...], preferred_element_type=jnp.float32).astype(jnp.bfloat16)
    query = query.astype(jnp.float32)
    spread = jnp.concatenate([query] * rows, axis=1)
    row = lax.broadcasted_iota(jnp.int32, spread.shape, 0)
    own = lax.broadcasted_iota(jnp.int32, spread.shape, 1) // heads == row
    spread = jnp.where(own, spread, 0.0).astype(jnp.bfloat16)
    keys = key_ref[:, 0].reshape(rows * heads, cache)
    scores = jnp.dot(spread, keys, preferred_element_type=jnp.float32) * heads ** (-0.5)
    scores = scores + bias_ref[:, 0, :]
    line = lax.broadcasted_iota(jnp.int32, (rows, cache), 0)
    length = jnp.zeros((rows, cache), jnp.int32)
    for n in range(rows):
        length = jnp.where(line == n, lengths_ref[n], length)
    live = lax.broadcasted_iota(jnp.int32, (rows, cache), 1) < length
    soft = jnp.maximum(scores, 0.0) + jnp.log1p(jnp.exp(-jnp.abs(scores)))
    drop = jnp.where(live, soft, 0.0)
    chunks = cache // lanes
    stacked = jnp.concatenate([drop[:, c * lanes : (c + 1) * lanes] for c in range(chunks)], axis=0)
    below = lax.broadcasted_iota(jnp.int32, (lanes, lanes), 0)
    across = lax.broadcasted_iota(jnp.int32, (lanes, lanes), 1)
    later = (below > across).astype(jnp.bfloat16)
    high = stacked.astype(jnp.bfloat16)
    rest = stacked - high.astype(jnp.float32)
    middle = rest.astype(jnp.bfloat16)
    low = (rest - middle.astype(jnp.float32)).astype(jnp.bfloat16)
    after = (
        jnp.dot(high, later, preferred_element_type=jnp.float32)
        + jnp.dot(middle, later, preferred_element_type=jnp.float32)
        + jnp.dot(low, later, preferred_element_type=jnp.float32)
    )
    sums = jnp.sum(stacked, axis=1, keepdims=True)
    running = jnp.zeros((rows, 1), jnp.float32)
    pieces = [None] * chunks
    for c in reversed(range(chunks)):
        pieces[c] = after[c * rows : (c + 1) * rows] + running
        running = running + sums[c * rows : (c + 1) * rows]
    after = jnp.concatenate(pieces, axis=1)
    weights = jnp.where(live, jnp.exp(scores - soft - after), 0.0).astype(jnp.bfloat16)
    values = value_ref[:, 0].reshape(rows * heads, cache)
    crossed = lax.dot_general(
        weights, values, (((1,), (1,)), ((), ())), preferred_element_type=jnp.float32
    )
    crossed = jnp.where(own, crossed, 0.0)
    folded = crossed[:, :lanes]
    for c in range(1, crossed.shape[1] // lanes):
        folded = folded + crossed[:, c * lanes : (c + 1) * lanes]
    square = jnp.sum(folded * folded, axis=1, keepdims=True)
    attended = folded[:, :heads] + folded[:, heads : 2 * heads]
    ready = (attended * mix_ref[...]).astype(jnp.bfloat16)
    branch = jnp.dot(ready, wout_ref[...], preferred_element_type=jnp.float32)
    top = square.astype(jnp.bfloat16).astype(jnp.float32)
    half = lax.broadcasted_iota(jnp.int32, (rows, lanes), 1) < lanes // 2
    tail = jnp.where(half, top, square - top)
    for t in range(blocks):
        both = jnp.concatenate([branch[:, t * lanes : (t + 1) * lanes], tail], axis=0)
        out_ref[t] = both.astype(jnp.bfloat16)


def expert_kernel(rows_ref, gain_ref, gate_ref, up_ref, down_ref, out_ref):
    blocks, rows, lanes = rows_ref.shape
    total = jnp.zeros((rows, lanes), jnp.float32)
    scaled = []
    for t in range(blocks):
        x = rows_ref[t].astype(jnp.float32)
        total = total + x * x
        scaled.append((x * gain_ref[t : t + 1, :]).astype(jnp.bfloat16))
    scaled = jnp.concatenate(scaled, axis=1)
    scale = lax.rsqrt(jnp.sum(total, axis=1, keepdims=True) / (blocks * lanes) + eps)
    gate = jnp.dot(scaled, gate_ref[0], preferred_element_type=jnp.float32) * scale
    upper = jnp.dot(scaled, up_ref[0], preferred_element_type=jnp.float32) * scale
    gate = jnp.minimum(gate, limit)
    upper = jnp.clip(upper, -limit, limit)
    active = ((upper + 1.0) * gate * jax.nn.sigmoid(alpha * gate)).astype(jnp.bfloat16)
    result = jnp.dot(active, down_ref[0], preferred_element_type=jnp.float32).astype(jnp.bfloat16)
    for t in range(blocks):
        out_ref[t] = result[:, t * lanes : (t + 1) * lanes]


def vmem():
    return pl.BlockSpec(memory_space=pltpu.VMEM)


def body(
    resid,
    attn_gain,
    w_query,
    w_key,
    w_value,
    key_cache,
    value_cache,
    key_bias,
    lengths,
    mix_gain,
    w_out,
    ffn_gain,
    route_experts,
    route_weights,
    w_gate,
    w_up,
    w_down,
):
    blocks = lax.axis_size(TP)
    rows, lanes = resid.shape
    width = blocks * lanes
    parts = from_everyone(resid, TP)
    normed_in, partial_branch = pl.pallas_call(
        attend_kernel,
        in_specs=[pl.BlockSpec(memory_space=pltpu.SMEM)] + [vmem()] * 8,
        out_specs=[vmem(), vmem()],
        out_shape=[
            jax.ShapeDtypeStruct((rows, width), jnp.bfloat16),
            jax.ShapeDtypeStruct((blocks, 2 * rows, lanes), jnp.bfloat16),
        ],
        name="attend",
    )(
        lengths,
        parts,
        attn_gain.reshape(blocks, lanes),
        w_query,
        key_cache,
        value_cache,
        key_bias,
        mix_gain.reshape(1, -1),
        w_out,
    )
    new_keys = jnp.dot(normed_in, w_key, preferred_element_type=jnp.float32).astype(jnp.bfloat16)
    new_values = jnp.dot(normed_in, w_value, preferred_element_type=jnp.float32).astype(
        jnp.bfloat16
    )
    summed = jnp.sum(
        lax.all_to_all(partial_branch, TP, 0, 0, tiled=True).astype(jnp.float32), axis=0
    )
    channels = mix_gain.shape[0] * blocks
    square = summed[rows:, :1] + summed[rows:, lanes - 1 :]
    middle = resid.astype(jnp.float32) + summed[:rows] * lax.rsqrt(square / channels + eps)

    top = route_experts.shape[1]
    share = route_weights / jnp.sum(route_weights, axis=1, keepdims=True)
    groups = lax.axis_size("ep")
    experts_all = w_gate.shape[0] * groups
    count = rows * top
    position = lax.broadcasted_iota(jnp.int32, (count, count), 0)
    later = position > position.T
    chosen = route_experts.reshape(-1)
    earlier = (chosen[:, None] == chosen[None, :]) & later
    rank = jnp.sum(earlier.astype(jnp.int32), axis=1)
    target = chosen * SLOTS + rank
    slots_total = experts_all * SLOTS
    slot_iota = lax.broadcasted_iota(jnp.int32, (slots_total, rows, top), 0)
    dispatch = jnp.any(slot_iota == target.reshape(rows, top)[None], axis=2).astype(jnp.bfloat16)
    outgoing = jnp.dot(
        dispatch, middle.astype(jnp.bfloat16), preferred_element_type=jnp.float32
    ).astype(jnp.bfloat16)
    arrived = lax.all_to_all(
        outgoing.reshape(experts_all, SLOTS, lanes), "ep", split_axis=0, concat_axis=0, tiled=True
    )
    items = groups * CAP
    item = lax.broadcasted_iota(jnp.int32, (items, slots_total), 0)
    slot = lax.broadcasted_iota(jnp.int32, (items, slots_total), 1)
    packed = (item // CAP * SLOTS + item % CAP == slot).astype(jnp.bfloat16)
    held = jnp.dot(
        packed, arrived.reshape(slots_total, lanes), preferred_element_type=jnp.float32
    ).astype(jnp.bfloat16)
    gathered = from_everyone(held, TP)
    partial_out = pl.pallas_call(
        expert_kernel,
        in_specs=[vmem()] * 5,
        out_specs=vmem(),
        out_shape=jax.ShapeDtypeStruct((blocks, items, lanes), jnp.bfloat16),
        name="expert",
    )(gathered, ffn_gain.reshape(blocks, lanes), w_gate, w_up, w_down)
    result = jnp.sum(
        lax.all_to_all(partial_out, TP, 0, 0, tiled=True).astype(jnp.float32), axis=0
    ).astype(jnp.bfloat16)
    spaced = jnp.dot(packed.T, result, preferred_element_type=jnp.float32).astype(jnp.bfloat16)
    returned = lax.all_to_all(
        spaced.reshape(groups, SLOTS, lanes), "ep", split_axis=0, concat_axis=0, tiled=True
    )
    picker = (target[:, None] == lax.broadcasted_iota(jnp.int32, (count, slots_total), 1)).astype(
        jnp.bfloat16
    )
    picked = jnp.dot(
        picker, returned.reshape(slots_total, lanes), preferred_element_type=jnp.float32
    ).reshape(rows, top, lanes)
    mixture = jnp.sum(share[:, :, None] * picked, axis=1)
    mixed = (middle + mixture).astype(jnp.bfloat16)
    return (mixed, new_keys, new_values)


def solution(mesh):
    torus = Mesh(mesh.devices.reshape(mesh.shape["ep"], 4, 4), ("ep", "tp_0", "tp_1"))
    in_specs = (
        P("ep", TP),
        P(),
        P(None, TP),
        P(None, TP),
        P(None, TP),
        P("ep", TP, None, None),
        P("ep", TP, None, None),
        P("ep", TP, None),
        P("ep"),
        P(TP),
        P(TP, None),
        P(),
        P("ep", None),
        P("ep", None),
        P("ep", None, TP),
        P("ep", None, TP),
        P("ep", TP, None),
    )
    out_specs = (P("ep", TP), P("ep", TP), P("ep", TP))
    return jax.shard_map(body, mesh=torus, in_specs=in_specs, out_specs=out_specs, check_vma=False)
```

time: 151 us -> 113 us (0.75)
  blocking collectives: 27.6 us -> 0 us
  other arithmetic: 12.2 us -> 1.24 us
  waiting for transfers between devices: 60.6 us -> 50.4 us
  starting transfers between devices: 35.2 us -> 43.5 us
  Pallas kernels: 0 us -> 6.55 us
  local copies, waits for them, and re-layouts: 9.13 us -> 6.29 us
    all_to_all x3 -> x4, waiting for transfers between devices: 52.3 us -> 37.5 us  [the longest x1 12 us: body(): lax.all_to_all(outgoing.reshape(experts_all, SLOTS, lanes), 'ep', split_a...]
    all_to_all x1 -> x0, blocking collectives: 13.8 us -> none  [from_everyone(): lax.all_to_all(jnp.broadcast_to(x[None], (size, *x.shape)), axis, 0, 0, t...]
    psum x2 -> x0, blocking collectives: 13.8 us -> none  [over_axes(): return functools.reduce(lax.psum, axes, x)]
    another operation x2 -> x0, other arithmetic: 10.1 us -> none
    all_to_all x1 -> x2, starting transfers between devices: 3.7 us -> 11.4 us  [from_everyone(): lax.all_to_all(jnp.broadcast_to(x[None], (size, *x.shape)), axis, 0, 0, t...]
    pallas_call x0 -> x2, Pallas kernels: none -> 6.55 us  [the longest x1 3.72 us: body(): pl.pallas_call(attend_kernel, in_specs=[pl.BlockSpec(memory_space=pltpu.S...]
    all_to_all x1 -> x2, waiting for transfers between devices: 8.34 us -> 12.8 us  [from_everyone(): lax.all_to_all(jnp.broadcast_to(x[None], (size, *x.shape)), axis, 0, 0, t...]
    reshape x5 -> x0, local copies, waits for them, and re-layouts: 2.81 us -> none  [the longest x1 1.03 us: body(): outgoing = outgoing.reshape(experts_all, capacity, model_width)]
  transfers between devices with their start and end apart: 4 -> 6, of which waited for: 4 -> 6; matrix products, arithmetic and copies ran while one was open for 2% -> 4% of each run, Pallas kernels for 0% -> 0%
where the time goes in v1:
time: 113 us
  waiting for transfers between devices  50.4 us (45%)
  starting transfers between devices  43.5 us (38%)
  Pallas kernels  6.55 us (6%)
  local copies, waits for them, and re-layouts  6.29 us (6%)
  matrix products  3.76 us (3%)
  other arithmetic  1.24 us (1%)
    all_to_all x1, starting transfers between devices, body(): lax.all_to_all(outgoing.reshape(experts_all, SLOTS, lanes), 'ep', split_a...  18.5 us
    all_to_all x2, waiting for transfers between devices, from_everyone(): lax.all_to_all(jnp.broadcast_to(x[None], (size, *x.shape)), axis, 0, 0, t...  12.8 us
    all_to_all x1, waiting for transfers between devices, body(): lax.all_to_all(outgoing.reshape(experts_all, SLOTS, lanes), 'ep', split_a...  12 us
    all_to_all x1, waiting for transfers between devices, body(): lax.all_to_all(spaced.reshape(groups, SLOTS, lanes), 'ep', split_axis=0,...  11.5 us
    all_to_all x2, starting transfers between devices, from_everyone(): lax.all_to_all(jnp.broadcast_to(x[None], (size, *x.shape)), axis, 0, 0, t...  11.4 us
    all_to_all x1, waiting for transfers between devices, body(): lax.all_to_all(partial_out, TP, 0, 0, tiled=True).astype(jnp.float32)  7.58 us
    all_to_all x1, starting transfers between devices, body(): lax.all_to_all(spaced.reshape(groups, SLOTS, lanes), 'ep', split_axis=0,...  6.45 us
    all_to_all x1, waiting for transfers between devices, body(): lax.all_to_all(partial_branch, TP, 0, 0, tiled=True).astype(jnp.float32)  6.44 us
  transfers between devices with their start and end apart: 6, of which 6 were waited for; matrix products, arithmetic and copies ran while one was open for 4% of the time, Pallas kernels for 0%

profile of v1, /device:TPU:1, one launch (start us, length us, event | category | flops | bytes accessed | tf_op | source)
XLA Modules:
  0.0 112.5 jit_solution(16662290788769346288)
XLA Ops:
  0.6 1.3 %broadcast_in_dim.4 = bf16[16,8,128]{2,1,0:T(8,128)(2,1)} broadcast(bf16[8,128]{1,0:T(8,128)(2,1)} %param.17), dimensions={1,2} | broadcast | bytes 34816 | tf_op jit(solution)/shard_map/broadcast_in_dim | solution.py:21
  2.0 7.7 %all-to-all-start = ((bf16[16,8,128]{2,1,0:T(8,128)(2,1)}), bf16[16,8,128]{2,1,0:T(8,128)(2,1)S(1)}, u32[]{:S(2)}, u32[]{:S(2)}) async-start(bf16[16,8,128]{2,1,0:T(8,128)(2,1)} %broadcast_in_dim.4), calls=%async_computation | async-start | bytes 65536 | tf_op jit(solution)/shard_map/all_to_all | solution.py:21
  9.7 0.1 copy.29
  9.8 0.1 eq.54
  9.9 0.2 convert_reduce_fusion.1
  10.1 0.1 copy.31
  10.3 2.0 %copy.28.wq_ref = bf16[2048,64]{1,0:T(8,128)(2,1)} copy(bf16[2048,64]{0,1:T(8,128)(2,1)} %param.19) | data formatting | bytes 524288 | tf_op args[2]
  12.3 3.9 %all-to-all-done.parts_ref = bf16[16,8,128]{2,1,0:T(8,128)(2,1)S(1)} async-done(((bf16[16,8,128]{2,1,0:T(8,128)(2,1)}), bf16[16,8,128]{2,1,0:T(8,128)(2,1)S(1)}, u32[]{:S(2)}, u32[]{:S(2)}) %all-to-all-start) | async-done | bytes 32800 | tf_op jit(solution)/shard_map/all_to_all | solution.py:21
  16.1 0.6 copy-done.3
  16.7 3.7 %attend.1 = (bf16[8,2048]{1,0:T(8,128)(2,1)}, bf16[16,16,128]{2,1,0:T(8,128)(2,1)}) custom-call(s32[8]{0:T(128)} %lengths_ref.1, bf16[16,8,128]{2,1,0:T(8,128)(2,1)} %copy-done.3, f32[16,128]{1,0:T(8,128)} %bitcast.28, bf16[2048,64]{1,0:T(8,128)(2,1)} %copy.28.wq_ref, bf16[8,1,64,1024]{3,2,1,0:T(8,128)(2,1)} %key_ref.1, bf16[8,1,64,1024]{3,2,1,0:T(8,128)(2,1)} %value_ref.1, ...), custom_call_target="tpu_custom_call" | custom-call | tf_op jit(solution)/shard_map/attend/pallas_call | solution.py:145
  20.5 3.5 %all-to-all-start.1 = ((bf16[16,16,128]{2,1,0:T(8,128)(2,1)}), bf16[16,16,128]{2,1,0:T(8,128)(2,1)S(1)}, u32[]{:S(2)}, u32[]{:S(2)}) async-start(bf16[16,16,128]{2,1,0:T(8,128)(2,1)} %get-tuple-element.5), calls=%async_computation.1 | async-start | bytes 131072 | tf_op jit(solution)/shard_map/all_to_all | solution.py:170
  24.0 6.4 %all-to-all-done.1 = bf16[16,16,128]{2,1,0:T(8,128)(2,1)S(1)} async-done(((bf16[16,16,128]{2,1,0:T(8,128)(2,1)}), bf16[16,16,128]{2,1,0:T(8,128)(2,1)S(1)}, u32[]{:S(2)}, u32[]{:S(2)}) %all-to-all-start.1) | async-done | bytes 65568 | tf_op jit(solution)/shard_map/all_to_all | solution.py:170
  30.5 0.2 fusion.9
  30.6 0.5 copy-done.5
  31.1 0.8 convolution_convert_fusion.1
  32.0 18.5 %all-to-all-start.2 = ((bf16[32,4,128]{2,1,0:T(4,128)(2,1)}), bf16[32,4,128]{2,1,0:T(4,128)(2,1)S(1)}, u32[]{:S(2)}, u32[]{:S(2)}) async-start(bf16[32,4,128]{2,1,0:T(4,128)(2,1)} %bitcast.4), calls=%async_computation.2 | async-start | bytes 65536 | tf_op jit(solution)/shard_map/all_to_all | solution.py:193
  50.5 12.0 %all-to-all-done.2 = bf16[32,4,128]{2,1,0:T(4,128)(2,1)S(1)} async-done(((bf16[32,4,128]{2,1,0:T(4,128)(2,1)}), bf16[32,4,128]{2,1,0:T(4,128)(2,1)S(1)}, u32[]{:S(2)}, u32[]{:S(2)}) %all-to-all-start.2) | async-done | bytes 32800 | tf_op jit(solution)/shard_map/all_to_all | solution.py:193
  62.5 0.3 convolution_convert_fusion.2
  62.8 0.8 broadcast_in_dim.5
  63.6 3.7 %all-to-all-start.3 = ((bf16[16,96,128]{2,1,0:T(8,128)(2,1)}), bf16[16,96,128]{2,1,0:T(8,128)(2,1)S(1)}, u32[]{:S(2)}, u32[]{:S(2)}) async-start(bf16[16,96,128]{2,1,0:T(8,128)(2,1)} %broadcast_in_dim.5), calls=%async_computation.3 | async-start | bytes 786432 | tf_op jit(solution)/shard_map/all_to_all | solution.py:21
  67.3 9.0 %all-to-all-done.3.rows_ref = bf16[16,96,128]{2,1,0:T(8,128)(2,1)S(1)} async-done(((bf16[16,96,128]{2,1,0:T(8,128)(2,1)}), bf16[16,96,128]{2,1,0:T(8,128)(2,1)S(1)}, u32[]{:S(2)}, u32[]{:S(2)}) %all-to-all-start.3) | async-done | bytes 393248 | tf_op jit(solution)/shard_map/all_to_all | solution.py:21
  76.3 0.7 copy-done.1
  77.0 2.8 %expert.1 = bf16[16,96,128]{2,1,0:T(8,128)(2,1)} custom-call(bf16[16,96,128]{2,1,0:T(8,128)(2,1)} %copy-done.1, f32[16,128]{1,0:T(8,128)} %bitcast.29, bf16[1,2048,128]{2,1,0:T(8,128)(2,1)} %gate_ref.1, bf16[1,2048,128]{2,1,0:T(8,128)(2,1)} %up_ref.1, bf16[1,128,2048]{2,1,0:T(8,128)(2,1)} %down_ref.1), custom_call_target="tpu_custom_call" | custom-call | tf_op jit(solution)/shard_map/expert/pallas_call | solution.py:204
  79.9 3.7 %all-to-all-start.4 = ((bf16[16,96,128]{2,1,0:T(8,128)(2,1)}), bf16[16,96,128]{2,1,0:T(8,128)(2,1)S(1)}, u32[]{:S(2)}, u32[]{:S(2)}) async-start(bf16[16,96,128]{2,1,0:T(8,128)(2,1)} %expert.1), calls=%async_computation.4 | async-start | bytes 786432 | tf_op jit(solution)/shard_map/all_to_all | solution.py:212
  83.6 0.8 convolution_convert_fusion.3
  84.4 7.6 %all-to-all-done.4 = bf16[16,96,128]{2,1,0:T(8,128)(2,1)S(1)} async-done(((bf16[16,96,128]{2,1,0:T(8,128)(2,1)}), bf16[16,96,128]{2,1,0:T(8,128)(2,1)S(1)}, u32[]{:S(2)}, u32[]{:S(2)}) %all-to-all-start.4) | async-done | bytes 393248 | tf_op jit(solution)/shard_map/all_to_all | solution.py:212
  92.0 0.9 convolution_convert_fusion
  93.0 6.4 %all-to-all-start.5 = ((bf16[32,4,128]{2,1,0:T(4,128)(2,1)}), bf16[32,4,128]{2,1,0:T(4,128)(2,1)S(1)}, u32[]{:S(2)}, u32[]{:S(2)}) async-start(bf16[32,4,128]{2,1,0:T(4,128)(2,1)} %bitcast.7), calls=%async_computation.5 | async-start | bytes 65536 | tf_op jit(solution)/shard_map/all_to_all | solution.py:215
  99.4 0.8 convolution_convert_fusion.4
  100.2 11.5 %all-to-all-done.5 = bf16[32,4,128]{2,1,0:T(4,128)(2,1)S(1)} async-done(((bf16[32,4,128]{2,1,0:T(4,128)(2,1)}), bf16[32,4,128]{2,1,0:T(4,128)(2,1)S(1)}, u32[]{:S(2)}, u32[]{:S(2)}) %all-to-all-start.5) | async-done | bytes 32800 | tf_op jit(solution)/shard_map/all_to_all | solution.py:215
  111.7 0.2 fusion
  111.9 0.7 add_convert_fusion
  (23 shorter events, 0.3 us)
Async XLA Ops:
  0.6 82.9 %copy-start = (bf16[2048,64]{0,1:T(8,128)(2,1)S(1)}, bf16[2048,64]{0,1:T(8,128)(2,1)}, u32[]{:S(2)}) copy-start(bf16[2048,64]{0,1:T(8,128)(2,1)} %param.21) | copy-start | bytes 786436
  2.0 7.7 %copy-start.7 = (s32[8,4]{0,1:T(4,128)S(1)}, s32[8,4]{0,1:T(4,128)}, u32[]{:S(2)}) copy-start(s32[8,4]{0,1:T(4,128)} %param.29) | copy-start | bytes 388
  2.0 14.2 %all-to-all-start = ((bf16[16,8,128]{2,1,0:T(8,128)(2,1)}), bf16[16,8,128]{2,1,0:T(8,128)(2,1)S(1)}, u32[]{:S(2)}, u32[]{:S(2)}) async-start(bf16[16,8,128]{2,1,0:T(8,128)(2,1)} %broadcast_in_dim.4), calls=%async_computation | async-start | bytes 65536 | tf_op jit(solution)/shard_map/all_to_all | solution.py:21
  16.1 0.6 copy-start.3
  20.5 10.0 %all-to-all-start.1 = ((bf16[16,16,128]{2,1,0:T(8,128)(2,1)}), bf16[16,16,128]{2,1,0:T(8,128)(2,1)S(1)}, u32[]{:S(2)}, u32[]{:S(2)}) async-start(bf16[16,16,128]{2,1,0:T(8,128)(2,1)} %get-tuple-element.5), calls=%async_computation.1 | async-start | bytes 131072 | tf_op jit(solution)/shard_map/all_to_all | solution.py:170
  30.4 0.7 copy-start.5
  32.0 30.6 %all-to-all-start.2 = ((bf16[32,4,128]{2,1,0:T(4,128)(2,1)}), bf16[32,4,128]{2,1,0:T(4,128)(2,1)S(1)}, u32[]{:S(2)}, u32[]{:S(2)}) async-start(bf16[32,4,128]{2,1,0:T(4,128)(2,1)} %bitcast.4), calls=%async_computation.2 | async-start | bytes 65536 | tf_op jit(solution)/shard_map/all_to_all | solution.py:193
  63.6 3.7 %copy-start.6 = (f32[8,4]{0,1:T(4,128)S(1)}, f32[8,4]{0,1:T(4,128)}, u32[]{:S(2)}) copy-start(f32[8,4]{0,1:T(4,128)} %param.30) | copy-start | bytes 388
  63.6 12.7 %all-to-all-start.3 = ((bf16[16,96,128]{2,1,0:T(8,128)(2,1)}), bf16[16,96,128]{2,1,0:T(8,128)(2,1)S(1)}, u32[]{:S(2)}, u32[]{:S(2)}) async-start(bf16[16,96,128]{2,1,0:T(8,128)(2,1)} %broadcast_in_dim.5), calls=%async_computation.3 | async-start | bytes 786432 | tf_op jit(solution)/shard_map/all_to_all | solution.py:21
  76.3 0.7 copy-start.1
  79.9 3.7 %copy-start.4 = (bf16[8,2048]{1,0:T(8,128)(2,1)S(1)}, bf16[8,2048]{1,0:T(8,128)(2,1)}, u32[]{:S(2)}) copy-start(bf16[8,2048]{1,0:T(8,128)(2,1)} %get-tuple-element.6) | copy-start | bytes 98308
  79.9 12.1 %all-to-all-start.4 = ((bf16[16,96,128]{2,1,0:T(8,128)(2,1)}), bf16[16,96,128]{2,1,0:T(8,128)(2,1)S(1)}, u32[]{:S(2)}, u32[]{:S(2)}) async-start(bf16[16,96,128]{2,1,0:T(8,128)(2,1)} %expert.1), calls=%async_computation.4 | async-start | bytes 786432 | tf_op jit(solution)/shard_map/all_to_all | solution.py:212
  92.0 7.4 %copy-start.2 = (bf16[2048,64]{0,1:T(8,128)(2,1)S(1)}, bf16[2048,64]{0,1:T(8,128)(2,1)}, u32[]{:S(2)}) copy-start(bf16[2048,64]{0,1:T(8,128)(2,1)} %param.20) | copy-start | bytes 786436
  93.0 18.7 %all-to-all-start.5 = ((bf16[32,4,128]{2,1,0:T(4,128)(2,1)}), bf16[32,4,128]{2,1,0:T(4,128)(2,1)S(1)}, u32[]{:S(2)}, u32[]{:S(2)}) async-start(bf16[32,4,128]{2,1,0:T(4,128)(2,1)} %bitcast.7), calls=%async_computation.5 | async-start | bytes 65536 | tf_op jit(solution)/shard_map/all_to_all | solution.py:215

commit v2 on v1

--- a/solution.py
+++ b/solution.py
@@ -14,15 +14,19 @@
 LANES = 128
 SLOTS = 4
 CAP = 3
-
-
-def from_everyone(x, axis):
-    size = lax.axis_size(axis)
-    return lax.all_to_all(jnp.broadcast_to(x[None], (size, *x.shape)), axis, 0, 0, tiled=True)
-
-
-def attend_kernel(lengths_ref, parts_ref, gain_ref, wq_ref, key_ref, value_ref, bias_ref,
-                  mix_ref, wout_ref, normed_ref, out_ref):
+LIMIT = 16 * 1024 * 1024
+LONG = 4 * 10**10
+SHORT = 10**9
+
+
+def project(rows, weight_ref):
+    return lax.dot_general(
+        rows, weight_ref[...], (((1,), (1,)), ((), ())), preferred_element_type=jnp.float32
+    ).astype(jnp.bfloat16)
+
+
+def attend_kernel(lengths_ref, parts_ref, gain_ref, wq_ref, wk_ref, wv_ref, key_ref, value_ref,
+                  bias_ref, mix_ref, wout_ref, new_key_ref, new_value_ref, out_ref):
     blocks, rows, lanes = parts_ref.shape
     heads = key_ref.shape[2]
     cache = key_ref.shape[3]
@@ -36,9 +40,7 @@
         [(xs[t] * scale * gain_ref[t : t + 1, :]).astype(jnp.bfloat16) for t in range(blocks)],
         axis=1,
     )
-    normed_ref[...] = normed
-    query = jnp.dot(normed, wq_ref[...], preferred_element_type=jnp.float32).astype(jnp.bfloat16)
-    query = query.astype(jnp.float32)
+    query = project(normed, wq_ref).astype(jnp.float32)
     spread = jnp.concatenate([query] * rows, axis=1)
     row = lax.broadcasted_iota(jnp.int32, spread.shape, 0)
     own = lax.broadcasted_iota(jnp.int32, spread.shape, 1) // heads == row
@@ -93,6 +95,106 @@
     for t in range(blocks):
         both = jnp.concatenate([branch[:, t * lanes : (t + 1) * lanes], tail], axis=0)
         out_ref[t] = both.astype(jnp.bfloat16)
+    new_key_ref[...] = project(normed, wk_ref)
+    new_value_ref[...] = project(normed, wv_ref)
+
+
+def chosen_slots(experts_ref, slots):
+    top, rows = experts_ref.shape
+    slot = lax.broadcasted_iota(jnp.int32, (slots, rows), 0)
+    hits = [experts_ref[k : k + 1, :] == slot // SLOTS for k in range(top)]
+    named = hits[0]
+    for hit in hits[1:]:
+        named = named | hit
+    first = lax.broadcasted_iota(jnp.int32, (rows, rows), 0)
+    second = lax.broadcasted_iota(jnp.int32, (rows, rows), 1)
+    earlier = (first < second).astype(jnp.bfloat16)
+    rank = jnp.dot(
+        named.astype(jnp.bfloat16), earlier, preferred_element_type=jnp.float32
+    ).astype(jnp.int32)
+    return hits, named & (rank == slot % SLOTS)
+
+
+def copies_kernel(row_ref, out_ref):
+    for t in range(out_ref.shape[0]):
+        out_ref[t] = row_ref[...]
+
+
+def middle_kernel(parts_ref, resid_ref, experts_ref, middle_ref, out_ref):
+    blocks, both, lanes = parts_ref.shape
+    rows = both // 2
+    total = parts_ref[0].astype(jnp.float32)
+    for t in range(1, blocks):
+        total = total + parts_ref[t].astype(jnp.float32)
+    square = total[rows:, :1] + total[rows:, lanes - 1 :]
+    channels = blocks * (lanes // 2)
+    scale = lax.rsqrt(square / channels + eps)
+    middle = resid_ref[...].astype(jnp.float32) + total[:rows] * scale
+    middle_ref[...] = middle
+    groups, slots, _ = out_ref.shape
+    _, placed = chosen_slots(experts_ref, groups * slots)
+    out = jnp.dot(
+        placed.astype(jnp.bfloat16),
+        middle.astype(jnp.bfloat16),
+        preferred_element_type=jnp.float32,
+    )
+    out_ref[...] = out.reshape(groups, slots, lanes).astype(jnp.bfloat16)
+
+
+def packing(items, slots):
+    item = lax.broadcasted_iota(jnp.int32, (items, slots), 0)
+    slot = lax.broadcasted_iota(jnp.int32, (items, slots), 1)
+    return (item // CAP * SLOTS + item % CAP == slot).astype(jnp.bfloat16)
+
+
+def spread_kernel(arrived_ref, out_ref):
+    blocks, items, lanes = out_ref.shape
+    groups, slots, _ = arrived_ref.shape
+    arrived = arrived_ref[...].astype(jnp.float32).reshape(groups * slots, lanes)
+    held = jnp.dot(
+        packing(items, groups * slots),
+        arrived.astype(jnp.bfloat16),
+        preferred_element_type=jnp.float32,
+    ).astype(jnp.bfloat16)
+    for t in range(blocks):
+        out_ref[t] = held
+
+
+def total_kernel(parts_ref, out_ref):
+    blocks, items, lanes = parts_ref.shape
+    groups, slots, _ = out_ref.shape
+    total = parts_ref[0].astype(jnp.float32)
+    for t in range(1, blocks):
+        total = total + parts_ref[t].astype(jnp.float32)
+    spaced = lax.dot_general(
+        packing(items, groups * slots),
+        total.astype(jnp.bfloat16),
+        (((0,), (0,)), ((), ())),
+        preferred_element_type=jnp.float32,
+    )
+    out_ref[...] = spaced.reshape(groups, slots, lanes).astype(jnp.bfloat16)
+
+
+def mixture_kernel(returned_ref, middle_ref, experts_ref, share_ref, out_ref):
+    groups, slots, lanes = returned_ref.shape
+    hits, placed = chosen_slots(experts_ref, groups * slots)
+    share = share_ref[...]
+    share = share / jnp.sum(share, axis=0, keepdims=True)
+    weight = jnp.where(hits[0], share[:1, :], 0.0)
+    for k in range(1, len(hits)):
+        weight = weight + jnp.where(hits[k], share[k : k + 1, :], 0.0)
+    weight = jnp.where(placed, weight, 0.0)
+    high = weight.astype(jnp.bfloat16)
+    low = (weight - high.astype(jnp.float32)).astype(jnp.bfloat16)
+    returned = returned_ref[...].astype(jnp.float32).reshape(groups * slots, lanes)
+    returned = returned.astype(jnp.bfloat16)
+    mixture = sum(
+        lax.dot_general(
+            part, returned, (((0,), (0,)), ((), ())), preferred_element_type=jnp.float32
+        )
+        for part in (high, low)
+    )
+    out_ref[...] = (middle_ref[...] + mixture).astype(jnp.bfloat16)
 
 
 def expert_kernel(rows_ref, gain_ref, gate_ref, up_ref, down_ref, out_ref):
@@ -117,6 +219,24 @@
 
 def vmem():
     return pl.BlockSpec(memory_space=pltpu.VMEM)
+
+
+def local(kernel, name, out_shape, *args, scalars=0, flops=0):
+    single = not isinstance(out_shape, list)
+    specs = [pl.BlockSpec(memory_space=pltpu.SMEM)] * scalars + [vmem()] * (len(args) - scalars)
+    return pl.pallas_call(
+        kernel,
+        in_specs=specs,
+        out_specs=vmem() if single else [vmem()] * len(out_shape),
+        out_shape=out_shape,
+        compiler_params=pltpu.CompilerParams(vmem_limit_bytes=LIMIT),
+        cost_estimate=pl.CostEstimate(flops=flops, bytes_accessed=0, transcendentals=0),
+        name=name,
+    )(*args)
+
+
+def exchange(x, axis):
+    return lax.all_to_all(x, axis, 0, 0, tiled=True)
 
 
 def body(
@@ -139,90 +259,75 @@
     w_down,
 ):
     blocks = lax.axis_size(TP)
+    groups = lax.axis_size("ep")
     rows, lanes = resid.shape
-    width = blocks * lanes
-    parts = from_everyone(resid, TP)
-    normed_in, partial_branch = pl.pallas_call(
+    heads = mix_gain.shape[0]
+    items = groups * CAP
+    bf16 = jnp.bfloat16
+    shape = jax.ShapeDtypeStruct
+    new = shape((rows, heads), bf16)
+    experts = route_experts.T
+    copies = local(copies_kernel, "copies", shape((blocks, rows, lanes), bf16), resid, flops=LONG)
+    parts = exchange(copies, TP)
+    new_keys, new_values, partial_branch = local(
         attend_kernel,
-        in_specs=[pl.BlockSpec(memory_space=pltpu.SMEM)] + [vmem()] * 8,
-        out_specs=[vmem(), vmem()],
-        out_shape=[
-            jax.ShapeDtypeStruct((rows, width), jnp.bfloat16),
-            jax.ShapeDtypeStruct((blocks, 2 * rows, lanes), jnp.bfloat16),
-        ],
-        name="attend",
-    )(
+        "attend",
+        [new, new, shape((blocks, 2 * rows, lanes), bf16)],
         lengths,
         parts,
         attn_gain.reshape(blocks, lanes),
-        w_query,
+        w_query.T,
+        w_key.T,
+        w_value.T,
         key_cache,
         value_cache,
         key_bias,
-        mix_gain.reshape(1, -1),
+        mix_gain.reshape(1, heads),
         w_out,
-    )
-    new_keys = jnp.dot(normed_in, w_key, preferred_element_type=jnp.float32).astype(jnp.bfloat16)
-    new_values = jnp.dot(normed_in, w_value, preferred_element_type=jnp.float32).astype(
-        jnp.bfloat16
-    )
-    summed = jnp.sum(
-        lax.all_to_all(partial_branch, TP, 0, 0, tiled=True).astype(jnp.float32), axis=0
-    )
-    channels = mix_gain.shape[0] * blocks
-    square = summed[rows:, :1] + summed[rows:, lanes - 1 :]
-    middle = resid.astype(jnp.float32) + summed[:rows] * lax.rsqrt(square / channels + eps)
-
-    top = route_experts.shape[1]
-    share = route_weights / jnp.sum(route_weights, axis=1, keepdims=True)
-    groups = lax.axis_size("ep")
-    experts_all = w_gate.shape[0] * groups
-    count = rows * top
-    position = lax.broadcasted_iota(jnp.int32, (count, count), 0)
-    later = position > position.T
-    chosen = route_experts.reshape(-1)
-    earlier = (chosen[:, None] == chosen[None, :]) & later
-    rank = jnp.sum(earlier.astype(jnp.int32), axis=1)
-    target = chosen * SLOTS + rank
-    slots_total = experts_all * SLOTS
-    slot_iota = lax.broadcasted_iota(jnp.int32, (slots_total, rows, top), 0)
-    dispatch = jnp.any(slot_iota == target.reshape(rows, top)[None], axis=2).astype(jnp.bfloat16)
-    outgoing = jnp.dot(
-        dispatch, middle.astype(jnp.bfloat16), preferred_element_type=jnp.float32
-    ).astype(jnp.bfloat16)
-    arrived = lax.all_to_all(
-        outgoing.reshape(experts_all, SLOTS, lanes), "ep", split_axis=0, concat_axis=0, tiled=True
-    )
-    items = groups * CAP
-    item = lax.broadcasted_iota(jnp.int32, (items, slots_total), 0)
-    slot = lax.broadcasted_iota(jnp.int32, (items, slots_total), 1)
-    packed = (item // CAP * SLOTS + item % CAP == slot).astype(jnp.bfloat16)
-    held = jnp.dot(
-        packed, arrived.reshape(slots_total, lanes), preferred_element_type=jnp.float32
-    ).astype(jnp.bfloat16)
-    gathered = from_everyone(held, TP)
-    partial_out = pl.pallas_call(
+        scalars=1,
+    )
+    middle, outgoing = local(
+        middle_kernel,
+        "middle",
+        [shape((rows, lanes), jnp.float32), shape((groups, SLOTS, lanes), bf16)],
+        exchange(partial_branch, TP),
+        resid,
+        experts,
+        flops=SHORT,
+    )
+    held = local(
+        spread_kernel,
+        "spread",
+        shape((blocks, items, lanes), bf16),
+        exchange(outgoing, "ep"),
+        flops=SHORT,
+    )
+    partial_out = local(
         expert_kernel,
-        in_specs=[vmem()] * 5,
-        out_specs=vmem(),
-        out_shape=jax.ShapeDtypeStruct((blocks, items, lanes), jnp.bfloat16),
-        name="expert",
-    )(gathered, ffn_gain.reshape(blocks, lanes), w_gate, w_up, w_down)
-    result = jnp.sum(
-        lax.all_to_all(partial_out, TP, 0, 0, tiled=True).astype(jnp.float32), axis=0
-    ).astype(jnp.bfloat16)
-    spaced = jnp.dot(packed.T, result, preferred_element_type=jnp.float32).astype(jnp.bfloat16)
-    returned = lax.all_to_all(
-        spaced.reshape(groups, SLOTS, lanes), "ep", split_axis=0, concat_axis=0, tiled=True
-    )
-    picker = (target[:, None] == lax.broadcasted_iota(jnp.int32, (count, slots_total), 1)).astype(
-        jnp.bfloat16
-    )
-    picked = jnp.dot(
-        picker, returned.reshape(slots_total, lanes), preferred_element_type=jnp.float32
-    ).reshape(rows, top, lanes)
-    mixture = jnp.sum(share[:, :, None] * picked, axis=1)
-    mixed = (middle + mixture).astype(jnp.bfloat16)
+        "expert",
+        shape((blocks, items, lanes), bf16),
+        exchange(held, TP),
+        ffn_gain.reshape(blocks, lanes),
+        w_gate,
+        w_up,
+        w_down,
+    )
+    result = local(
+        total_kernel,
+        "total",
+        shape((groups, SLOTS, lanes), bf16),
+        exchange(partial_out, TP),
+        flops=SHORT,
+    )
+    mixed = local(
+        mixture_kernel,
+        "mixture",
+        shape((rows, lanes), bf16),
+        exchange(result, "ep"),
+        middle,
+        experts,
+        route_weights.T,
+    )
     return (mixed, new_keys, new_values)
 
 

time: 113 us -> 103 us (0.912)
  blocking collectives: 0 us -> 95.2 us
  waiting for transfers between devices: 50.4 us -> 0 us
  starting transfers between devices: 43.5 us -> 0 us
  local copies, waits for them, and re-layouts: 6.29 us -> 2.2 us
  matrix products: 3.76 us -> 0 us
  Pallas kernels: 6.55 us -> 4.83 us
  other arithmetic: 1.24 us -> 0 us
    all_to_all x0 -> x6, blocking collectives: none -> 95.2 us  [exchange(): return lax.all_to_all(x, axis, 0, 0, tiled=True)]
    all_to_all x6 -> x0, waiting for transfers between devices: 50.4 us -> none  [the longest x2 12.8 us: from_everyone(): lax.all_to_all(jnp.broadcast_to(x[None], (size, *x.shape)), axis, 0, 0, t...]
    all_to_all x6 -> x0, starting transfers between devices: 43.5 us -> none  [the longest x1 18.5 us: body(): lax.all_to_all(outgoing.reshape(experts_all, SLOTS, lanes), 'ep', split_a...]
    dot_general x6 -> x0, matrix products: 3.76 us -> none  [the longest x1 0.94 us: body(): jnp.dot(packed.T, result, preferred_element_type=jnp.float32)]
    broadcast_in_dim x2 -> x0, local copies, waits for them, and re-layouts: 2.14 us -> none  [from_everyone(): jnp.broadcast_to(x[None], (size, *x.shape))]
    pallas_call x2 -> x7, Pallas kernels: 6.55 us -> 4.83 us  [local(): pl.pallas_call(kernel, in_specs=specs, out_specs=vmem() if single else [v...]
    unnamed x18 -> x36, local copies, waits for them, and re-layouts: 3.91 us -> 2.2 us
  transfers between devices with their start and end apart: 6 -> 0, of which waited for: 6 -> 0; matrix products, arithmetic and copies ran while one was open for 4% -> 0% of each run, Pallas kernels for 0% -> 0%
where the time goes in v2:
time: 103 us
  blocking collectives  95.2 us (92%)
  Pallas kernels  4.83 us (5%)
  local copies, waits for them, and re-layouts  2.2 us (2%)
    all_to_all x6, blocking collectives, exchange(): return lax.all_to_all(x, axis, 0, 0, tiled=True)  95.2 us
    pallas_call x7, Pallas kernels, local(): pl.pallas_call(kernel, in_specs=specs, out_specs=vmem() if single else [v...  4.83 us
    unnamed x36, local copies, waits for them, and re-layouts  2.2 us

profile of v2, /device:TPU:1, one launch (start us, length us, event | category | flops | bytes accessed | tf_op | source)
XLA Modules:
  0.0 103.0 jit_solution(10047437308520322811)
XLA Ops:
  0.6 0.0 copy-start.8
  0.6 0.0 copy-start.1
  0.7 0.0 copy-start
  0.7 0.0 copy-start.7
  0.7 0.0 copy-start.6
  0.7 0.0 copy-start.5
  0.7 0.0 copy-start.16
  0.7 0.8 copy-done.16
  1.5 14.0 %all_to_all.30.parts_ref = bf16[16,8,128]{2,1,0:T(8,128)(2,1)S(1)} all-to-all(bf16[16,8,128]{2,1,0:T(8,128)(2,1)S(1)} %copies.1), channel_id=1, replica_groups=mesh['ep'=32,'tp_0'=4,'tp_1'=4] {'tp_0','tp_1'}, dimensions={0} | all-to-all | bytes 65536 | tf_op jit(solution)/shard_map/all_to_all | solution.py:239
  15.5 0.0 copy-done.8
  15.5 0.0 copy-done.1
  15.5 0.0 copy-done
  15.5 0.0 copy-done.7
  15.5 0.0 copy-done.6
  15.6 0.6 copy-done.10
  16.2 0.0 copy-done.15
  16.2 2.7 %attend.1 = (bf16[8,64]{1,0:T(8,128)(2,1)}, bf16[8,64]{1,0:T(8,128)(2,1)}, bf16[16,16,128]{2,1,0:T(8,128)(2,1)S(1)}) custom-call(s32[8]{0:T(128)S(1)} %copy-done.14, bf16[16,8,128]{2,1,0:T(8,128)(2,1)S(1)} %all_to_all.30.parts_ref, f32[16,128]{1,0:T(8,128)S(1)} %bitcast.11, bf16[64,2048]{1,0:T(8,128)(2,1)S(1)} %bitcast.8, bf16[64,2048]{1,0:T(8,128)(2,1)S(1)} %bitcast.9, ...), custom_call_target="tpu_custom_call" | custom-call | tf_op jit(solution)/shard_map/attend/pallas_call | solution.py:227
  18.9 9.7 %all_to_all.31.parts_ref = bf16[16,16,128]{2,1,0:T(8,128)(2,1)S(1)} all-to-all(bf16[16,16,128]{2,1,0:T(8,128)(2,1)S(1)} %get-tuple-element.8), channel_id=1, replica_groups=mesh['ep'=32,'tp_0'=4,'tp_1'=4] {'tp_0','tp_1'}, dimensions={0} | all-to-all | bytes 131072 | tf_op jit(solution)/shard_map/all_to_all | solution.py:239
  28.6 0.3 middle.1
  28.9 30.3 %all_to_all.32.arrived_ref = bf16[32,4,128]{2,1,0:T(4,128)(2,1)S(1)} all-to-all(bf16[32,4,128]{2,1,0:T(4,128)(2,1)S(1)} %get-tuple-element.9), channel_id=1, replica_groups=mesh['ep'=32,'tp_0'=4,'tp_1'=4] {'ep'}, dimensions={0} | all-to-all | bytes 65536 | tf_op jit(solution)/shard_map/all_to_all | solution.py:239
  59.2 0.2 spread.1
  59.4 0.0 copy-start.2
  59.4 0.0 copy-start.11
  59.4 11.7 %all_to_all.33.rows_ref = bf16[16,96,128]{2,1,0:T(8,128)(2,1)S(1)} all-to-all(bf16[16,96,128]{2,1,0:T(8,128)(2,1)S(1)} %spread.1), channel_id=1, replica_groups=mesh['ep'=32,'tp_0'=4,'tp_1'=4] {'tp_0','tp_1'}, dimensions={0} | all-to-all | bytes 786432 | tf_op jit(solution)/shard_map/all_to_all | solution.py:239
  71.2 0.0 copy-done.3
  71.2 0.0 copy-done.2
  71.2 0.6 expert.1
  71.8 10.9 %all_to_all.34.parts_ref = bf16[16,96,128]{2,1,0:T(8,128)(2,1)S(1)} all-to-all(bf16[16,96,128]{2,1,0:T(8,128)(2,1)S(1)} %expert.1), channel_id=1, replica_groups=mesh['ep'=32,'tp_0'=4,'tp_1'=4] {'tp_0','tp_1'}, dimensions={0} | all-to-all | bytes 786432 | tf_op jit(solution)/shard_map/all_to_all | solution.py:239
  82.6 0.2 total.1
  82.9 18.6 %all_to_all.35.returned_ref = bf16[32,4,128]{2,1,0:T(4,128)(2,1)S(1)} all-to-all(bf16[32,4,128]{2,1,0:T(4,128)(2,1)S(1)} %total.1), channel_id=1, replica_groups=mesh['ep'=32,'tp_0'=4,'tp_1'=4] {'ep'}, dimensions={0} | all-to-all | bytes 65536 | tf_op jit(solution)/shard_map/all_to_all | solution.py:239
  101.5 0.7 copy-done.13
  102.2 0.9 mixture.1
  (17 shorter events, 0.0 us)
Async XLA Ops:
  0.6 14.9 %copy-start.8 = (bf16[64,2048]{1,0:T(8,128)(2,1)S(1)}, bf16[64,2048]{1,0:T(8,128)(2,1)}, u32[]{:S(2)}) copy-start(bf16[64,2048]{1,0:T(8,128)(2,1)} %wout_ref.1) | copy-start | bytes 786436
  0.6 14.9 %copy-start.1 = (bf16[8,1,64,1024]{3,2,1,0:T(8,128)(2,1)S(1)}, bf16[8,1,64,1024]{3,2,1,0:T(8,128)(2,1)}, u32[]{:S(2)}) copy-start(bf16[8,1,64,1024]{3,2,1,0:T(8,128)(2,1)} %value_ref.1) | copy-start | bytes 3145732
  0.7 14.9 %copy-start = (bf16[8,1,64,1024]{3,2,1,0:T(8,128)(2,1)S(1)}, bf16[8,1,64,1024]{3,2,1,0:T(8,128)(2,1)}, u32[]{:S(2)}) copy-start(bf16[8,1,64,1024]{3,2,1,0:T(8,128)(2,1)} %key_ref.1) | copy-start | bytes 3145732
  0.7 14.9 %copy-start.7 = (bf16[2048,64]{0,1:T(8,128)(2,1)S(1)}, bf16[2048,64]{0,1:T(8,128)(2,1)}, u32[]{:S(2)}) copy-start(bf16[2048,64]{0,1:T(8,128)(2,1)} %param.21) | copy-start | bytes 786436
  0.7 14.9 %copy-start.6 = (bf16[2048,64]{0,1:T(8,128)(2,1)S(1)}, bf16[2048,64]{0,1:T(8,128)(2,1)}, u32[]{:S(2)}) copy-start(bf16[2048,64]{0,1:T(8,128)(2,1)} %param.20) | copy-start | bytes 786436
  0.7 14.9 %copy-start.5 = (bf16[2048,64]{0,1:T(8,128)(2,1)S(1)}, bf16[2048,64]{0,1:T(8,128)(2,1)}, u32[]{:S(2)}) copy-start(bf16[2048,64]{0,1:T(8,128)(2,1)} %param.19) | copy-start | bytes 786436
  0.7 0.8 copy-start.16
  1.5 14.0 %copy-start.9 = (f32[8,1,1024]{2,1,0:T(1,128)S(1)}, f32[8,1,1024]{2,1,0:T(1,128)}, u32[]{:S(2)}) copy-start(f32[8,1,1024]{2,1,0:T(1,128)} %bias_ref.1) | copy-start | bytes 98308
  15.5 0.7 copy-start.10
  15.5 0.7 copy-start.14
  15.5 0.7 copy-start.15
  18.9 9.7 %copy-start.12 = (s32[8,4]{0,1:T(4,128)S(1)}, s32[8,4]{0,1:T(4,128)}, u32[]{:S(2)}) copy-start(s32[8,4]{0,1:T(4,128)} %param.29) | copy-start | bytes 388
  18.9 9.7 %copy-start.17 = (bf16[8,128]{1,0:T(8,128)(2,1)S(1)}, bf16[8,128]{1,0:T(8,128)(2,1)}, u32[]{:S(2)}) copy-start(bf16[8,128]{1,0:T(8,128)(2,1)} %resid_ref.1) | copy-start | bytes 6148
  59.2 11.9 %copy-start.3 = (bf16[1,2048,128]{2,1,0:T(8,128)(2,1)S(1)}, bf16[1,2048,128]{2,1,0:T(8,128)(2,1)}, u32[]{:S(2)}) copy-start(bf16[1,2048,128]{2,1,0:T(8,128)(2,1)} %up_ref.1) | copy-start | bytes 1572868
  59.2 11.9 %copy-start.4 = (bf16[1,128,2048]{2,1,0:T(8,128)(2,1)S(1)}, bf16[1,128,2048]{2,1,0:T(8,128)(2,1)}, u32[]{:S(2)}) copy-start(bf16[1,128,2048]{2,1,0:T(8,128)(2,1)} %down_ref.1) | copy-start | bytes 1572868
  59.4 11.8 %copy-start.2 = (bf16[1,2048,128]{2,1,0:T(8,128)(2,1)S(1)}, bf16[1,2048,128]{2,1,0:T(8,128)(2,1)}, u32[]{:S(2)}) copy-start(bf16[1,2048,128]{2,1,0:T(8,128)(2,1)} %gate_ref.1) | copy-start | bytes 1572868
  59.4 11.8 %copy-start.11 = (f32[2048]{0:T(1024)S(1)}, f32[2048]{0:T(1024)}, u32[]{:S(2)}) copy-start(f32[2048]{0:T(1024)} %param.28) | copy-start | bytes 24580
  101.5 0.7 copy-start.13

commit v3 on v2

--- a/solution.py
+++ b/solution.py
@@ -7,6 +7,8 @@
 from jax.sharding import PartitionSpec as P
 
 TP = ("tp_0", "tp_1")
+EP = ("ep_1", "ep_0")
+CORES = 2
 
 eps = 1e-06
 limit = 7.0
@@ -25,8 +27,28 @@
     ).astype(jnp.bfloat16)
 
 
-def attend_kernel(lengths_ref, parts_ref, gain_ref, wq_ref, wk_ref, wv_ref, key_ref, value_ref,
-                  bias_ref, mix_ref, wout_ref, new_key_ref, new_value_ref, out_ref):
+def chosen_slots(experts_ref, slots):
+    top, rows = experts_ref.shape
+    slot = lax.broadcasted_iota(jnp.int32, (slots, rows), 0)
+    block = slot // SLOTS
+    chips = slots // SLOTS // CORES
+    expert = block % chips * CORES + block // chips
+    hits = [experts_ref[k : k + 1, :] == expert for k in range(top)]
+    named = hits[0]
+    for hit in hits[1:]:
+        named = named | hit
+    first = lax.broadcasted_iota(jnp.int32, (rows, rows), 0)
+    second = lax.broadcasted_iota(jnp.int32, (rows, rows), 1)
+    earlier = (first < second).astype(jnp.bfloat16)
+    rank = jnp.dot(
+        named.astype(jnp.bfloat16), earlier, preferred_element_type=jnp.float32
+    ).astype(jnp.int32)
+    return hits, named & (rank == slot % SLOTS)
+
+
+def attend_kernel(parts_ref, lengths_ref, gain_ref, mix_ref, experts_ref, share_ref, wq_ref,
+                  wk_ref, wv_ref, key_ref, value_ref, bias_ref, wout_ref, new_key_ref,
+                  new_value_ref, out_ref, placed_ref, high_ref, low_ref, fresh_ref, sems):
     blocks, rows, lanes = parts_ref.shape
     heads = key_ref.shape[2]
     cache = key_ref.shape[3]
@@ -41,6 +63,14 @@
         axis=1,
     )
     query = project(normed, wq_ref).astype(jnp.float32)
+    fresh_ref[0] = project(normed, wk_ref)
+    fresh_ref[1] = project(normed, wv_ref)
+    stores = [
+        pltpu.make_async_copy(fresh_ref.at[i], new_ref, sems.at[i])
+        for i, new_ref in enumerate((new_key_ref, new_value_ref))
+    ]
+    for store in stores:
+        store.start()
     spread = jnp.concatenate([query] * rows, axis=1)
     row = lax.broadcasted_iota(jnp.int32, spread.shape, 0)
     own = lax.broadcasted_iota(jnp.int32, spread.shape, 1) // heads == row
@@ -48,10 +78,11 @@
     keys = key_ref[:, 0].reshape(rows * heads, cache)
     scores = jnp.dot(spread, keys, preferred_element_type=jnp.float32) * heads ** (-0.5)
     scores = scores + bias_ref[:, 0, :]
-    line = lax.broadcasted_iota(jnp.int32, (rows, cache), 0)
-    length = jnp.zeros((rows, cache), jnp.int32)
-    for n in range(rows):
-        length = jnp.where(line == n, lengths_ref[n], length)
+    diagonal = lax.broadcasted_iota(jnp.int32, (rows, rows), 0) == lax.broadcasted_iota(
+        jnp.int32, (rows, rows), 1
+    )
+    counts = lengths_ref[...].astype(jnp.float32)
+    length = jnp.sum(jnp.where(diagonal, counts, 0.0), axis=1, keepdims=True).astype(jnp.int32)
     live = lax.broadcasted_iota(jnp.int32, (rows, cache), 1) < length
     soft = jnp.maximum(scores, 0.0) + jnp.log1p(jnp.exp(-jnp.abs(scores)))
     drop = jnp.where(live, soft, 0.0)
@@ -95,32 +126,40 @@
     for t in range(blocks):
         both = jnp.concatenate([branch[:, t * lanes : (t + 1) * lanes], tail], axis=0)
         out_ref[t] = both.astype(jnp.bfloat16)
-    new_key_ref[...] = project(normed, wk_ref)
-    new_value_ref[...] = project(normed, wv_ref)
-
-
-def chosen_slots(experts_ref, slots):
-    top, rows = experts_ref.shape
-    slot = lax.broadcasted_iota(jnp.int32, (slots, rows), 0)
-    hits = [experts_ref[k : k + 1, :] == slot // SLOTS for k in range(top)]
-    named = hits[0]
-    for hit in hits[1:]:
-        named = named | hit
-    first = lax.broadcasted_iota(jnp.int32, (rows, rows), 0)
-    second = lax.broadcasted_iota(jnp.int32, (rows, rows), 1)
-    earlier = (first < second).astype(jnp.bfloat16)
-    rank = jnp.dot(
-        named.astype(jnp.bfloat16), earlier, preferred_element_type=jnp.float32
-    ).astype(jnp.int32)
-    return hits, named & (rank == slot % SLOTS)
-
-
-def copies_kernel(row_ref, out_ref):
-    for t in range(out_ref.shape[0]):
-        out_ref[t] = row_ref[...]
-
-
-def middle_kernel(parts_ref, resid_ref, experts_ref, middle_ref, out_ref):
+    hits, placed = chosen_slots(experts_ref, placed_ref.shape[0])
+    share = share_ref[...]
+    share = share / jnp.sum(share, axis=0, keepdims=True)
+    weight = jnp.where(hits[0], share[:1, :], 0.0)
+    for k in range(1, len(hits)):
+        weight = weight + jnp.where(hits[k], share[k : k + 1, :], 0.0)
+    weight = jnp.where(placed, weight, 0.0)
+    high = weight.astype(jnp.bfloat16)
+    placed_ref[...] = placed.astype(jnp.bfloat16)
+    high_ref[...] = high
+    low_ref[...] = (weight - high.astype(jnp.float32)).astype(jnp.bfloat16)
+    for store in stores:
+        store.wait()
+
+
+def copies_kernel(*refs):
+    count = (len(refs) - 1) // 2
+    sources, targets, sems = refs[:count], refs[count : 2 * count], refs[2 * count]
+    out_ref = targets[0]
+    loads = [
+        pltpu.make_async_copy(source, target, sems.at[i])
+        for i, (source, target) in enumerate(zip(sources, (out_ref.at[0], *targets[1:])))
+    ]
+    for load in loads:
+        load.start()
+    loads[0].wait()
+    row = out_ref[0]
+    for t in range(1, out_ref.shape[0]):
+        out_ref[t] = row
+    for load in loads[1:]:
+        load.wait()
+
+
+def middle_kernel(parts_ref, resid_ref, placed_ref, middle_ref, out_ref):
     blocks, both, lanes = parts_ref.shape
     rows = both // 2
     total = parts_ref[0].astype(jnp.float32)
@@ -131,14 +170,10 @@
     scale = lax.rsqrt(square / channels + eps)
     middle = resid_ref[...].astype(jnp.float32) + total[:rows] * scale
     middle_ref[...] = middle
-    groups, slots, _ = out_ref.shape
-    _, placed = chosen_slots(experts_ref, groups * slots)
     out = jnp.dot(
-        placed.astype(jnp.bfloat16),
-        middle.astype(jnp.bfloat16),
-        preferred_element_type=jnp.float32,
-    )
-    out_ref[...] = out.reshape(groups, slots, lanes).astype(jnp.bfloat16)
+        placed_ref[...], middle.astype(jnp.bfloat16), preferred_element_type=jnp.float32
+    )
+    out_ref[...] = out.reshape(out_ref.shape).astype(jnp.bfloat16)
 
 
 def packing(items, slots):
@@ -175,24 +210,15 @@
     out_ref[...] = spaced.reshape(groups, slots, lanes).astype(jnp.bfloat16)
 
 
-def mixture_kernel(returned_ref, middle_ref, experts_ref, share_ref, out_ref):
+def mixture_kernel(returned_ref, middle_ref, high_ref, low_ref, out_ref):
     groups, slots, lanes = returned_ref.shape
-    hits, placed = chosen_slots(experts_ref, groups * slots)
-    share = share_ref[...]
-    share = share / jnp.sum(share, axis=0, keepdims=True)
-    weight = jnp.where(hits[0], share[:1, :], 0.0)
-    for k in range(1, len(hits)):
-        weight = weight + jnp.where(hits[k], share[k : k + 1, :], 0.0)
-    weight = jnp.where(placed, weight, 0.0)
-    high = weight.astype(jnp.bfloat16)
-    low = (weight - high.astype(jnp.float32)).astype(jnp.bfloat16)
     returned = returned_ref[...].astype(jnp.float32).reshape(groups * slots, lanes)
     returned = returned.astype(jnp.bfloat16)
     mixture = sum(
         lax.dot_general(
-            part, returned, (((0,), (0,)), ((), ())), preferred_element_type=jnp.float32
+            part[...], returned, (((0,), (0,)), ((), ())), preferred_element_type=jnp.float32
         )
-        for part in (high, low)
+        for part in (high_ref, low_ref)
     )
     out_ref[...] = (middle_ref[...] + mixture).astype(jnp.bfloat16)
 
@@ -217,22 +243,24 @@
         out_ref[t] = result[:, t * lanes : (t + 1) * lanes]
 
 
-def vmem():
-    return pl.BlockSpec(memory_space=pltpu.VMEM)
-
-
-def local(kernel, name, out_shape, *args, scalars=0, flops=0):
+def local(kernel, name, out_shape, *args, flops=0, far_in=0, far_out=0, scratch=()):
+    def places(count, far):
+        return [pl.BlockSpec(memory_space=pltpu.HBM)] * far + [
+            pl.BlockSpec(memory_space=pltpu.VMEM)
+        ] * (count - far)
+
     single = not isinstance(out_shape, list)
-    specs = [pl.BlockSpec(memory_space=pltpu.SMEM)] * scalars + [vmem()] * (len(args) - scalars)
+    outs = places(1 if single else len(out_shape), far_out)
     return pl.pallas_call(
         kernel,
-        in_specs=specs,
-        out_specs=vmem() if single else [vmem()] * len(out_shape),
+        in_specs=places(len(args), far_in),
+        out_specs=outs[0] if single else outs,
         out_shape=out_shape,
+        scratch_shapes=scratch,
         compiler_params=pltpu.CompilerParams(vmem_limit_bytes=LIMIT),
         cost_estimate=pl.CostEstimate(flops=flops, bytes_accessed=0, transcendentals=0),
         name=name,
-    )(*args)
+    )(*[pltpu.with_memory_space_constraint(x, pltpu.HBM) for x in args[:far_in]], *args[far_in:])
 
 
 def exchange(x, axis):
@@ -259,32 +287,46 @@
     w_down,
 ):
     blocks = lax.axis_size(TP)
-    groups = lax.axis_size("ep")
+    groups = lax.axis_size(EP)
     rows, lanes = resid.shape
     heads = mix_gain.shape[0]
     items = groups * CAP
     bf16 = jnp.bfloat16
     shape = jax.ShapeDtypeStruct
+    slots = groups * SLOTS
     new = shape((rows, heads), bf16)
-    experts = route_experts.T
-    copies = local(copies_kernel, "copies", shape((blocks, rows, lanes), bf16), resid, flops=LONG)
-    parts = exchange(copies, TP)
-    new_keys, new_values, partial_branch = local(
+    small = (
+        lengths.reshape(1, rows),
+        attn_gain.reshape(blocks, lanes),
+        mix_gain.reshape(1, heads),
+        route_experts.T,
+        route_weights.T,
+    )
+    copies, *small = local(
+        copies_kernel,
+        "copies",
+        [shape((blocks, rows, lanes), bf16)] + [shape(x.shape, x.dtype) for x in small],
+        resid,
+        *small,
+        flops=LONG,
+        far_in=1 + len(small),
+        scratch=[pltpu.SemaphoreType.DMA((1 + len(small),))],
+    )
+    new_keys, new_values, partial_branch, placed, high, low = local(
         attend_kernel,
         "attend",
-        [new, new, shape((blocks, 2 * rows, lanes), bf16)],
-        lengths,
-        parts,
-        attn_gain.reshape(blocks, lanes),
+        [new, new, shape((blocks, 2 * rows, lanes), bf16)] + [shape((slots, rows), bf16)] * 3,
+        exchange(copies, TP),
+        *small,
         w_query.T,
         w_key.T,
         w_value.T,
         key_cache,
         value_cache,
         key_bias,
-        mix_gain.reshape(1, heads),
         w_out,
-        scalars=1,
+        far_out=2,
+        scratch=[pltpu.VMEM((2, rows, heads), bf16), pltpu.SemaphoreType.DMA((2,))],
     )
     middle, outgoing = local(
         middle_kernel,
@@ -292,14 +334,14 @@
         [shape((rows, lanes), jnp.float32), shape((groups, SLOTS, lanes), bf16)],
         exchange(partial_branch, TP),
         resid,
-        experts,
+        placed,
         flops=SHORT,
     )
     held = local(
         spread_kernel,
         "spread",
         shape((blocks, items, lanes), bf16),
-        exchange(outgoing, "ep"),
+        exchange(outgoing, EP),
         flops=SHORT,
     )
     partial_out = local(
@@ -323,34 +365,38 @@
         mixture_kernel,
         "mixture",
         shape((rows, lanes), bf16),
-        exchange(result, "ep"),
+        exchange(result, EP),
         middle,
-        experts,
-        route_weights.T,
+        high,
+        low,
     )
     return (mixed, new_keys, new_values)
 
 
 def solution(mesh):
-    torus = Mesh(mesh.devices.reshape(mesh.shape["ep"], 4, 4), ("ep", "tp_0", "tp_1"))
+    torus = Mesh(
+        mesh.devices.reshape(mesh.shape["ep"] // CORES, CORES, 4, 4),
+        ("ep_0", "ep_1", "tp_0", "tp_1"),
+    )
+    rows = ("ep_0", "ep_1")
     in_specs = (
-        P("ep", TP),
+        P(rows, TP),
         P(),
         P(None, TP),
         P(None, TP),
         P(None, TP),
-        P("ep", TP, None, None),
-        P("ep", TP, None, None),
-        P("ep", TP, None),
-        P("ep"),
+        P(rows, TP, None, None),
+        P(rows, TP, None, None),
+        P(rows, TP, None),
+        P(rows),
         P(TP),
         P(TP, None),
         P(),
-        P("ep", None),
-        P("ep", None),
-        P("ep", None, TP),
-        P("ep", None, TP),
-        P("ep", TP, None),
-    )
-    out_specs = (P("ep", TP), P("ep", TP), P("ep", TP))
+        P(rows, None),
+        P(rows, None),
+        P(rows, None, TP),
+        P(rows, None, TP),
+        P(rows, TP, None),
+    )
+    out_specs = (P(rows, TP), P(rows, TP), P(rows, TP))
     return jax.shard_map(body, mesh=torus, in_specs=in_specs, out_specs=out_specs, check_vma=False)

time: 103 us -> 102 us (level)
  local copies, waits for them, and re-layouts: 2.2 us -> 0.06 us
    unnamed x36 -> x24, local copies, waits for them, and re-layouts: 2.2 us -> 0.06 us
where the time goes in v3:
time: 102 us; the launch traced here: 101 us
  blocking collectives  96 us (94%)
  Pallas kernels  4.4 us (4%)
    all_to_all x6, blocking collectives, exchange(): return lax.all_to_all(x, axis, 0, 0, tiled=True)  96 us
    pallas_call x7, Pallas kernels, local(): pl.pallas_call(kernel, in_specs=places(len(args), far_in), out_specs=outs...  4.4 us

profile of v3, /device:TPU:1, one launch (start us, length us, event | category | flops | bytes accessed | tf_op | source)
XLA Modules:
  0.0 101.3 jit_solution(1094303957344103758)
XLA Ops:
  0.6 0.0 copy-start
  0.6 0.0 copy-start.1
  0.7 0.0 copy-start.5
  0.7 0.0 copy-start.6
  0.7 0.0 copy-start.7
  0.7 0.0 copy-start.8
  0.7 0.9 copies.1
  1.6 0.0 copy-start.9
  1.7 13.8 %all_to_all.30.parts_ref = bf16[16,8,128]{2,1,0:T(8,128)(2,1)S(1)} all-to-all(bf16[16,8,128]{2,1,0:T(8,128)(2,1)S(1)} %get-tuple-element.17), channel_id=1, replica_groups=mesh['ep_0'=16,'ep_1'=2,'tp_0'=4,'tp_1'=4] {'tp_0','tp_1'}, dimensions={0} | all-to-all | bytes 65536 | tf_op jit(solution)/shard_map/all_to_all | solution.py:267
  15.5 0.0 copy-done
  15.5 0.0 copy-done.1
  15.5 0.0 copy-done.5
  15.5 0.0 copy-done.6
  15.5 0.0 copy-done.7
  15.5 0.0 copy-done.8
  15.5 0.0 copy-done.9
  15.5 1.5 %attend.1 = (bf16[8,64]{1,0:T(8,128)(2,1)}, bf16[8,64]{1,0:T(8,128)(2,1)}, bf16[16,16,128]{2,1,0:T(8,128)(2,1)S(1)}, bf16[128,8]{1,0:T(8,128)(2,1)S(1)}, bf16[12...) custom-call(bf16[16,8,128]{2,1,0:T(8,128)(2,1)S(1)} %all_to_all.30.parts_ref, s32[1,8]{1,0:T(1,128)S(1)} %get-tuple-element.18.lengths_ref, ...), custom_call_target="tpu_custom_call" | custom-call | tf_op jit(solution)/shard_map/attend/pallas_call | solution.py:254
  17.0 0.0 copy-start.11
  17.0 9.6 %all_to_all.31.parts_ref = bf16[16,16,128]{2,1,0:T(8,128)(2,1)S(1)} all-to-all(bf16[16,16,128]{2,1,0:T(8,128)(2,1)S(1)} %get-tuple-element.23), channel_id=1, replica_groups=mesh['ep_0'=16,'ep_1'=2,'tp_0'=4,'tp_1'=4] {'tp_0','tp_1'}, dimensions={0} | all-to-all | bytes 131072 | tf_op jit(solution)/shard_map/all_to_all | solution.py:267
  26.6 0.3 middle.1
  26.9 30.7 %all_to_all.32.arrived_ref = bf16[32,4,128]{2,1,0:T(4,128)(2,1)S(1)} all-to-all(bf16[32,4,128]{2,1,0:T(4,128)(2,1)S(1)} %get-tuple-element.25), channel_id=1, replica_groups=mesh['ep_0'=16,'ep_1'=2,'tp_0'=4,'tp_1'=4] {'ep_1','ep_0'}, dimensions={0} | all-to-all | bytes 65536 | tf_op jit(solution)/shard_map/all_to_all | solution.py:267
  57.6 0.2 spread.1
  57.8 0.0 copy-start.2
  57.8 0.0 copy-start.10
  57.8 12.6 %all_to_all.33.rows_ref = bf16[16,96,128]{2,1,0:T(8,128)(2,1)S(1)} all-to-all(bf16[16,96,128]{2,1,0:T(8,128)(2,1)S(1)} %spread.1), channel_id=1, replica_groups=mesh['ep_0'=16,'ep_1'=2,'tp_0'=4,'tp_1'=4] {'tp_0','tp_1'}, dimensions={0} | all-to-all | bytes 786432 | tf_op jit(solution)/shard_map/all_to_all | solution.py:267
  70.4 0.0 copy-done.2
  70.4 0.0 copy-done.10
  70.5 0.6 expert.1
  71.1 12.0 %all_to_all.34.parts_ref = bf16[16,96,128]{2,1,0:T(8,128)(2,1)S(1)} all-to-all(bf16[16,96,128]{2,1,0:T(8,128)(2,1)S(1)} %expert.1), channel_id=1, replica_groups=mesh['ep_0'=16,'ep_1'=2,'tp_0'=4,'tp_1'=4] {'tp_0','tp_1'}, dimensions={0} | all-to-all | bytes 786432 | tf_op jit(solution)/shard_map/all_to_all | solution.py:267
  83.0 0.2 total.1
  83.2 17.3 %all_to_all.35.returned_ref = bf16[32,4,128]{2,1,0:T(4,128)(2,1)S(1)} all-to-all(bf16[32,4,128]{2,1,0:T(4,128)(2,1)S(1)} %total.1), channel_id=1, replica_groups=mesh['ep_0'=16,'ep_1'=2,'tp_0'=4,'tp_1'=4] {'ep_1','ep_0'}, dimensions={0} | all-to-all | bytes 65536 | tf_op jit(solution)/shard_map/all_to_all | solution.py:267
  100.5 0.8 mixture.1
  (5 shorter events, 0.0 us)
Async XLA Ops:
  0.6 14.8 %copy-start = (bf16[8,1,64,1024]{3,2,1,0:T(8,128)(2,1)S(1)}, bf16[8,1,64,1024]{3,2,1,0:T(8,128)(2,1)}, u32[]{:S(2)}) copy-start(bf16[8,1,64,1024]{3,2,1,0:T(8,128)(2,1)} %key_ref.1) | copy-start | bytes 3145732
  0.6 14.8 %copy-start.1 = (bf16[8,1,64,1024]{3,2,1,0:T(8,128)(2,1)S(1)}, bf16[8,1,64,1024]{3,2,1,0:T(8,128)(2,1)}, u32[]{:S(2)}) copy-start(bf16[8,1,64,1024]{3,2,1,0:T(8,128)(2,1)} %value_ref.1) | copy-start | bytes 3145732
  0.7 14.8 %copy-start.5 = (bf16[2048,64]{0,1:T(8,128)(2,1)S(1)}, bf16[2048,64]{0,1:T(8,128)(2,1)}, u32[]{:S(2)}) copy-start(bf16[2048,64]{0,1:T(8,128)(2,1)} %param.19) | copy-start | bytes 786436
  0.7 14.8 %copy-start.6 = (bf16[2048,64]{0,1:T(8,128)(2,1)S(1)}, bf16[2048,64]{0,1:T(8,128)(2,1)}, u32[]{:S(2)}) copy-start(bf16[2048,64]{0,1:T(8,128)(2,1)} %param.20) | copy-start | bytes 786436
  0.7 14.8 %copy-start.7 = (bf16[2048,64]{0,1:T(8,128)(2,1)S(1)}, bf16[2048,64]{0,1:T(8,128)(2,1)}, u32[]{:S(2)}) copy-start(bf16[2048,64]{0,1:T(8,128)(2,1)} %param.21) | copy-start | bytes 786436
  0.7 14.8 %copy-start.8 = (bf16[64,2048]{1,0:T(8,128)(2,1)S(1)}, bf16[64,2048]{1,0:T(8,128)(2,1)}, u32[]{:S(2)}) copy-start(bf16[64,2048]{1,0:T(8,128)(2,1)} %wout_ref.1) | copy-start | bytes 786436
  1.6 13.9 %copy-start.9 = (f32[8,1,1024]{2,1,0:T(1,128)S(1)}, f32[8,1,1024]{2,1,0:T(1,128)}, u32[]{:S(2)}) copy-start(f32[8,1,1024]{2,1,0:T(1,128)} %bias_ref.1) | copy-start | bytes 98308
  17.0 9.6 %copy-start.11 = (bf16[8,128]{1,0:T(8,128)(2,1)S(1)}, bf16[8,128]{1,0:T(8,128)(2,1)}, u32[]{:S(2)}) copy-start(bf16[8,128]{1,0:T(8,128)(2,1)} %resid_ref.1) | copy-start | bytes 6148
  57.6 12.8 %copy-start.3 = (bf16[1,2048,128]{2,1,0:T(8,128)(2,1)S(1)}, bf16[1,2048,128]{2,1,0:T(8,128)(2,1)}, u32[]{:S(2)}) copy-start(bf16[1,2048,128]{2,1,0:T(8,128)(2,1)} %up_ref.1) | copy-start | bytes 1572868
  57.6 12.8 %copy-start.4 = (bf16[1,128,2048]{2,1,0:T(8,128)(2,1)S(1)}, bf16[1,128,2048]{2,1,0:T(8,128)(2,1)}, u32[]{:S(2)}) copy-start(bf16[1,128,2048]{2,1,0:T(8,128)(2,1)} %down_ref.1) | copy-start | bytes 1572868
  57.8 12.6 %copy-start.2 = (bf16[1,2048,128]{2,1,0:T(8,128)(2,1)S(1)}, bf16[1,2048,128]{2,1,0:T(8,128)(2,1)}, u32[]{:S(2)}) copy-start(bf16[1,2048,128]{2,1,0:T(8,128)(2,1)} %gate_ref.1) | copy-start | bytes 1572868
  57.8 12.6 %copy-start.10 = (f32[2048]{0:T(1024)S(1)}, f32[2048]{0:T(1024)}, u32[]{:S(2)}) copy-start(f32[2048]{0:T(1024)} %param.28) | copy-start | bytes 24580

commit v4 on v3

--- a/solution.py
+++ b/solution.py
@@ -141,22 +141,23 @@
         store.wait()
 
 
-def copies_kernel(*refs):
-    count = (len(refs) - 1) // 2
+def load_kernel(*refs):
+    count = len(refs) // 2
     sources, targets, sems = refs[:count], refs[count : 2 * count], refs[2 * count]
-    out_ref = targets[0]
     loads = [
         pltpu.make_async_copy(source, target, sems.at[i])
-        for i, (source, target) in enumerate(zip(sources, (out_ref.at[0], *targets[1:])))
+        for i, (source, target) in enumerate(zip(sources, targets))
     ]
     for load in loads:
         load.start()
-    loads[0].wait()
-    row = out_ref[0]
-    for t in range(1, out_ref.shape[0]):
+    for load in loads:
+        load.wait()
+
+
+def copies_kernel(row_ref, out_ref):
+    row = row_ref[...]
+    for t in range(out_ref.shape[0]):
         out_ref[t] = row
-    for load in loads[1:]:
-        load.wait()
 
 
 def middle_kernel(parts_ref, resid_ref, placed_ref, middle_ref, out_ref):
@@ -296,21 +297,23 @@
     slots = groups * SLOTS
     new = shape((rows, heads), bf16)
     small = (
+        resid,
         lengths.reshape(1, rows),
         attn_gain.reshape(blocks, lanes),
         mix_gain.reshape(1, heads),
         route_experts.T,
         route_weights.T,
     )
-    copies, *small = local(
-        copies_kernel,
-        "copies",
-        [shape((blocks, rows, lanes), bf16)] + [shape(x.shape, x.dtype) for x in small],
-        resid,
+    near, *small = local(
+        load_kernel,
+        "load",
+        [shape(x.shape, x.dtype) for x in small],
         *small,
-        flops=LONG,
-        far_in=1 + len(small),
-        scratch=[pltpu.SemaphoreType.DMA((1 + len(small),))],
+        far_in=len(small),
+        scratch=[pltpu.SemaphoreType.DMA((len(small),))],
+    )
+    copies = local(
+        copies_kernel, "copies", shape((blocks, rows, lanes), bf16), near, flops=LONG
     )
     new_keys, new_values, partial_branch, placed, high, low = local(
         attend_kernel,
@@ -333,7 +336,7 @@
         "middle",
         [shape((rows, lanes), jnp.float32), shape((groups, SLOTS, lanes), bf16)],
         exchange(partial_branch, TP),
-        resid,
+        near,
         placed,
         flops=SHORT,
     )

time: 102 us -> 102 us (level)
    pallas_call x7 -> x8, Pallas kernels: 4.4 us -> 4.28 us  [local(): pl.pallas_call(kernel, in_specs=places(len(args), far_in), out_specs=outs...]
where the time goes in v4:
time: 102 us; the launch traced here: 101 us
  blocking collectives  96.3 us (94%)
  Pallas kernels  4.28 us (4%)
    all_to_all x6, blocking collectives, exchange(): return lax.all_to_all(x, axis, 0, 0, tiled=True)  96.3 us
    pallas_call x8, Pallas kernels, local(): pl.pallas_call(kernel, in_specs=places(len(args), far_in), out_specs=outs...  4.28 us

profile of v4, /device:TPU:1, one launch (start us, length us, event | category | flops | bytes accessed | tf_op | source)
XLA Modules:
  0.0 101.4 jit_solution(17222134198550874929)
XLA Ops:
  0.6 0.8 load.1
  1.5 0.0 copy-start
  1.5 0.0 copy-start.1
  1.5 0.0 copy-start.5
  1.5 0.0 copy-start.6
  1.5 0.0 copy-start.7
  1.5 0.0 copy-start.8
  1.5 0.0 copy-start.9
  1.6 14.1 %all_to_all.30.parts_ref = bf16[16,8,128]{2,1,0:T(8,128)(2,1)S(1)} all-to-all(bf16[16,8,128]{2,1,0:T(8,128)(2,1)S(1)} %copies.1), channel_id=1, replica_groups=mesh['ep_0'=16,'ep_1'=2,'tp_0'=4,'tp_1'=4] {'tp_0','tp_1'}, dimensions={0} | all-to-all | bytes 65536 | tf_op jit(solution)/shard_map/all_to_all | solution.py:268
  15.6 0.0 copy-done
  15.6 0.0 copy-done.1
  15.6 0.0 copy-done.5
  15.7 0.0 copy-done.6
  15.7 0.0 copy-done.7
  15.7 0.0 copy-done.8
  15.7 0.0 copy-done.9
  15.7 1.5 %attend.1 = (bf16[8,64]{1,0:T(8,128)(2,1)}, bf16[8,64]{1,0:T(8,128)(2,1)}, bf16[16,16,128]{2,1,0:T(8,128)(2,1)S(1)}, bf16[128,8]{1,0:T(8,128)(2,1)S(1)}, bf16[12...) custom-call(bf16[16,8,128]{2,1,0:T(8,128)(2,1)S(1)} %all_to_all.30.parts_ref, s32[1,8]{1,0:T(1,128)S(1)} %get-tuple-element.18.lengths_ref, ...), custom_call_target="tpu_custom_call" | custom-call | tf_op jit(solution)/shard_map/attend/pallas_call | solution.py:255
  17.2 9.6 %all_to_all.31.parts_ref = bf16[16,16,128]{2,1,0:T(8,128)(2,1)S(1)} all-to-all(bf16[16,16,128]{2,1,0:T(8,128)(2,1)S(1)} %get-tuple-element.23), channel_id=1, replica_groups=mesh['ep_0'=16,'ep_1'=2,'tp_0'=4,'tp_1'=4] {'tp_0','tp_1'}, dimensions={0} | all-to-all | bytes 131072 | tf_op jit(solution)/shard_map/all_to_all | solution.py:268
  26.8 0.3 middle.1
  27.1 30.7 %all_to_all.32.arrived_ref = bf16[32,4,128]{2,1,0:T(4,128)(2,1)S(1)} all-to-all(bf16[32,4,128]{2,1,0:T(4,128)(2,1)S(1)} %get-tuple-element.25), channel_id=1, replica_groups=mesh['ep_0'=16,'ep_1'=2,'tp_0'=4,'tp_1'=4] {'ep_1','ep_0'}, dimensions={0} | all-to-all | bytes 65536 | tf_op jit(solution)/shard_map/all_to_all | solution.py:268
  57.8 0.2 spread.1
  58.0 0.0 copy-start.2
  58.0 0.0 copy-start.10
  58.0 12.6 %all_to_all.33.rows_ref = bf16[16,96,128]{2,1,0:T(8,128)(2,1)S(1)} all-to-all(bf16[16,96,128]{2,1,0:T(8,128)(2,1)S(1)} %spread.1), channel_id=1, replica_groups=mesh['ep_0'=16,'ep_1'=2,'tp_0'=4,'tp_1'=4] {'tp_0','tp_1'}, dimensions={0} | all-to-all | bytes 786432 | tf_op jit(solution)/shard_map/all_to_all | solution.py:268
  70.6 0.0 copy-done.3
  70.6 0.0 copy-done.4
  70.6 0.0 copy-done.2
  70.6 0.6 expert.1
  71.2 12.0 %all_to_all.34.parts_ref = bf16[16,96,128]{2,1,0:T(8,128)(2,1)S(1)} all-to-all(bf16[16,96,128]{2,1,0:T(8,128)(2,1)S(1)} %expert.1), channel_id=1, replica_groups=mesh['ep_0'=16,'ep_1'=2,'tp_0'=4,'tp_1'=4] {'tp_0','tp_1'}, dimensions={0} | all-to-all | bytes 786432 | tf_op jit(solution)/shard_map/all_to_all | solution.py:268
  83.2 0.2 total.1
  83.4 17.3 %all_to_all.35.returned_ref = bf16[32,4,128]{2,1,0:T(4,128)(2,1)S(1)} all-to-all(bf16[32,4,128]{2,1,0:T(4,128)(2,1)S(1)} %total.1), channel_id=1, replica_groups=mesh['ep_0'=16,'ep_1'=2,'tp_0'=4,'tp_1'=4] {'ep_1','ep_0'}, dimensions={0} | all-to-all | bytes 65536 | tf_op jit(solution)/shard_map/all_to_all | solution.py:268
  100.7 0.8 mixture.1
  (4 shorter events, 0.0 us)
Async XLA Ops:
  1.5 14.2 %copy-start = (bf16[8,1,64,1024]{3,2,1,0:T(8,128)(2,1)S(1)}, bf16[8,1,64,1024]{3,2,1,0:T(8,128)(2,1)}, u32[]{:S(2)}) copy-start(bf16[8,1,64,1024]{3,2,1,0:T(8,128)(2,1)} %key_ref.1) | copy-start | bytes 3145732
  1.5 14.2 %copy-start.1 = (bf16[8,1,64,1024]{3,2,1,0:T(8,128)(2,1)S(1)}, bf16[8,1,64,1024]{3,2,1,0:T(8,128)(2,1)}, u32[]{:S(2)}) copy-start(bf16[8,1,64,1024]{3,2,1,0:T(8,128)(2,1)} %value_ref.1) | copy-start | bytes 3145732
  1.5 14.2 %copy-start.5 = (bf16[2048,64]{0,1:T(8,128)(2,1)S(1)}, bf16[2048,64]{0,1:T(8,128)(2,1)}, u32[]{:S(2)}) copy-start(bf16[2048,64]{0,1:T(8,128)(2,1)} %param.19) | copy-start | bytes 786436
  1.5 14.2 %copy-start.6 = (bf16[2048,64]{0,1:T(8,128)(2,1)S(1)}, bf16[2048,64]{0,1:T(8,128)(2,1)}, u32[]{:S(2)}) copy-start(bf16[2048,64]{0,1:T(8,128)(2,1)} %param.20) | copy-start | bytes 786436
  1.5 14.2 %copy-start.7 = (bf16[2048,64]{0,1:T(8,128)(2,1)S(1)}, bf16[2048,64]{0,1:T(8,128)(2,1)}, u32[]{:S(2)}) copy-start(bf16[2048,64]{0,1:T(8,128)(2,1)} %param.21) | copy-start | bytes 786436
  1.5 14.2 %copy-start.8 = (bf16[64,2048]{1,0:T(8,128)(2,1)S(1)}, bf16[64,2048]{1,0:T(8,128)(2,1)}, u32[]{:S(2)}) copy-start(bf16[64,2048]{1,0:T(8,128)(2,1)} %wout_ref.1) | copy-start | bytes 786436
  1.5 14.1 %copy-start.9 = (f32[8,1,1024]{2,1,0:T(1,128)S(1)}, f32[8,1,1024]{2,1,0:T(1,128)}, u32[]{:S(2)}) copy-start(f32[8,1,1024]{2,1,0:T(1,128)} %bias_ref.1) | copy-start | bytes 98308
  57.8 12.8 %copy-start.3 = (bf16[1,2048,128]{2,1,0:T(8,128)(2,1)S(1)}, bf16[1,2048,128]{2,1,0:T(8,128)(2,1)}, u32[]{:S(2)}) copy-start(bf16[1,2048,128]{2,1,0:T(8,128)(2,1)} %up_ref.1) | copy-start | bytes 1572868
  57.8 12.8 %copy-start.4 = (bf16[1,128,2048]{2,1,0:T(8,128)(2,1)S(1)}, bf16[1,128,2048]{2,1,0:T(8,128)(2,1)}, u32[]{:S(2)}) copy-start(bf16[1,128,2048]{2,1,0:T(8,128)(2,1)} %down_ref.1) | copy-start | bytes 1572868
  58.0 12.6 %copy-start.2 = (bf16[1,2048,128]{2,1,0:T(8,128)(2,1)S(1)}, bf16[1,2048,128]{2,1,0:T(8,128)(2,1)}, u32[]{:S(2)}) copy-start(bf16[1,2048,128]{2,1,0:T(8,128)(2,1)} %gate_ref.1) | copy-start | bytes 1572868
  58.0 12.6 %copy-start.10 = (f32[2048]{0:T(1024)S(1)}, f32[2048]{0:T(1024)}, u32[]{:S(2)}) copy-start(f32[2048]{0:T(1024)} %param.28) | copy-start | bytes 24580

commit v5 on v4

--- a/solution.py
+++ b/solution.py
@@ -6,7 +6,8 @@
 from jax.sharding import Mesh
 from jax.sharding import PartitionSpec as P
 
-TP = ("tp_0", "tp_1")
+TP = ("tp_0", "tp_1", "tp_2")
+NEAR = ("tp_0", "tp_2")
 EP = ("ep_1", "ep_0")
 CORES = 2
 
@@ -25,6 +26,10 @@
     return lax.dot_general(
         rows, weight_ref[...], (((1,), (1,)), ((), ())), preferred_element_type=jnp.float32
     ).astype(jnp.bfloat16)
+
+
+def pair_of(t):
+    return t & ~2, t | 2
 
 
 def chosen_slots(experts_ref, slots):
@@ -123,9 +128,12 @@
     top = square.astype(jnp.bfloat16).astype(jnp.float32)
     half = lax.broadcasted_iota(jnp.int32, (rows, lanes), 1) < lanes // 2
     tail = jnp.where(half, top, square - top)
+    tail = tail.astype(jnp.bfloat16)
     for t in range(blocks):
-        both = jnp.concatenate([branch[:, t * lanes : (t + 1) * lanes], tail], axis=0)
-        out_ref[t] = both.astype(jnp.bfloat16)
+        low, high = [
+            branch[:, i * lanes : (i + 1) * lanes].astype(jnp.bfloat16) for i in pair_of(t)
+        ]
+        out_ref[t] = jnp.concatenate([low, high, tail], axis=0)
     hits, placed = chosen_slots(experts_ref, placed_ref.shape[0])
     share = share_ref[...]
     share = share / jnp.sum(share, axis=0, keepdims=True)
@@ -161,20 +169,28 @@
 
 
 def middle_kernel(parts_ref, resid_ref, placed_ref, middle_ref, out_ref):
-    blocks, both, lanes = parts_ref.shape
-    rows = both // 2
+    blocks, stacked, lanes = parts_ref.shape
+    rows = stacked // 3
     total = parts_ref[0].astype(jnp.float32)
     for t in range(1, blocks):
         total = total + parts_ref[t].astype(jnp.float32)
-    square = total[rows:, :1] + total[rows:, lanes - 1 :]
+    square = total[2 * rows :, :1] + total[2 * rows :, lanes - 1 :]
     channels = blocks * (lanes // 2)
     scale = lax.rsqrt(square / channels + eps)
-    middle = resid_ref[...].astype(jnp.float32) + total[:rows] * scale
-    middle_ref[...] = middle
-    out = jnp.dot(
-        placed_ref[...], middle.astype(jnp.bfloat16), preferred_element_type=jnp.float32
-    )
-    out_ref[...] = out.reshape(out_ref.shape).astype(jnp.bfloat16)
+    low = lax.axis_index("tp_0") * 4 + lax.axis_index("tp_2")
+    pair = [
+        resid_ref[low + 2 * i].astype(jnp.float32) + total[i * rows : (i + 1) * rows] * scale
+        for i in range(2)
+    ]
+    middle_ref[...] = jnp.where(lax.axis_index("tp_1") == 0, pair[0], pair[1])
+    for i in range(2):
+        out = jnp.dot(
+            placed_ref[...], pair[i].astype(jnp.bfloat16), preferred_element_type=jnp.float32
+        )
+        groups = out_ref.shape[0]
+        out_ref[:, i * SLOTS : (i + 1) * SLOTS, :] = out.reshape(groups, SLOTS, lanes).astype(
+            jnp.bfloat16
+        )
 
 
 def packing(items, slots):
@@ -184,14 +200,21 @@
 
 
 def spread_kernel(arrived_ref, out_ref):
-    blocks, items, lanes = out_ref.shape
-    groups, slots, _ = arrived_ref.shape
-    arrived = arrived_ref[...].astype(jnp.float32).reshape(groups * slots, lanes)
-    held = jnp.dot(
-        packing(items, groups * slots),
-        arrived.astype(jnp.bfloat16),
-        preferred_element_type=jnp.float32,
-    ).astype(jnp.bfloat16)
+    blocks, both, lanes = out_ref.shape
+    groups = arrived_ref.shape[0]
+    pack = packing(both // 2, groups * SLOTS)
+    arrived = arrived_ref[...].astype(jnp.float32)
+    held = [
+        jnp.dot(
+            pack,
+            arrived[:, i * SLOTS : (i + 1) * SLOTS]
+            .reshape(groups * SLOTS, lanes)
+            .astype(jnp.bfloat16),
+            preferred_element_type=jnp.float32,
+        )
+        for i in range(2)
+    ]
+    held = jnp.concatenate(held, axis=0).astype(jnp.bfloat16)
     for t in range(blocks):
         out_ref[t] = held
 
@@ -225,11 +248,12 @@
 
 
 def expert_kernel(rows_ref, gain_ref, gate_ref, up_ref, down_ref, out_ref):
-    blocks, rows, lanes = rows_ref.shape
+    blocks, rows, lanes = out_ref.shape
     total = jnp.zeros((rows, lanes), jnp.float32)
     scaled = []
     for t in range(blocks):
-        x = rows_ref[t].astype(jnp.float32)
+        side = t % 4 // 2
+        x = rows_ref[t // 4 * 2 + t % 2, side * rows : (side + 1) * rows].astype(jnp.float32)
         total = total + x * x
         scaled.append((x * gain_ref[t : t + 1, :]).astype(jnp.bfloat16))
     scaled = jnp.concatenate(scaled, axis=1)
@@ -315,11 +339,12 @@
     copies = local(
         copies_kernel, "copies", shape((blocks, rows, lanes), bf16), near, flops=LONG
     )
+    parts = exchange(copies, TP)
     new_keys, new_values, partial_branch, placed, high, low = local(
         attend_kernel,
         "attend",
-        [new, new, shape((blocks, 2 * rows, lanes), bf16)] + [shape((slots, rows), bf16)] * 3,
-        exchange(copies, TP),
+        [new, new, shape((blocks, 3 * rows, lanes), bf16)] + [shape((slots, rows), bf16)] * 3,
+        parts,
         *small,
         w_query.T,
         w_key.T,
@@ -334,16 +359,16 @@
     middle, outgoing = local(
         middle_kernel,
         "middle",
-        [shape((rows, lanes), jnp.float32), shape((groups, SLOTS, lanes), bf16)],
+        [shape((rows, lanes), jnp.float32), shape((groups, 2 * SLOTS, lanes), bf16)],
         exchange(partial_branch, TP),
-        near,
+        parts,
         placed,
         flops=SHORT,
     )
     held = local(
         spread_kernel,
         "spread",
-        shape((blocks, items, lanes), bf16),
+        shape((blocks // 2, 2 * items, lanes), bf16),
         exchange(outgoing, EP),
         flops=SHORT,
     )
@@ -351,7 +376,7 @@
         expert_kernel,
         "expert",
         shape((blocks, items, lanes), bf16),
-        exchange(held, TP),
+        exchange(held, NEAR),
         ffn_gain.reshape(blocks, lanes),
         w_gate,
         w_up,
@@ -378,8 +403,8 @@
 
 def solution(mesh):
     torus = Mesh(
-        mesh.devices.reshape(mesh.shape["ep"] // CORES, CORES, 4, 4),
-        ("ep_0", "ep_1", "tp_0", "tp_1"),
+        mesh.devices.reshape(mesh.shape["ep"] // CORES, CORES, 4, 2, 2),
+        ("ep_0", "ep_1", "tp_0", "tp_1", "tp_2"),
     )
     rows = ("ep_0", "ep_1")
     in_specs = (

time: 102 us -> 102 us (level)
  no operation moved by 1% of the time
where the time goes in v5:
time: 102 us
  blocking collectives  96.5 us (95%)
  Pallas kernels  4.64 us (5%)
    all_to_all x6, blocking collectives, exchange(): return lax.all_to_all(x, axis, 0, 0, tiled=True)  96.5 us
    pallas_call x8, Pallas kernels, local(): pl.pallas_call(kernel, in_specs=places(len(args), far_in), out_specs=outs...  4.64 us

profile of v5, /device:TPU:1, one launch (start us, length us, event | category | flops | bytes accessed | tf_op | source)
XLA Modules:
  0.0 102.0 jit_solution(5488271642888440203)
XLA Ops:
  0.6 0.8 load.1
  1.5 0.0 copy-start
  1.5 0.0 copy-start.1
  1.5 0.0 copy-start.5
  1.5 0.0 copy-start.6
  1.5 0.0 copy-start.7
  1.5 0.0 copy-start.8
  1.5 0.0 copy-start.9
  1.6 14.1 %all_to_all.30.parts_ref.resid_ref = bf16[16,8,128]{2,1,0:T(8,128)(2,1)S(1)} all-to-all(bf16[16,8,128]{2,1,0:T(8,128)(2,1)S(1)} %copies.1), channel_id=1, replica_groups=mesh['ep_0'=16,'ep_1'=2,'tp_0'=4,'tp_1'=2,'tp_2'=2] {'tp_0','tp_1','tp_2'}, dimensions={0} | all-to-all | bytes 65536 | tf_op jit(solution)/shard_map/all_to_all | solution.py:292
  15.6 0.0 copy-done
  15.6 0.0 copy-done.1
  15.6 0.0 copy-done.5
  15.7 0.0 copy-done.6
  15.7 0.0 copy-done.7
  15.7 0.0 copy-done.8
  15.7 0.0 copy-done.9
  15.7 1.8 %attend.1 = (bf16[8,64]{1,0:T(8,128)(2,1)}, bf16[8,64]{1,0:T(8,128)(2,1)}, bf16[16,24,128]{2,1,0:T(8,128)(2,1)S(1)}, bf16[128,8]{1,0:T(8,128)(2,1)S(1)}, bf16[12...) custom-call(bf16[16,8,128]{2,1,0:T(8,128)(2,1)S(1)} %all_to_all.30.parts_ref.resid_ref, ...), custom_call_target="tpu_custom_call" | custom-call | tf_op jit(solution)/shard_map/attend/pallas_call | solution.py:279
  17.5 9.7 %all_to_all.31.parts_ref = bf16[16,24,128]{2,1,0:T(8,128)(2,1)S(1)} all-to-all(bf16[16,24,128]{2,1,0:T(8,128)(2,1)S(1)} %get-tuple-element.23), channel_id=1, replica_groups=mesh['ep_0'=16,'ep_1'=2,'tp_0'=4,'tp_1'=2,'tp_2'=2] {'tp_0','tp_1','tp_2'}, dimensions={0} | all-to-all | bytes 196608 | tf_op jit(solution)/shard_map/all_to_all | solution.py:292
  27.2 0.3 middle.1
  27.5 32.0 %all_to_all.32.arrived_ref = bf16[32,8,128]{2,1,0:T(8,128)(2,1)S(1)} all-to-all(bf16[32,8,128]{2,1,0:T(8,128)(2,1)S(1)} %get-tuple-element.25), channel_id=1, replica_groups=mesh['ep_0'=16,'ep_1'=2,'tp_0'=4,'tp_1'=2,'tp_2'=2] {'ep_1','ep_0'}, dimensions={0} | all-to-all | bytes 131072 | tf_op jit(solution)/shard_map/all_to_all | solution.py:292
  59.6 0.2 spread.1
  59.7 0.0 copy-start.2
  59.8 0.0 copy-start.10
  59.8 11.7 %all_to_all.33.rows_ref = bf16[8,192,128]{2,1,0:T(8,128)(2,1)S(1)} all-to-all(bf16[8,192,128]{2,1,0:T(8,128)(2,1)S(1)} %spread.1), channel_id=1, replica_groups=mesh['ep_0'=16,'ep_1'=2,'tp_0'=4,'tp_1'=2,'tp_2'=2] {'tp_0','tp_2'}, dimensions={0} | all-to-all | bytes 786432 | tf_op jit(solution)/shard_map/all_to_all | solution.py:292
  71.5 0.0 copy-done.3
  71.5 0.0 copy-done.4
  71.5 0.0 copy-done.2
  71.5 0.6 expert.1
  72.1 11.7 %all_to_all.34.parts_ref = bf16[16,96,128]{2,1,0:T(8,128)(2,1)S(1)} all-to-all(bf16[16,96,128]{2,1,0:T(8,128)(2,1)S(1)} %expert.1), channel_id=1, replica_groups=mesh['ep_0'=16,'ep_1'=2,'tp_0'=4,'tp_1'=2,'tp_2'=2] {'tp_0','tp_1','tp_2'}, dimensions={0} | all-to-all | bytes 786432 | tf_op jit(solution)/shard_map/all_to_all | solution.py:292
  83.8 0.2 total.1
  84.0 17.2 %all_to_all.35.returned_ref = bf16[32,4,128]{2,1,0:T(4,128)(2,1)S(1)} all-to-all(bf16[32,4,128]{2,1,0:T(4,128)(2,1)S(1)} %total.1), channel_id=1, replica_groups=mesh['ep_0'=16,'ep_1'=2,'tp_0'=4,'tp_1'=2,'tp_2'=2] {'ep_1','ep_0'}, dimensions={0} | all-to-all | bytes 65536 | tf_op jit(solution)/shard_map/all_to_all | solution.py:292
  101.3 0.8 mixture.1
  (4 shorter events, 0.0 us)
Async XLA Ops:
  1.5 14.2 %copy-start = (bf16[8,1,64,1024]{3,2,1,0:T(8,128)(2,1)S(1)}, bf16[8,1,64,1024]{3,2,1,0:T(8,128)(2,1)}, u32[]{:S(2)}) copy-start(bf16[8,1,64,1024]{3,2,1,0:T(8,128)(2,1)} %key_ref.1) | copy-start | bytes 3145732
  1.5 14.2 %copy-start.1 = (bf16[8,1,64,1024]{3,2,1,0:T(8,128)(2,1)S(1)}, bf16[8,1,64,1024]{3,2,1,0:T(8,128)(2,1)}, u32[]{:S(2)}) copy-start(bf16[8,1,64,1024]{3,2,1,0:T(8,128)(2,1)} %value_ref.1) | copy-start | bytes 3145732
  1.5 14.2 %copy-start.5 = (bf16[2048,64]{0,1:T(8,128)(2,1)S(1)}, bf16[2048,64]{0,1:T(8,128)(2,1)}, u32[]{:S(2)}) copy-start(bf16[2048,64]{0,1:T(8,128)(2,1)} %param.19) | copy-start | bytes 786436
  1.5 14.2 %copy-start.6 = (bf16[2048,64]{0,1:T(8,128)(2,1)S(1)}, bf16[2048,64]{0,1:T(8,128)(2,1)}, u32[]{:S(2)}) copy-start(bf16[2048,64]{0,1:T(8,128)(2,1)} %param.20) | copy-start | bytes 786436
  1.5 14.2 %copy-start.7 = (bf16[2048,64]{0,1:T(8,128)(2,1)S(1)}, bf16[2048,64]{0,1:T(8,128)(2,1)}, u32[]{:S(2)}) copy-start(bf16[2048,64]{0,1:T(8,128)(2,1)} %param.21) | copy-start | bytes 786436
  1.5 14.2 %copy-start.8 = (bf16[64,2048]{1,0:T(8,128)(2,1)S(1)}, bf16[64,2048]{1,0:T(8,128)(2,1)}, u32[]{:S(2)}) copy-start(bf16[64,2048]{1,0:T(8,128)(2,1)} %wout_ref.1) | copy-start | bytes 786436
  1.5 14.1 %copy-start.9 = (f32[8,1,1024]{2,1,0:T(1,128)S(1)}, f32[8,1,1024]{2,1,0:T(1,128)}, u32[]{:S(2)}) copy-start(f32[8,1,1024]{2,1,0:T(1,128)} %bias_ref.1) | copy-start | bytes 98308
  59.6 11.9 %copy-start.3 = (bf16[1,2048,128]{2,1,0:T(8,128)(2,1)S(1)}, bf16[1,2048,128]{2,1,0:T(8,128)(2,1)}, u32[]{:S(2)}) copy-start(bf16[1,2048,128]{2,1,0:T(8,128)(2,1)} %up_ref.1) | copy-start | bytes 1572868
  59.6 11.9 %copy-start.4 = (bf16[1,128,2048]{2,1,0:T(8,128)(2,1)S(1)}, bf16[1,128,2048]{2,1,0:T(8,128)(2,1)}, u32[]{:S(2)}) copy-start(bf16[1,128,2048]{2,1,0:T(8,128)(2,1)} %down_ref.1) | copy-start | bytes 1572868
  59.7 11.8 %copy-start.2 = (bf16[1,2048,128]{2,1,0:T(8,128)(2,1)S(1)}, bf16[1,2048,128]{2,1,0:T(8,128)(2,1)}, u32[]{:S(2)}) copy-start(bf16[1,2048,128]{2,1,0:T(8,128)(2,1)} %gate_ref.1) | copy-start | bytes 1572868
  59.8 11.8 %copy-start.10 = (f32[2048]{0:T(1024)S(1)}, f32[2048]{0:T(1024)}, u32[]{:S(2)}) copy-start(f32[2048]{0:T(1024)} %param.28) | copy-start | bytes 24580

commit v6 on v4

--- a/solution.py
+++ b/solution.py
@@ -6,14 +6,15 @@
 from jax.sharding import Mesh
 from jax.sharding import PartitionSpec as P
 
+
 TP = ("tp_0", "tp_1")
 EP = ("ep_1", "ep_0")
 CORES = 2
+PAIRS = (1, 4)
 
 eps = 1e-06
 limit = 7.0
 alpha = 1.702
-LANES = 128
 SLOTS = 4
 CAP = 3
 LIMIT = 16 * 1024 * 1024
@@ -184,26 +185,37 @@
 
 
 def spread_kernel(arrived_ref, out_ref):
-    blocks, items, lanes = out_ref.shape
+    blocks, half, lanes = out_ref.shape
     groups, slots, _ = arrived_ref.shape
     arrived = arrived_ref[...].astype(jnp.float32).reshape(groups * slots, lanes)
     held = jnp.dot(
-        packing(items, groups * slots),
+        packing(2 * half, groups * slots),
         arrived.astype(jnp.bfloat16),
         preferred_element_type=jnp.float32,
     ).astype(jnp.bfloat16)
+    first = lax.axis_index(EP[0]) == 0
+    halves = [held[i * half : (i + 1) * half] for i in range(2)]
+    mixed = [jnp.where(first, halves[i], halves[1 - i]) for i in range(2)]
     for t in range(blocks):
-        out_ref[t] = held
+        side, other = [int(t & step > 0) for step in PAIRS]
+        out_ref[t] = halves[side] if side == other else mixed[side]
 
 
 def total_kernel(parts_ref, out_ref):
-    blocks, items, lanes = parts_ref.shape
+    blocks, half, lanes = parts_ref.shape
     groups, slots, _ = out_ref.shape
-    total = parts_ref[0].astype(jnp.float32)
-    for t in range(1, blocks):
-        total = total + parts_ref[t].astype(jnp.float32)
+    sums = {}
+    for t in range(blocks):
+        kind = tuple(int(t & step > 0) for step in PAIRS)
+        part = parts_ref[t].astype(jnp.float32)
+        sums[kind] = sums[kind] + part if kind in sums else part
+    first = lax.axis_index(EP[0]) == 0
+    total = [
+        sums[i, i] + jnp.where(first, sums[i, 1 - i], sums[1 - i, i]) for i in range(2)
+    ]
+    total = jnp.concatenate(total, axis=0)
     spaced = lax.dot_general(
-        packing(items, groups * slots),
+        packing(2 * half, groups * slots),
         total.astype(jnp.bfloat16),
         (((0,), (0,)), ((), ())),
         preferred_element_type=jnp.float32,
@@ -224,7 +236,8 @@
     out_ref[...] = (middle_ref[...] + mixture).astype(jnp.bfloat16)
 
 
-def expert_kernel(rows_ref, gain_ref, gate_ref, up_ref, down_ref, out_ref):
+def expert_kernel(rows_ref, gain_ref, *refs):
+    gates, ups, downs, out_ref = refs[0:2], refs[2:4], refs[4:6], refs[6]
     blocks, rows, lanes = rows_ref.shape
     total = jnp.zeros((rows, lanes), jnp.float32)
     scaled = []
@@ -234,17 +247,20 @@
         scaled.append((x * gain_ref[t : t + 1, :]).astype(jnp.bfloat16))
     scaled = jnp.concatenate(scaled, axis=1)
     scale = lax.rsqrt(jnp.sum(total, axis=1, keepdims=True) / (blocks * lanes) + eps)
-    gate = jnp.dot(scaled, gate_ref[0], preferred_element_type=jnp.float32) * scale
-    upper = jnp.dot(scaled, up_ref[0], preferred_element_type=jnp.float32) * scale
+    gate = jnp.concatenate([ref[0] for ref in gates], axis=1)
+    gate = jnp.dot(scaled, gate, preferred_element_type=jnp.float32) * scale
+    upper = jnp.concatenate([ref[0] for ref in ups], axis=1)
+    upper = jnp.dot(scaled, upper, preferred_element_type=jnp.float32) * scale
     gate = jnp.minimum(gate, limit)
     upper = jnp.clip(upper, -limit, limit)
     active = ((upper + 1.0) * gate * jax.nn.sigmoid(alpha * gate)).astype(jnp.bfloat16)
-    result = jnp.dot(active, down_ref[0], preferred_element_type=jnp.float32).astype(jnp.bfloat16)
+    down = jnp.concatenate([ref[0] for ref in downs], axis=0)
+    result = jnp.dot(active, down, preferred_element_type=jnp.float32).astype(jnp.bfloat16)
     for t in range(blocks):
         out_ref[t] = result[:, t * lanes : (t + 1) * lanes]
 
 
-def local(kernel, name, out_shape, *args, flops=0, far_in=0, far_out=0, scratch=()):
+def local(kernel, out_shape, *args, flops=0, far_in=0, far_out=0, scratch=()):
     def places(count, far):
         return [pl.BlockSpec(memory_space=pltpu.HBM)] * far + [
             pl.BlockSpec(memory_space=pltpu.VMEM)
@@ -260,7 +276,6 @@
         scratch_shapes=scratch,
         compiler_params=pltpu.CompilerParams(vmem_limit_bytes=LIMIT),
         cost_estimate=pl.CostEstimate(flops=flops, bytes_accessed=0, transcendentals=0),
-        name=name,
     )(*[pltpu.with_memory_space_constraint(x, pltpu.HBM) for x in args[:far_in]], *args[far_in:])
 
 
@@ -268,7 +283,7 @@
     return lax.all_to_all(x, axis, 0, 0, tiled=True)
 
 
-def body(
+def layer(
     resid,
     attn_gain,
     w_query,
@@ -306,18 +321,18 @@
     )
     near, *small = local(
         load_kernel,
-        "load",
         [shape(x.shape, x.dtype) for x in small],
         *small,
         far_in=len(small),
         scratch=[pltpu.SemaphoreType.DMA((len(small),))],
     )
-    copies = local(
-        copies_kernel, "copies", shape((blocks, rows, lanes), bf16), near, flops=LONG
-    )
+    copies = local(copies_kernel, shape((blocks, rows, lanes), bf16), near, flops=LONG)
+    weights = []
+    pairs = [(i, i ^ PAIRS[i // blocks]) for i in range(CORES * blocks)]
+    for weight in (w_gate, w_up, w_down):
+        weights += [weight, lax.ppermute(weight, (EP[0], *TP), pairs)]
     new_keys, new_values, partial_branch, placed, high, low = local(
         attend_kernel,
-        "attend",
         [new, new, shape((blocks, 2 * rows, lanes), bf16)] + [shape((slots, rows), bf16)] * 3,
         exchange(copies, TP),
         *small,
@@ -333,45 +348,26 @@
     )
     middle, outgoing = local(
         middle_kernel,
-        "middle",
         [shape((rows, lanes), jnp.float32), shape((groups, SLOTS, lanes), bf16)],
         exchange(partial_branch, TP),
         near,
         placed,
         flops=SHORT,
     )
-    held = local(
-        spread_kernel,
-        "spread",
-        shape((blocks, items, lanes), bf16),
-        exchange(outgoing, EP),
-        flops=SHORT,
-    )
+    arrived = exchange(outgoing, EP)
+    held = local(spread_kernel, shape((blocks, items // 2, lanes), bf16), arrived, flops=SHORT)
     partial_out = local(
         expert_kernel,
-        "expert",
-        shape((blocks, items, lanes), bf16),
+        shape((blocks, items // 2, lanes), bf16),
         exchange(held, TP),
         ffn_gain.reshape(blocks, lanes),
-        w_gate,
-        w_up,
-        w_down,
+        *weights,
     )
     result = local(
-        total_kernel,
-        "total",
-        shape((groups, SLOTS, lanes), bf16),
-        exchange(partial_out, TP),
-        flops=SHORT,
+        total_kernel, shape((groups, SLOTS, lanes), bf16), exchange(partial_out, TP), flops=SHORT
     )
     mixed = local(
-        mixture_kernel,
-        "mixture",
-        shape((rows, lanes), bf16),
-        exchange(result, EP),
-        middle,
-        high,
-        low,
+        mixture_kernel, shape((rows, lanes), bf16), exchange(result, EP), middle, high, low
     )
     return (mixed, new_keys, new_values)
 
@@ -402,4 +398,4 @@
         P(rows, TP, None),
     )
     out_specs = (P(rows, TP), P(rows, TP), P(rows, TP))
-    return jax.shard_map(body, mesh=torus, in_specs=in_specs, out_specs=out_specs, check_vma=False)
+    return jax.shard_map(layer, mesh=torus, in_specs=in_specs, out_specs=out_specs, check_vma=False)

time: 102 us -> 105 us (1.029)
  starting transfers between devices: 0 us -> 12 us
  blocking collectives: 96.3 us -> 86.3 us
    all_to_all x6 -> x5, blocking collectives: 96.3 us -> 86.3 us  [exchange(): return lax.all_to_all(x, axis, 0, 0, tiled=True)]
    ppermute x0 -> x3, starting transfers between devices: none -> 8.45 us  [layer(): weights += [weight, lax.ppermute(weight, (EP[0], *TP), pairs)]]
    all_to_all x0 -> x1, starting transfers between devices: none -> 3.5 us  [exchange(): return lax.all_to_all(x, axis, 0, 0, tiled=True)]
  transfers between devices with their start and end apart: 0 -> 4, of which waited for: 0 -> 0; matrix products, arithmetic and copies ran while one was open for 0% -> 0% of each run, Pallas kernels for 0% -> 0%
where the time goes in v6:
time: 105 us; the launch traced here: 104 us
  blocking collectives  86.3 us (82%)
  starting transfers between devices  12 us (11%)
  Pallas kernels  5.04 us (5%)
    all_to_all x5, blocking collectives, exchange(): return lax.all_to_all(x, axis, 0, 0, tiled=True)  86.3 us
    ppermute x3, starting transfers between devices, layer(): weights += [weight, lax.ppermute(weight, (EP[0], *TP), pairs)]  8.45 us
    pallas_call x8, Pallas kernels, local(): pl.pallas_call(kernel, in_specs=places(len(args), far_in), out_specs=outs...  5.04 us
    all_to_all x1, starting transfers between devices, exchange(): return lax.all_to_all(x, axis, 0, 0, tiled=True)  3.5 us
  transfers between devices with their start and end apart: 4, of which 0 were waited for; matrix products, arithmetic and copies ran while one was open for 0% of the time, Pallas kernels for 0%

profile of v6, /device:TPU:1, one launch (start us, length us, event | category | flops | bytes accessed | tf_op | source)
XLA Modules:
  0.0 104.2 jit_solution(13708457368955455172)
XLA Ops:
  0.6 0.8 shard_map.184
  1.5 0.0 copy-start
  1.5 0.0 copy-start.1
  1.5 0.0 copy-start.5
  1.5 0.0 copy-start.6
  1.5 0.0 copy-start.7
  1.5 0.0 copy-start.8
  1.5 0.0 copy-start.9
  1.6 14.1 %all_to_all.30.parts_ref = bf16[16,8,128]{2,1,0:T(8,128)(2,1)S(1)} all-to-all(bf16[16,8,128]{2,1,0:T(8,128)(2,1)S(1)} %shard_map.185), channel_id=1, replica_groups=mesh['ep_0'=16,'ep_1'=2,'tp_0'=4,'tp_1'=4] {'tp_0','tp_1'}, dimensions={0} | all-to-all | bytes 65536 | tf_op jit(solution)/shard_map/all_to_all | solution.py:283
  15.7 0.0 copy-start.2
  15.7 0.0 copy-start.3
  15.7 0.0 copy-start.4
  15.7 2.1 %shard_map.186 = (bf16[8,64]{1,0:T(8,128)(2,1)}, bf16[8,64]{1,0:T(8,128)(2,1)}, bf16[16,16,128]{2,1,0:T(8,128)(2,1)}, bf16[128,8]{1,0:T(8,128)(2,1)S(1)}, bf16[1...) custom-call(bf16[16,8,128]{2,1,0:T(8,128)(2,1)S(1)} %all_to_all.30.parts_ref, s32[1,8]{1,0:T(1,128)S(1)} %get-tuple-element.18.lengths_ref, ...), custom_call_target="tpu_custom_call" | custom-call | tf_op jit(solution)/shard_map/pallas_call | solution.py:271
  17.8 3.5 %all-to-all-start.1 = ((bf16[16,16,128]{2,1,0:T(8,128)(2,1)}), bf16[16,16,128]{2,1,0:T(8,128)(2,1)S(1)}, u32[]{:S(2)}, u32[]{:S(2)}) async-start(bf16[16,16,128]{2,1,0:T(8,128)(2,1)} %get-tuple-element.23), calls=%async_computation.1 | async-start | bytes 131072 | tf_op jit(solution)/shard_map/all_to_all | solution.py:283
  21.3 0.0 copy-done.2
  21.3 3.2 %collective-permute-start = (bf16[1,2048,128]{2,1,0:T(8,128)(2,1)S(1)}, bf16[1,2048,128]{2,1,0:T(8,128)(2,1)S(1)}, u32[]{:S(2)}, u32[]{:S(2)}) collective-permute-start(bf16[1,2048,128]{2,1,0:T(8,128)(2,1)S(1)} %copy-done.2), channel_id=1, source_target_pairs={{0,1},{1,0},{2,3},{3,2},{4,5},{5,4},{6,7},{7,6},{8,9},{9,8},{10,11... | collective-permute-start | bytes 1572872 | tf_op jit(solution)/shard_map/ppermute | solution.py:333
  24.5 2.1 %collective-permute-start.1 = (bf16[1,2048,128]{2,1,0:T(8,128)(2,1)S(1)}, bf16[1,2048,128]{2,1,0:T(8,128)(2,1)S(1)}, u32[]{:S(2)}, u32[]{:S(2)}) collective-permute-start(bf16[1,2048,128]{2,1,0:T(8,128)(2,1)S(1)} %copy-done.3), channel_id=1, source_target_pairs={{0,1},{1,0},{2,3},{3,2},{4,5},{5,4},{6,7},{7,6},{8,9},{9,8},{10,11... | collective-permute-start | bytes 1572872 | tf_op jit(solution)/shard_map/ppermute | solution.py:333
  26.7 3.2 %collective-permute-start.2 = (bf16[1,128,2048]{2,1,0:T(8,128)(2,1)S(1)}, bf16[1,128,2048]{2,1,0:T(8,128)(2,1)S(1)}, u32[]{:S(2)}, u32[]{:S(2)}) collective-permute-start(bf16[1,128,2048]{2,1,0:T(8,128)(2,1)S(1)} %copy-done.4), channel_id=1, source_target_pairs={{0,1},{1,0},{2,3},{3,2},{4,5},{5,4},{6,7},{7,6},{8,9},{9,8},{10,11... | collective-permute-start | bytes 1572872 | tf_op jit(solution)/shard_map/ppermute | solution.py:333
  29.8 0.0 all-to-all-done.1.parts_ref
  29.9 0.3 shard_map.187
  30.2 30.7 %all_to_all.31.arrived_ref = bf16[32,4,128]{2,1,0:T(4,128)(2,1)S(1)} all-to-all(bf16[32,4,128]{2,1,0:T(4,128)(2,1)S(1)} %get-tuple-element.25), channel_id=1, replica_groups=mesh['ep_0'=16,'ep_1'=2,'tp_0'=4,'tp_1'=4] {'ep_1','ep_0'}, dimensions={0} | all-to-all | bytes 65536 | tf_op jit(solution)/shard_map/all_to_all | solution.py:283
  60.8 0.2 shard_map.188
  61.0 0.0 copy-start.10
  61.0 13.8 %all_to_all.32.rows_ref = bf16[16,48,128]{2,1,0:T(8,128)(2,1)S(1)} all-to-all(bf16[16,48,128]{2,1,0:T(8,128)(2,1)S(1)} %shard_map.188), channel_id=1, replica_groups=mesh['ep_0'=16,'ep_1'=2,'tp_0'=4,'tp_1'=4] {'tp_0','tp_1'}, dimensions={0} | all-to-all | bytes 393216 | tf_op jit(solution)/shard_map/all_to_all | solution.py:283
  74.8 0.0 collective-permute-done.refs_1_
  74.8 0.0 collective-permute-done.1.refs_3_
  74.9 0.0 collective-permute-done.2.refs_5_
  74.9 0.7 shard_map.189
  75.6 9.9 %all_to_all.33.parts_ref = bf16[16,48,128]{2,1,0:T(8,128)(2,1)S(1)} all-to-all(bf16[16,48,128]{2,1,0:T(8,128)(2,1)S(1)} %shard_map.189), channel_id=1, replica_groups=mesh['ep_0'=16,'ep_1'=2,'tp_0'=4,'tp_1'=4] {'tp_0','tp_1'}, dimensions={0} | all-to-all | bytes 393216 | tf_op jit(solution)/shard_map/all_to_all | solution.py:283
  85.5 0.2 shard_map.190
  85.7 17.8 %all_to_all.34.returned_ref = bf16[32,4,128]{2,1,0:T(4,128)(2,1)S(1)} all-to-all(bf16[32,4,128]{2,1,0:T(4,128)(2,1)S(1)} %shard_map.190), channel_id=1, replica_groups=mesh['ep_0'=16,'ep_1'=2,'tp_0'=4,'tp_1'=4] {'ep_1','ep_0'}, dimensions={0} | all-to-all | bytes 65536 | tf_op jit(solution)/shard_map/all_to_all | solution.py:283
  103.5 0.8 shard_map.191
  (11 shorter events, 0.0 us)
Async XLA Ops:
  1.5 14.2 %copy-start = (bf16[8,1,64,1024]{3,2,1,0:T(8,128)(2,1)S(1)}, bf16[8,1,64,1024]{3,2,1,0:T(8,128)(2,1)}, u32[]{:S(2)}) copy-start(bf16[8,1,64,1024]{3,2,1,0:T(8,128)(2,1)} %key_ref.1) | copy-start | bytes 3145732
  1.5 14.2 %copy-start.1 = (bf16[8,1,64,1024]{3,2,1,0:T(8,128)(2,1)S(1)}, bf16[8,1,64,1024]{3,2,1,0:T(8,128)(2,1)}, u32[]{:S(2)}) copy-start(bf16[8,1,64,1024]{3,2,1,0:T(8,128)(2,1)} %value_ref.1) | copy-start | bytes 3145732
  1.5 14.2 %copy-start.5 = (bf16[2048,64]{0,1:T(8,128)(2,1)S(1)}, bf16[2048,64]{0,1:T(8,128)(2,1)}, u32[]{:S(2)}) copy-start(bf16[2048,64]{0,1:T(8,128)(2,1)} %param.19) | copy-start | bytes 786436
  1.5 14.2 %copy-start.6 = (bf16[2048,64]{0,1:T(8,128)(2,1)S(1)}, bf16[2048,64]{0,1:T(8,128)(2,1)}, u32[]{:S(2)}) copy-start(bf16[2048,64]{0,1:T(8,128)(2,1)} %param.20) | copy-start | bytes 786436
  1.5 14.2 %copy-start.7 = (bf16[2048,64]{0,1:T(8,128)(2,1)S(1)}, bf16[2048,64]{0,1:T(8,128)(2,1)}, u32[]{:S(2)}) copy-start(bf16[2048,64]{0,1:T(8,128)(2,1)} %param.21) | copy-start | bytes 786436
  1.5 14.2 %copy-start.8 = (bf16[64,2048]{1,0:T(8,128)(2,1)S(1)}, bf16[64,2048]{1,0:T(8,128)(2,1)}, u32[]{:S(2)}) copy-start(bf16[64,2048]{1,0:T(8,128)(2,1)} %wout_ref.1) | copy-start | bytes 786436
  1.5 14.1 %copy-start.9 = (f32[8,1,1024]{2,1,0:T(1,128)S(1)}, f32[8,1,1024]{2,1,0:T(1,128)}, u32[]{:S(2)}) copy-start(f32[8,1,1024]{2,1,0:T(1,128)} %bias_ref.1) | copy-start | bytes 98308
  15.7 5.6 %copy-start.2 = (bf16[1,2048,128]{2,1,0:T(8,128)(2,1)S(1)}, bf16[1,2048,128]{2,1,0:T(8,128)(2,1)}, u32[]{:S(2)}) copy-start(bf16[1,2048,128]{2,1,0:T(8,128)(2,1)} %refs_0_.3) | copy-start | bytes 1572868
  15.7 8.8 %copy-start.3 = (bf16[1,2048,128]{2,1,0:T(8,128)(2,1)S(1)}, bf16[1,2048,128]{2,1,0:T(8,128)(2,1)}, u32[]{:S(2)}) copy-start(bf16[1,2048,128]{2,1,0:T(8,128)(2,1)} %refs_2_.1) | copy-start | bytes 1572868
  15.7 10.9 %copy-start.4 = (bf16[1,128,2048]{2,1,0:T(8,128)(2,1)S(1)}, bf16[1,128,2048]{2,1,0:T(8,128)(2,1)}, u32[]{:S(2)}) copy-start(bf16[1,128,2048]{2,1,0:T(8,128)(2,1)} %refs_4_.1) | copy-start | bytes 1572868
  17.8 12.0 %all-to-all-start.1 = ((bf16[16,16,128]{2,1,0:T(8,128)(2,1)}), bf16[16,16,128]{2,1,0:T(8,128)(2,1)S(1)}, u32[]{:S(2)}, u32[]{:S(2)}) async-start(bf16[16,16,128]{2,1,0:T(8,128)(2,1)} %get-tuple-element.23), calls=%async_computation.1 | async-start | bytes 131072 | tf_op jit(solution)/shard_map/all_to_all | solution.py:283
  21.3 53.5 %collective-permute-start = (bf16[1,2048,128]{2,1,0:T(8,128)(2,1)S(1)}, bf16[1,2048,128]{2,1,0:T(8,128)(2,1)S(1)}, u32[]{:S(2)}, u32[]{:S(2)}) collective-permute-start(bf16[1,2048,128]{2,1,0:T(8,128)(2,1)S(1)} %copy-done.2), channel_id=1, source_target_pairs={{0,1},{1,0},{2,3},{3,2},{4,5},{5,4},{6,7},{7,6},{8,9},{9,8},{10,11... | collective-permute-start | bytes 1572872 | tf_op jit(solution)/shard_map/ppermute | solution.py:333
  24.5 50.3 %collective-permute-start.1 = (bf16[1,2048,128]{2,1,0:T(8,128)(2,1)S(1)}, bf16[1,2048,128]{2,1,0:T(8,128)(2,1)S(1)}, u32[]{:S(2)}, u32[]{:S(2)}) collective-permute-start(bf16[1,2048,128]{2,1,0:T(8,128)(2,1)S(1)} %copy-done.3), channel_id=1, source_target_pairs={{0,1},{1,0},{2,3},{3,2},{4,5},{5,4},{6,7},{7,6},{8,9},{9,8},{10,11... | collective-permute-start | bytes 1572872 | tf_op jit(solution)/shard_map/ppermute | solution.py:333
  26.7 48.2 %collective-permute-start.2 = (bf16[1,128,2048]{2,1,0:T(8,128)(2,1)S(1)}, bf16[1,128,2048]{2,1,0:T(8,128)(2,1)S(1)}, u32[]{:S(2)}, u32[]{:S(2)}) collective-permute-start(bf16[1,128,2048]{2,1,0:T(8,128)(2,1)S(1)} %copy-done.4), channel_id=1, source_target_pairs={{0,1},{1,0},{2,3},{3,2},{4,5},{5,4},{6,7},{7,6},{8,9},{9,8},{10,11... | collective-permute-start | bytes 1572872 | tf_op jit(solution)/shard_map/ppermute | solution.py:333
  61.0 13.8 %copy-start.10 = (f32[2048]{0:T(1024)S(1)}, f32[2048]{0:T(1024)}, u32[]{:S(2)}) copy-start(f32[2048]{0:T(1024)} %param.28) | copy-start | bytes 24580

commit v7 on v6

--- a/solution.py
+++ b/solution.py
@@ -47,17 +47,29 @@
     return hits, named & (rank == slot % SLOTS)
 
 
-def attend_kernel(parts_ref, lengths_ref, gain_ref, mix_ref, experts_ref, share_ref, wq_ref,
+def attend_kernel(wgate_ref, wup_ref, wdown_ref, parts_ref, lengths_ref, gain_ref, mix_ref, experts_ref, share_ref, wq_ref,
                   wk_ref, wv_ref, key_ref, value_ref, bias_ref, wout_ref, new_key_ref,
-                  new_value_ref, out_ref, placed_ref, high_ref, low_ref, fresh_ref, sems):
+                  new_value_ref, joined_ref, out_ref, placed_ref, high_ref, low_ref, fresh_ref,
+                  sems, join_sems):
     blocks, rows, lanes = parts_ref.shape
+    width = blocks * lanes
+    pieces = [(wgate_ref.at[0], 0), (wup_ref.at[0], width)] + [
+        (wdown_ref.at[0, :, pl.ds(t * lanes, lanes)], 2 * width + t * lanes) for t in range(blocks)
+    ]
+    joins = [
+        pltpu.make_async_copy(
+            source, joined_ref.at[pl.ds(start, source.shape[0])], join_sems.at[i]
+        )
+        for i, (source, start) in enumerate(pieces)
+    ]
+    for join in joins:
+        join.start()
     heads = key_ref.shape[2]
     cache = key_ref.shape[3]
     xs = [parts_ref[t].astype(jnp.float32) for t in range(blocks)]
     total = xs[0] * xs[0]
     for x in xs[1:]:
         total = total + x * x
-    width = blocks * lanes
     scale = lax.rsqrt(jnp.sum(total, axis=1, keepdims=True) / width + eps)
     normed = jnp.concatenate(
         [(xs[t] * scale * gain_ref[t : t + 1, :]).astype(jnp.bfloat16) for t in range(blocks)],
@@ -138,8 +150,8 @@
     placed_ref[...] = placed.astype(jnp.bfloat16)
     high_ref[...] = high
     low_ref[...] = (weight - high.astype(jnp.float32)).astype(jnp.bfloat16)
-    for store in stores:
-        store.wait()
+    for copy in stores + joins:
+        copy.wait()
 
 
 def load_kernel(*refs):
@@ -237,7 +249,7 @@
 
 
 def expert_kernel(rows_ref, gain_ref, *refs):
-    gates, ups, downs, out_ref = refs[0:2], refs[2:4], refs[4:6], refs[6]
+    gate_ref, up_ref, down_ref, joined_ref, out_ref = refs
     blocks, rows, lanes = rows_ref.shape
     total = jnp.zeros((rows, lanes), jnp.float32)
     scaled = []
@@ -247,14 +259,16 @@
         scaled.append((x * gain_ref[t : t + 1, :]).astype(jnp.bfloat16))
     scaled = jnp.concatenate(scaled, axis=1)
     scale = lax.rsqrt(jnp.sum(total, axis=1, keepdims=True) / (blocks * lanes) + eps)
-    gate = jnp.concatenate([ref[0] for ref in gates], axis=1)
+    width = blocks * lanes
+    gate = jnp.concatenate([gate_ref[0], joined_ref[:width]], axis=1)
     gate = jnp.dot(scaled, gate, preferred_element_type=jnp.float32) * scale
-    upper = jnp.concatenate([ref[0] for ref in ups], axis=1)
+    upper = jnp.concatenate([up_ref[0], joined_ref[width : 2 * width]], axis=1)
     upper = jnp.dot(scaled, upper, preferred_element_type=jnp.float32) * scale
     gate = jnp.minimum(gate, limit)
     upper = jnp.clip(upper, -limit, limit)
     active = ((upper + 1.0) * gate * jax.nn.sigmoid(alpha * gate)).astype(jnp.bfloat16)
-    down = jnp.concatenate([ref[0] for ref in downs], axis=0)
+    other = [joined_ref[2 * width + t * lanes : 2 * width + (t + 1) * lanes] for t in range(blocks)]
+    down = jnp.concatenate([down_ref[0], jnp.concatenate(other, axis=1)], axis=0)
     result = jnp.dot(active, down, preferred_element_type=jnp.float32).astype(jnp.bfloat16)
     for t in range(blocks):
         out_ref[t] = result[:, t * lanes : (t + 1) * lanes]
@@ -327,13 +341,13 @@
         scratch=[pltpu.SemaphoreType.DMA((len(small),))],
     )
     copies = local(copies_kernel, shape((blocks, rows, lanes), bf16), near, flops=LONG)
-    weights = []
-    pairs = [(i, i ^ PAIRS[i // blocks]) for i in range(CORES * blocks)]
-    for weight in (w_gate, w_up, w_down):
-        weights += [weight, lax.ppermute(weight, (EP[0], *TP), pairs)]
-    new_keys, new_values, partial_branch, placed, high, low = local(
+    new_keys, new_values, joined, partial_branch, placed, high, low = local(
         attend_kernel,
-        [new, new, shape((blocks, 2 * rows, lanes), bf16)] + [shape((slots, rows), bf16)] * 3,
+        [new, new, shape((3 * blocks * lanes, lanes), bf16), shape((blocks, 2 * rows, lanes), bf16)]
+        + [shape((slots, rows), bf16)] * 3,
+        w_gate,
+        w_up,
+        w_down,
         exchange(copies, TP),
         *small,
         w_query.T,
@@ -343,25 +357,37 @@
         value_cache,
         key_bias,
         w_out,
-        far_out=2,
-        scratch=[pltpu.VMEM((2, rows, heads), bf16), pltpu.SemaphoreType.DMA((2,))],
-    )
+        far_in=3,
+        far_out=3,
+        scratch=[
+            pltpu.VMEM((2, rows, heads), bf16),
+            pltpu.SemaphoreType.DMA((2,)),
+            pltpu.SemaphoreType.DMA((2 + blocks,)),
+        ],
+    )
+    pairs = [(i, i ^ PAIRS[i // blocks]) for i in range(CORES * blocks)]
+    branch = exchange(partial_branch, TP)
+    joined = lax.ppermute(joined, (EP[0], *TP), pairs)
     middle, outgoing = local(
         middle_kernel,
         [shape((rows, lanes), jnp.float32), shape((groups, SLOTS, lanes), bf16)],
-        exchange(partial_branch, TP),
+        branch,
         near,
         placed,
         flops=SHORT,
     )
-    arrived = exchange(outgoing, EP)
-    held = local(spread_kernel, shape((blocks, items // 2, lanes), bf16), arrived, flops=SHORT)
+    held = local(
+        spread_kernel, shape((blocks, items // 2, lanes), bf16), exchange(outgoing, EP), flops=SHORT
+    )
     partial_out = local(
         expert_kernel,
         shape((blocks, items // 2, lanes), bf16),
         exchange(held, TP),
         ffn_gain.reshape(blocks, lanes),
-        *weights,
+        w_gate,
+        w_up,
+        w_down,
+        joined,
     )
     result = local(
         total_kernel, shape((groups, SLOTS, lanes), bf16), exchange(partial_out, TP), flops=SHORT

time: 105 us -> 115 us (1.095)
  blocking collectives: 86.3 us -> 106 us
  starting transfers between devices: 12 us -> 2.19 us
    all_to_all x5 -> x6, blocking collectives: 86.3 us -> 106 us  [exchange(): return lax.all_to_all(x, axis, 0, 0, tiled=True)]
    ppermute x3 -> x1, starting transfers between devices: 8.45 us -> 2.19 us  [layer(): joined = lax.ppermute(joined, (EP[0], *TP), pairs)]
    all_to_all x1 -> x0, starting transfers between devices: 3.5 us -> none  [exchange(): return lax.all_to_all(x, axis, 0, 0, tiled=True)]
  transfers between devices with their start and end apart: 4 -> 1, of which waited for: 0 -> 0; matrix products, arithmetic and copies ran while one was open for 0% -> 0% of each run, Pallas kernels for 0% -> 0%
where the time goes in v7:
time: 115 us; the launch traced here: 114 us
  blocking collectives  106 us (92%)
  Pallas kernels  5.44 us (5%)
  starting transfers between devices  2.19 us (2%)
    all_to_all x6, blocking collectives, exchange(): return lax.all_to_all(x, axis, 0, 0, tiled=True)  106 us
    pallas_call x8, Pallas kernels, local(): pl.pallas_call(kernel, in_specs=places(len(args), far_in), out_specs=outs...  5.44 us
  transfers between devices with their start and end apart: 1, of which 0 were waited for; matrix products, arithmetic and copies ran while one was open for 0% of the time, Pallas kernels for 0%

profile of v7, /device:TPU:1, one launch (start us, length us, event | category | flops | bytes accessed | tf_op | source)
XLA Modules:
  0.0 114.3 jit_solution(2629551594811290439)
XLA Ops:
  0.6 0.8 shard_map.184
  1.5 0.0 copy-start.3
  1.5 0.0 copy-start.4
  1.5 0.0 copy-start.5
  1.5 0.0 copy-start.6
  1.5 0.0 copy-start.7
  1.5 0.0 copy-start.8
  1.5 0.0 copy-start.9
  1.6 14.1 %all_to_all.30.parts_ref = bf16[16,8,128]{2,1,0:T(8,128)(2,1)S(1)} all-to-all(bf16[16,8,128]{2,1,0:T(8,128)(2,1)S(1)} %shard_map.185), channel_id=1, replica_groups=mesh['ep_0'=16,'ep_1'=2,'tp_0'=4,'tp_1'=4] {'tp_0','tp_1'}, dimensions={0} | all-to-all | bytes 65536 | tf_op jit(solution)/shard_map/all_to_all | solution.py:297
  15.6 0.0 copy-done.3
  15.6 0.0 copy-done.4
  15.6 0.0 copy-done.5
  15.7 0.0 copy-done.6
  15.7 0.0 copy-done.7
  15.7 0.0 copy-done.8
  15.7 0.0 copy-done.9
  15.7 2.5 %shard_map.186 = (bf16[8,64]{1,0:T(8,128)(2,1)}, bf16[8,64]{1,0:T(8,128)(2,1)}, bf16[6144,128]{1,0:T(8,128)(2,1)S(1)}, bf16[16,16,128]{2,1,0:T(8,128)(2,1)S(1)},...) custom-call(bf16[1,2048,128]{2,1,0:T(8,128)(2,1)} %refs_0_.3, ...), custom_call_target="tpu_custom_call" | custom-call | tf_op jit(solution)/shard_map/pallas_call | solution.py:285
  18.2 2.2 %collective-permute-start = (bf16[6144,128]{1,0:T(8,128)(2,1)S(1)}, bf16[6144,128]{1,0:T(8,128)(2,1)S(1)}, u32[]{:S(2)}, u32[]{:S(2)}) collective-permute-start(bf16[6144,128]{1,0:T(8,128)(2,1)S(1)} %get-tuple-element.27), channel_id=1, source_target_pairs={{0,1},{1,0},{2,3},{3,2},{4,5},{5,4},{6,7},{7,6},{8,9},{9,8},{10,11... | collective-permute-start | bytes 4718600 | tf_op jit(solution)/shard_map/ppermute | solution.py:370
  20.4 20.1 %all_to_all.31.parts_ref = bf16[16,16,128]{2,1,0:T(8,128)(2,1)S(1)} all-to-all(bf16[16,16,128]{2,1,0:T(8,128)(2,1)S(1)} %get-tuple-element.24), channel_id=1, replica_groups=mesh['ep_0'=16,'ep_1'=2,'tp_0'=4,'tp_1'=4] {'tp_0','tp_1'}, dimensions={0} | all-to-all | bytes 131072 | tf_op jit(solution)/shard_map/all_to_all | solution.py:297
  40.5 0.3 shard_map.187
  40.8 31.6 %all_to_all.32.arrived_ref = bf16[32,4,128]{2,1,0:T(4,128)(2,1)S(1)} all-to-all(bf16[32,4,128]{2,1,0:T(4,128)(2,1)S(1)} %get-tuple-element.26), channel_id=1, replica_groups=mesh['ep_0'=16,'ep_1'=2,'tp_0'=4,'tp_1'=4] {'ep_1','ep_0'}, dimensions={0} | all-to-all | bytes 65536 | tf_op jit(solution)/shard_map/all_to_all | solution.py:297
  72.3 0.2 shard_map.188
  72.5 12.4 %all_to_all.33.rows_ref = bf16[16,48,128]{2,1,0:T(8,128)(2,1)S(1)} all-to-all(bf16[16,48,128]{2,1,0:T(8,128)(2,1)S(1)} %shard_map.188), channel_id=1, replica_groups=mesh['ep_0'=16,'ep_1'=2,'tp_0'=4,'tp_1'=4] {'tp_0','tp_1'}, dimensions={0} | all-to-all | bytes 393216 | tf_op jit(solution)/shard_map/all_to_all | solution.py:297
  84.9 0.0 collective-permute-done.refs_3_
  84.9 0.0 copy-done
  84.9 0.0 copy-done.1
  84.9 0.0 copy-done.2
  84.9 0.7 shard_map.189
  85.7 9.9 %all_to_all.34.parts_ref = bf16[16,48,128]{2,1,0:T(8,128)(2,1)S(1)} all-to-all(bf16[16,48,128]{2,1,0:T(8,128)(2,1)S(1)} %shard_map.189), channel_id=1, replica_groups=mesh['ep_0'=16,'ep_1'=2,'tp_0'=4,'tp_1'=4] {'tp_0','tp_1'}, dimensions={0} | all-to-all | bytes 393216 | tf_op jit(solution)/shard_map/all_to_all | solution.py:297
  95.6 0.2 shard_map.190
  95.8 17.8 %all_to_all.35.returned_ref = bf16[32,4,128]{2,1,0:T(4,128)(2,1)S(1)} all-to-all(bf16[32,4,128]{2,1,0:T(4,128)(2,1)S(1)} %shard_map.190), channel_id=1, replica_groups=mesh['ep_0'=16,'ep_1'=2,'tp_0'=4,'tp_1'=4] {'ep_1','ep_0'}, dimensions={0} | all-to-all | bytes 65536 | tf_op jit(solution)/shard_map/all_to_all | solution.py:297
  113.5 0.8 shard_map.191
  (6 shorter events, 0.0 us)
Async XLA Ops:
  1.5 14.2 %copy-start.3 = (bf16[8,1,64,1024]{3,2,1,0:T(8,128)(2,1)S(1)}, bf16[8,1,64,1024]{3,2,1,0:T(8,128)(2,1)}, u32[]{:S(2)}) copy-start(bf16[8,1,64,1024]{3,2,1,0:T(8,128)(2,1)} %key_ref.1) | copy-start | bytes 3145732
  1.5 14.2 %copy-start.4 = (bf16[8,1,64,1024]{3,2,1,0:T(8,128)(2,1)S(1)}, bf16[8,1,64,1024]{3,2,1,0:T(8,128)(2,1)}, u32[]{:S(2)}) copy-start(bf16[8,1,64,1024]{3,2,1,0:T(8,128)(2,1)} %value_ref.1) | copy-start | bytes 3145732
  1.5 14.2 %copy-start.5 = (bf16[2048,64]{0,1:T(8,128)(2,1)S(1)}, bf16[2048,64]{0,1:T(8,128)(2,1)}, u32[]{:S(2)}) copy-start(bf16[2048,64]{0,1:T(8,128)(2,1)} %param.19) | copy-start | bytes 786436
  1.5 14.2 %copy-start.6 = (bf16[2048,64]{0,1:T(8,128)(2,1)S(1)}, bf16[2048,64]{0,1:T(8,128)(2,1)}, u32[]{:S(2)}) copy-start(bf16[2048,64]{0,1:T(8,128)(2,1)} %param.20) | copy-start | bytes 786436
  1.5 14.2 %copy-start.7 = (bf16[2048,64]{0,1:T(8,128)(2,1)S(1)}, bf16[2048,64]{0,1:T(8,128)(2,1)}, u32[]{:S(2)}) copy-start(bf16[2048,64]{0,1:T(8,128)(2,1)} %param.21) | copy-start | bytes 786436
  1.5 14.2 %copy-start.8 = (bf16[64,2048]{1,0:T(8,128)(2,1)S(1)}, bf16[64,2048]{1,0:T(8,128)(2,1)}, u32[]{:S(2)}) copy-start(bf16[64,2048]{1,0:T(8,128)(2,1)} %wout_ref.1) | copy-start | bytes 786436
  1.5 14.2 %copy-start.9 = (f32[8,1,1024]{2,1,0:T(1,128)S(1)}, f32[8,1,1024]{2,1,0:T(1,128)}, u32[]{:S(2)}) copy-start(f32[8,1,1024]{2,1,0:T(1,128)} %bias_ref.1) | copy-start | bytes 98308
  18.2 66.7 %collective-permute-start = (bf16[6144,128]{1,0:T(8,128)(2,1)S(1)}, bf16[6144,128]{1,0:T(8,128)(2,1)S(1)}, u32[]{:S(2)}, u32[]{:S(2)}) collective-permute-start(bf16[6144,128]{1,0:T(8,128)(2,1)S(1)} %get-tuple-element.27), channel_id=1, source_target_pairs={{0,1},{1,0},{2,3},{3,2},{4,5},{5,4},{6,7},{7,6},{8,9},{9,8},{10,11... | collective-permute-start | bytes 4718600 | tf_op jit(solution)/shard_map/ppermute | solution.py:370
  72.3 12.6 %copy-start = (bf16[1,2048,128]{2,1,0:T(8,128)(2,1)S(1)}, bf16[1,2048,128]{2,1,0:T(8,128)(2,1)}, u32[]{:S(2)}) copy-start(bf16[1,2048,128]{2,1,0:T(8,128)(2,1)} %refs_0_.3) | copy-start | bytes 1572868
  72.3 12.6 %copy-start.1 = (bf16[1,2048,128]{2,1,0:T(8,128)(2,1)S(1)}, bf16[1,2048,128]{2,1,0:T(8,128)(2,1)}, u32[]{:S(2)}) copy-start(bf16[1,2048,128]{2,1,0:T(8,128)(2,1)} %refs_1_.1) | copy-start | bytes 1572868
  72.3 12.6 %copy-start.2 = (bf16[1,128,2048]{2,1,0:T(8,128)(2,1)S(1)}, bf16[1,128,2048]{2,1,0:T(8,128)(2,1)}, u32[]{:S(2)}) copy-start(bf16[1,128,2048]{2,1,0:T(8,128)(2,1)} %refs_2_.1) | copy-start | bytes 1572868
  72.3 12.6 %copy-start.10 = (f32[2048]{0:T(1024)S(1)}, f32[2048]{0:T(1024)}, u32[]{:S(2)}) copy-start(f32[2048]{0:T(1024)} %param.28) | copy-start | bytes 24580

commit v8 on v6

--- a/solution.py
+++ b/solution.py
@@ -47,9 +47,14 @@
     return hits, named & (rank == slot % SLOTS)
 
 
+def keys_kernel(normed_ref, wk_ref, wv_ref, new_key_ref, new_value_ref):
+    new_key_ref[...] = project(normed_ref[...], wk_ref)
+    new_value_ref[...] = project(normed_ref[...], wv_ref)
+
+
 def attend_kernel(parts_ref, lengths_ref, gain_ref, mix_ref, experts_ref, share_ref, wq_ref,
-                  wk_ref, wv_ref, key_ref, value_ref, bias_ref, wout_ref, new_key_ref,
-                  new_value_ref, out_ref, placed_ref, high_ref, low_ref, fresh_ref, sems):
+                  key_ref, value_ref, bias_ref, wout_ref, normed_ref, out_ref, placed_ref,
+                  high_ref, low_ref):
     blocks, rows, lanes = parts_ref.shape
     heads = key_ref.shape[2]
     cache = key_ref.shape[3]
@@ -64,14 +69,7 @@
         axis=1,
     )
     query = project(normed, wq_ref).astype(jnp.float32)
-    fresh_ref[0] = project(normed, wk_ref)
-    fresh_ref[1] = project(normed, wv_ref)
-    stores = [
-        pltpu.make_async_copy(fresh_ref.at[i], new_ref, sems.at[i])
-        for i, new_ref in enumerate((new_key_ref, new_value_ref))
-    ]
-    for store in stores:
-        store.start()
+    normed_ref[...] = normed
     spread = jnp.concatenate([query] * rows, axis=1)
     row = lax.broadcasted_iota(jnp.int32, spread.shape, 0)
     own = lax.broadcasted_iota(jnp.int32, spread.shape, 1) // heads == row
@@ -138,8 +136,6 @@
     placed_ref[...] = placed.astype(jnp.bfloat16)
     high_ref[...] = high
     low_ref[...] = (weight - high.astype(jnp.float32)).astype(jnp.bfloat16)
-    for store in stores:
-        store.wait()
 
 
 def load_kernel(*refs):
@@ -159,6 +155,16 @@
     row = row_ref[...]
     for t in range(out_ref.shape[0]):
         out_ref[t] = row
+
+
+def join_kernel(gate_ref, up_ref, down_ref, after_ref, out_ref):
+    lanes = out_ref.shape[1]
+    width = gate_ref.shape[1]
+    out_ref[:width] = gate_ref[0]
+    out_ref[width : 2 * width] = up_ref[0]
+    down = down_ref[0]
+    for start in range(0, width, lanes):
+        out_ref[2 * width + start : 2 * width + start + lanes] = down[:, start : start + lanes]
 
 
 def middle_kernel(parts_ref, resid_ref, placed_ref, middle_ref, out_ref):
@@ -237,7 +243,7 @@
 
 
 def expert_kernel(rows_ref, gain_ref, *refs):
-    gates, ups, downs, out_ref = refs[0:2], refs[2:4], refs[4:6], refs[6]
+    both, out_ref = refs[:2], refs[2]
     blocks, rows, lanes = rows_ref.shape
     total = jnp.zeros((rows, lanes), jnp.float32)
     scaled = []
@@ -247,14 +253,19 @@
         scaled.append((x * gain_ref[t : t + 1, :]).astype(jnp.bfloat16))
     scaled = jnp.concatenate(scaled, axis=1)
     scale = lax.rsqrt(jnp.sum(total, axis=1, keepdims=True) / (blocks * lanes) + eps)
-    gate = jnp.concatenate([ref[0] for ref in gates], axis=1)
+    width = blocks * lanes
+    gate = jnp.concatenate([ref[:width] for ref in both], axis=1)
     gate = jnp.dot(scaled, gate, preferred_element_type=jnp.float32) * scale
-    upper = jnp.concatenate([ref[0] for ref in ups], axis=1)
+    upper = jnp.concatenate([ref[width : 2 * width] for ref in both], axis=1)
     upper = jnp.dot(scaled, upper, preferred_element_type=jnp.float32) * scale
     gate = jnp.minimum(gate, limit)
     upper = jnp.clip(upper, -limit, limit)
     active = ((upper + 1.0) * gate * jax.nn.sigmoid(alpha * gate)).astype(jnp.bfloat16)
-    down = jnp.concatenate([ref[0] for ref in downs], axis=0)
+    columns = [
+        jnp.concatenate([ref[start : start + lanes] for ref in both], axis=0)
+        for start in range(2 * width, 3 * width, lanes)
+    ]
+    down = jnp.concatenate(columns, axis=1)
     result = jnp.dot(active, down, preferred_element_type=jnp.float32).astype(jnp.bfloat16)
     for t in range(blocks):
         out_ref[t] = result[:, t * lanes : (t + 1) * lanes]
@@ -327,41 +338,49 @@
         scratch=[pltpu.SemaphoreType.DMA((len(small),))],
     )
     copies = local(copies_kernel, shape((blocks, rows, lanes), bf16), near, flops=LONG)
-    weights = []
-    pairs = [(i, i ^ PAIRS[i // blocks]) for i in range(CORES * blocks)]
-    for weight in (w_gate, w_up, w_down):
-        weights += [weight, lax.ppermute(weight, (EP[0], *TP), pairs)]
-    new_keys, new_values, partial_branch, placed, high, low = local(
+    normed, partial_branch, placed, high, low = local(
         attend_kernel,
-        [new, new, shape((blocks, 2 * rows, lanes), bf16)] + [shape((slots, rows), bf16)] * 3,
+        [shape((rows, blocks * lanes), bf16), shape((blocks, 2 * rows, lanes), bf16)]
+        + [shape((slots, rows), bf16)] * 3,
         exchange(copies, TP),
         *small,
         w_query.T,
-        w_key.T,
-        w_value.T,
         key_cache,
         value_cache,
         key_bias,
         w_out,
-        far_out=2,
-        scratch=[pltpu.VMEM((2, rows, heads), bf16), pltpu.SemaphoreType.DMA((2,))],
-    )
+    )
+    new_keys, new_values = local(keys_kernel, [new, new], normed, w_key.T, w_value.T, flops=SHORT)
+    pairs = [(i, i ^ PAIRS[i // blocks]) for i in range(CORES * blocks)]
+    branch = exchange(partial_branch, TP)
+    joined = local(
+        join_kernel,
+        shape((3 * blocks * lanes, lanes), bf16),
+        w_gate,
+        w_up,
+        w_down,
+        low,
+        flops=SHORT,
+    )
+    swapped = lax.ppermute(joined, (EP[0], *TP), pairs)
     middle, outgoing = local(
         middle_kernel,
         [shape((rows, lanes), jnp.float32), shape((groups, SLOTS, lanes), bf16)],
-        exchange(partial_branch, TP),
+        branch,
         near,
         placed,
         flops=SHORT,
     )
-    arrived = exchange(outgoing, EP)
-    held = local(spread_kernel, shape((blocks, items // 2, lanes), bf16), arrived, flops=SHORT)
+    held = local(
+        spread_kernel, shape((blocks, items // 2, lanes), bf16), exchange(outgoing, EP), flops=SHORT
+    )
     partial_out = local(
         expert_kernel,
         shape((blocks, items // 2, lanes), bf16),
         exchange(held, TP),
         ffn_gain.reshape(blocks, lanes),
-        *weights,
+        joined,
+        swapped,
     )
     result = local(
         total_kernel, shape((groups, SLOTS, lanes), bf16), exchange(partial_out, TP), flops=SHORT

time: 105 us -> 115 us (1.095)
  waiting for transfers between devices: 0.01 us -> 11.6 us
  starting transfers between devices: 12 us -> 8.37 us
  blocking collectives: 86.3 us -> 87.9 us
    all_to_all x1, waiting for transfers between devices: 0.01 us -> 11.6 us  [exchange(): return lax.all_to_all(x, axis, 0, 0, tiled=True)]
    ppermute x3 -> x1, starting transfers between devices: 8.45 us -> 2.19 us  [layer(): swapped = lax.ppermute(joined, (EP[0], *TP), pairs)]
    all_to_all x1, starting transfers between devices: 3.5 us -> 6.18 us  [exchange(): return lax.all_to_all(x, axis, 0, 0, tiled=True)]
    all_to_all x5, blocking collectives: 86.3 us -> 87.9 us  [exchange(): return lax.all_to_all(x, axis, 0, 0, tiled=True)]
    pallas_call x8 -> x10, Pallas kernels: 5.04 us -> 5.94 us  [local(): pl.pallas_call(kernel, in_specs=places(len(args), far_in), out_specs=outs...]
  transfers between devices with their start and end apart: 4 -> 2, of which waited for: 0 -> 1; matrix products, arithmetic and copies ran while one was open for 0% -> 0% of each run, Pallas kernels for 0% -> 1%
where the time goes in v8:
time: 115 us
  blocking collectives  87.9 us (76%)
  waiting for transfers between devices  11.6 us (10%)
  starting transfers between devices  8.37 us (7%)
  Pallas kernels  5.94 us (5%)
    all_to_all x5, blocking collectives, exchange(): return lax.all_to_all(x, axis, 0, 0, tiled=True)  87.9 us
    all_to_all x1, waiting for transfers between devices, exchange(): return lax.all_to_all(x, axis, 0, 0, tiled=True)  11.6 us
    all_to_all x1, starting transfers between devices, exchange(): return lax.all_to_all(x, axis, 0, 0, tiled=True)  6.18 us
    pallas_call x10, Pallas kernels, local(): pl.pallas_call(kernel, in_specs=places(len(args), far_in), out_specs=outs...  5.94 us
  transfers between devices with their start and end apart: 2, of which 1 were waited for; matrix products, arithmetic and copies ran while one was open for 0% of the time, Pallas kernels for 1%

profile of v8, /device:TPU:1, one launch (start us, length us, event | category | flops | bytes accessed | tf_op | source)
XLA Modules:
  0.0 114.7 jit_solution(15959323481549140860)
XLA Ops:
  0.6 0.8 shard_map.184
  1.5 0.0 copy-start
  1.5 0.0 copy-start.1
  1.5 0.0 copy-start.2
  1.5 0.0 copy-start.3
  1.5 0.0 copy-start.4
  1.5 0.0 copy-start.6
  1.5 0.0 copy-start.7
  1.6 0.0 copy-start.8
  1.6 14.1 %all_to_all.30.parts_ref = bf16[16,8,128]{2,1,0:T(8,128)(2,1)S(1)} all-to-all(bf16[16,8,128]{2,1,0:T(8,128)(2,1)S(1)} %shard_map.185), channel_id=1, replica_groups=mesh['ep_0'=16,'ep_1'=2,'tp_0'=4,'tp_1'=4] {'tp_0','tp_1'}, dimensions={0} | all-to-all | bytes 65536 | tf_op jit(solution)/shard_map/all_to_all | solution.py:294
  15.7 0.0 copy-done
  15.7 0.0 copy-done.1
  15.7 0.0 copy-done.2
  15.7 0.0 copy-done.3
  15.7 0.0 copy-done.4
  15.7 1.4 %shard_map.186 = (bf16[8,2048]{1,0:T(8,128)(2,1)S(1)}, bf16[16,16,128]{2,1,0:T(8,128)(2,1)S(1)}, bf16[128,8]{1,0:T(8,128)(2,1)S(1)}, bf16[128,8]{1,0:T(8,128)(2,1)S(1)}, bf16[128,8]{1,0:T(8,128)(2,1)S(1)}) custom-call(bf16[16,8,128]{2,1,0:T(8,128)(2,1)S(1)} %all_to_all.30.parts_ref, s32[1,8]{1,0:T(1,128)S(1)} %get-tuple-element.19.lengths_ref, ...), custom_call_target="tpu_custom_call" | custom-call | tf_op jit(solution)/shard_map/pallas_call | solution.py:282
  17.1 0.0 copy-done.6
  17.1 0.1 shard_map.189.refs_0_
  17.3 2.2 %collective-permute-start = (bf16[6144,128]{1,0:T(8,128)(2,1)S(1)}, bf16[6144,128]{1,0:T(8,128)(2,1)S(1)}, u32[]{:S(2)}, u32[]{:S(2)}) collective-permute-start(bf16[6144,128]{1,0:T(8,128)(2,1)S(1)} %shard_map.189.refs_0_), channel_id=1, source_target_pairs={{0,1},{1,0},{2,3},{3,2},{4,5},{5,4},{6,7},{7,6},{8,9},{9,8},{10,11... | collective-permute-start | bytes 4718600 | tf_op jit(solution)/shard_map/ppermute | solution.py:365
  19.5 20.1 %all_to_all.31.parts_ref = bf16[16,16,128]{2,1,0:T(8,128)(2,1)S(1)} all-to-all(bf16[16,16,128]{2,1,0:T(8,128)(2,1)S(1)} %get-tuple-element.24), channel_id=1, replica_groups=mesh['ep_0'=16,'ep_1'=2,'tp_0'=4,'tp_1'=4] {'tp_0','tp_1'}, dimensions={0} | all-to-all | bytes 131072 | tf_op jit(solution)/shard_map/all_to_all | solution.py:294
  39.6 0.3 shard_map.187
  39.9 31.6 %all_to_all.32.arrived_ref = bf16[32,4,128]{2,1,0:T(4,128)(2,1)S(1)} all-to-all(bf16[32,4,128]{2,1,0:T(4,128)(2,1)S(1)} %get-tuple-element.26), channel_id=1, replica_groups=mesh['ep_0'=16,'ep_1'=2,'tp_0'=4,'tp_1'=4] {'ep_1','ep_0'}, dimensions={0} | all-to-all | bytes 65536 | tf_op jit(solution)/shard_map/all_to_all | solution.py:294
  71.4 0.2 shard_map.188
  71.6 12.3 %all_to_all.33.rows_ref = bf16[16,48,128]{2,1,0:T(8,128)(2,1)S(1)} all-to-all(bf16[16,48,128]{2,1,0:T(8,128)(2,1)S(1)} %shard_map.188), channel_id=1, replica_groups=mesh['ep_0'=16,'ep_1'=2,'tp_0'=4,'tp_1'=4] {'tp_0','tp_1'}, dimensions={0} | all-to-all | bytes 393216 | tf_op jit(solution)/shard_map/all_to_all | solution.py:294
  83.8 0.0 collective-permute-done.refs_1_
  83.8 0.7 shard_map.190
  84.6 9.9 %all_to_all.34.parts_ref = bf16[16,48,128]{2,1,0:T(8,128)(2,1)S(1)} all-to-all(bf16[16,48,128]{2,1,0:T(8,128)(2,1)S(1)} %shard_map.190), channel_id=1, replica_groups=mesh['ep_0'=16,'ep_1'=2,'tp_0'=4,'tp_1'=4] {'tp_0','tp_1'}, dimensions={0} | all-to-all | bytes 393216 | tf_op jit(solution)/shard_map/all_to_all | solution.py:294
  94.5 0.8 shard_map.191
  95.3 6.2 %all-to-all-start.5 = ((bf16[32,4,128]{2,1,0:T(4,128)(2,1)}), bf16[32,4,128]{2,1,0:T(4,128)(2,1)S(1)}, u32[]{:S(2)}, u32[]{:S(2)}) async-start(bf16[32,4,128]{2,1,0:T(4,128)(2,1)} %shard_map.191), calls=%async_computation.5 | async-start | bytes 65536 | tf_op jit(solution)/shard_map/all_to_all | solution.py:294
  101.5 0.8 shard_map.193
  102.3 11.6 %all-to-all-done.5.returned_ref = bf16[32,4,128]{2,1,0:T(4,128)(2,1)S(1)} async-done(((bf16[32,4,128]{2,1,0:T(4,128)(2,1)}), bf16[32,4,128]{2,1,0:T(4,128)(2,1)S(1)}, u32[]{:S(2)}, u32[]{:S(2)}) %all-to-all-start.5) | async-done | bytes 32800 | tf_op jit(solution)/shard_map/all_to_all | solution.py:294
  113.9 0.7 shard_map.192
  (9 shorter events, 0.0 us)
Async XLA Ops:
  1.5 14.2 %copy-start = (bf16[8,1,64,1024]{3,2,1,0:T(8,128)(2,1)S(1)}, bf16[8,1,64,1024]{3,2,1,0:T(8,128)(2,1)}, u32[]{:S(2)}) copy-start(bf16[8,1,64,1024]{3,2,1,0:T(8,128)(2,1)} %key_ref.1) | copy-start | bytes 3145732
  1.5 14.2 %copy-start.1 = (bf16[8,1,64,1024]{3,2,1,0:T(8,128)(2,1)S(1)}, bf16[8,1,64,1024]{3,2,1,0:T(8,128)(2,1)}, u32[]{:S(2)}) copy-start(bf16[8,1,64,1024]{3,2,1,0:T(8,128)(2,1)} %value_ref.1) | copy-start | bytes 3145732
  1.5 14.2 %copy-start.2 = (bf16[2048,64]{0,1:T(8,128)(2,1)S(1)}, bf16[2048,64]{0,1:T(8,128)(2,1)}, u32[]{:S(2)}) copy-start(bf16[2048,64]{0,1:T(8,128)(2,1)} %param.19) | copy-start | bytes 786436
  1.5 14.2 %copy-start.3 = (bf16[64,2048]{1,0:T(8,128)(2,1)S(1)}, bf16[64,2048]{1,0:T(8,128)(2,1)}, u32[]{:S(2)}) copy-start(bf16[64,2048]{1,0:T(8,128)(2,1)} %wout_ref.1) | copy-start | bytes 786436
  1.5 14.2 %copy-start.4 = (f32[8,1,1024]{2,1,0:T(1,128)S(1)}, f32[8,1,1024]{2,1,0:T(1,128)}, u32[]{:S(2)}) copy-start(f32[8,1,1024]{2,1,0:T(1,128)} %bias_ref.1) | copy-start | bytes 98308
  1.5 15.6 %copy-start.6 = (bf16[1,2048,128]{2,1,0:T(8,128)(2,1)S(1)}, bf16[1,2048,128]{2,1,0:T(8,128)(2,1)}, u32[]{:S(2)}) copy-start(bf16[1,2048,128]{2,1,0:T(8,128)(2,1)} %gate_ref.1) | copy-start | bytes 1572868
  1.5 15.6 %copy-start.7 = (bf16[1,2048,128]{2,1,0:T(8,128)(2,1)S(1)}, bf16[1,2048,128]{2,1,0:T(8,128)(2,1)}, u32[]{:S(2)}) copy-start(bf16[1,2048,128]{2,1,0:T(8,128)(2,1)} %up_ref.1) | copy-start | bytes 1572868
  1.6 15.6 %copy-start.8 = (bf16[1,128,2048]{2,1,0:T(8,128)(2,1)S(1)}, bf16[1,128,2048]{2,1,0:T(8,128)(2,1)}, u32[]{:S(2)}) copy-start(bf16[1,128,2048]{2,1,0:T(8,128)(2,1)} %down_ref.1) | copy-start | bytes 1572868
  17.3 66.6 %collective-permute-start = (bf16[6144,128]{1,0:T(8,128)(2,1)S(1)}, bf16[6144,128]{1,0:T(8,128)(2,1)S(1)}, u32[]{:S(2)}, u32[]{:S(2)}) collective-permute-start(bf16[6144,128]{1,0:T(8,128)(2,1)S(1)} %shard_map.189.refs_0_), channel_id=1, source_target_pairs={{0,1},{1,0},{2,3},{3,2},{4,5},{5,4},{6,7},{7,6},{8,9},{9,8},{10,11... | collective-permute-start | bytes 4718600 | tf_op jit(solution)/shard_map/ppermute | solution.py:365
  71.4 12.4 %copy-start.5 = (f32[2048]{0:T(1024)S(1)}, f32[2048]{0:T(1024)}, u32[]{:S(2)}) copy-start(f32[2048]{0:T(1024)} %param.28) | copy-start | bytes 24580
  94.5 7.0 %copy-start.9 = (bf16[2048,64]{0,1:T(8,128)(2,1)S(1)}, bf16[2048,64]{0,1:T(8,128)(2,1)}, u32[]{:S(2)}) copy-start(bf16[2048,64]{0,1:T(8,128)(2,1)} %param.20) | copy-start | bytes 786436
  94.5 7.0 %copy-start.10 = (bf16[2048,64]{0,1:T(8,128)(2,1)S(1)}, bf16[2048,64]{0,1:T(8,128)(2,1)}, u32[]{:S(2)}) copy-start(bf16[2048,64]{0,1:T(8,128)(2,1)} %param.21) | copy-start | bytes 786436
  95.3 18.6 %all-to-all-start.5 = ((bf16[32,4,128]{2,1,0:T(4,128)(2,1)}), bf16[32,4,128]{2,1,0:T(4,128)(2,1)S(1)}, u32[]{:S(2)}, u32[]{:S(2)}) async-start(bf16[32,4,128]{2,1,0:T(4,128)(2,1)} %shard_map.191), calls=%async_computation.5 | async-start | bytes 65536 | tf_op jit(solution)/shard_map/all_to_all | solution.py:294

commit v9 on v8

--- a/solution.py
+++ b/solution.py
@@ -11,6 +11,7 @@
 EP = ("ep_1", "ep_0")
 CORES = 2
 PAIRS = (1, 4)
+PIECE = 4
 
 eps = 1e-06
 limit = 7.0
@@ -47,14 +48,9 @@
     return hits, named & (rank == slot % SLOTS)
 
 
-def keys_kernel(normed_ref, wk_ref, wv_ref, new_key_ref, new_value_ref):
-    new_key_ref[...] = project(normed_ref[...], wk_ref)
-    new_value_ref[...] = project(normed_ref[...], wv_ref)
-
-
 def attend_kernel(parts_ref, lengths_ref, gain_ref, mix_ref, experts_ref, share_ref, wq_ref,
-                  key_ref, value_ref, bias_ref, wout_ref, normed_ref, out_ref, placed_ref,
-                  high_ref, low_ref):
+                  wk_ref, wv_ref, key_ref, value_ref, bias_ref, wout_ref, new_key_ref,
+                  new_value_ref, out_ref, placed_ref, high_ref, low_ref, fresh_ref, stage_ref, sems):
     blocks, rows, lanes = parts_ref.shape
     heads = key_ref.shape[2]
     cache = key_ref.shape[3]
@@ -69,7 +65,14 @@
         axis=1,
     )
     query = project(normed, wq_ref).astype(jnp.float32)
-    normed_ref[...] = normed
+    fresh_ref[0] = project(normed, wk_ref)
+    fresh_ref[1] = project(normed, wv_ref)
+    stores = [
+        pltpu.make_async_copy(fresh_ref.at[i], new_ref, sems.at[i])
+        for i, new_ref in enumerate((new_key_ref, new_value_ref))
+    ]
+    for store in stores:
+        store.start()
     spread = jnp.concatenate([query] * rows, axis=1)
     row = lax.broadcasted_iota(jnp.int32, spread.shape, 0)
     own = lax.broadcasted_iota(jnp.int32, spread.shape, 1) // heads == row
@@ -118,13 +121,26 @@
     square = jnp.sum(folded * folded, axis=1, keepdims=True)
     attended = folded[:, :heads] + folded[:, heads : 2 * heads]
     ready = (attended * mix_ref[...]).astype(jnp.bfloat16)
-    branch = jnp.dot(ready, wout_ref[...], preferred_element_type=jnp.float32)
     top = square.astype(jnp.bfloat16).astype(jnp.float32)
     half = lax.broadcasted_iota(jnp.int32, (rows, lanes), 1) < lanes // 2
     tail = jnp.where(half, top, square - top)
-    for t in range(blocks):
-        both = jnp.concatenate([branch[:, t * lanes : (t + 1) * lanes], tail], axis=0)
-        out_ref[t] = both.astype(jnp.bfloat16)
+    tail = tail.astype(jnp.bfloat16)
+    for t in range(blocks):
+        stage_ref[t, rows:] = tail
+
+    def send(first, last, low, high):
+        store = pltpu.make_async_copy(
+            stage_ref.at[first:last, low:high], out_ref.at[first:last, low:high], sems.at[len(stores)]
+        )
+        store.start()
+        stores.append(store)
+
+    send(0, blocks, rows, 2 * rows)
+    branch = jnp.dot(ready, wout_ref[...], preferred_element_type=jnp.float32)
+    for t in range(blocks):
+        stage_ref[t, :rows] = branch[:, t * lanes : (t + 1) * lanes].astype(jnp.bfloat16)
+        if t % PIECE == PIECE - 1:
+            send(t + 1 - PIECE, t + 1, 0, rows)
     hits, placed = chosen_slots(experts_ref, placed_ref.shape[0])
     share = share_ref[...]
     share = share / jnp.sum(share, axis=0, keepdims=True)
@@ -136,6 +152,8 @@
     placed_ref[...] = placed.astype(jnp.bfloat16)
     high_ref[...] = high
     low_ref[...] = (weight - high.astype(jnp.float32)).astype(jnp.bfloat16)
+    for store in stores:
+        store.wait()
 
 
 def load_kernel(*refs):
@@ -338,19 +356,25 @@
         scratch=[pltpu.SemaphoreType.DMA((len(small),))],
     )
     copies = local(copies_kernel, shape((blocks, rows, lanes), bf16), near, flops=LONG)
-    normed, partial_branch, placed, high, low = local(
+    new_keys, new_values, partial_branch, placed, high, low = local(
         attend_kernel,
-        [shape((rows, blocks * lanes), bf16), shape((blocks, 2 * rows, lanes), bf16)]
-        + [shape((slots, rows), bf16)] * 3,
+        [new, new, shape((blocks, 2 * rows, lanes), bf16)] + [shape((slots, rows), bf16)] * 3,
         exchange(copies, TP),
         *small,
         w_query.T,
+        w_key.T,
+        w_value.T,
         key_cache,
         value_cache,
         key_bias,
         w_out,
-    )
-    new_keys, new_values = local(keys_kernel, [new, new], normed, w_key.T, w_value.T, flops=SHORT)
+        far_out=3,
+        scratch=[
+            pltpu.VMEM((2, rows, heads), bf16),
+            pltpu.VMEM((blocks, 2 * rows, lanes), bf16),
+            pltpu.SemaphoreType.DMA((3 + blocks // PIECE,)),
+        ],
+    )
     pairs = [(i, i ^ PAIRS[i // blocks]) for i in range(CORES * blocks)]
     branch = exchange(partial_branch, TP)
     joined = local(

time: 115 us -> 114 us (level)
  blocking collectives: 87.9 us -> 106 us
  waiting for transfers between devices: 11.6 us -> 0.01 us
  starting transfers between devices: 8.37 us -> 2.19 us
    all_to_all x5 -> x6, blocking collectives: 87.9 us -> 106 us  [exchange(): return lax.all_to_all(x, axis, 0, 0, tiled=True)]
    all_to_all x1 -> x0, waiting for transfers between devices: 11.6 us -> none  [exchange(): return lax.all_to_all(x, axis, 0, 0, tiled=True)]
    all_to_all x1 -> x0, starting transfers between devices: 6.18 us -> none  [exchange(): return lax.all_to_all(x, axis, 0, 0, tiled=True)]
    pallas_call x10 -> x9, Pallas kernels: 5.94 us -> 4.82 us  [local(): pl.pallas_call(kernel, in_specs=places(len(args), far_in), out_specs=outs...]
  transfers between devices with their start and end apart: 2 -> 1, of which waited for: 1 -> 0; matrix products, arithmetic and copies ran while one was open for 0% -> 0% of each run, Pallas kernels for 1% -> 0%
where the time goes in v9:
time: 114 us
  blocking collectives  106 us (93%)
  Pallas kernels  4.82 us (4%)
  starting transfers between devices  2.19 us (2%)
    all_to_all x6, blocking collectives, exchange(): return lax.all_to_all(x, axis, 0, 0, tiled=True)  106 us
    pallas_call x9, Pallas kernels, local(): pl.pallas_call(kernel, in_specs=places(len(args), far_in), out_specs=outs...  4.82 us
  transfers between devices with their start and end apart: 1, of which 0 were waited for; matrix products, arithmetic and copies ran while one was open for 0% of the time, Pallas kernels for 0%

profile of v9, /device:TPU:1, one launch (start us, length us, event | category | flops | bytes accessed | tf_op | source)
XLA Modules:
  0.0 113.6 jit_solution(7801040019479035203)
XLA Ops:
  0.6 0.8 shard_map.184
  1.5 0.0 copy-start
  1.5 0.0 copy-start.1
  1.5 0.0 copy-start.2
  1.5 0.0 copy-start.3
  1.5 0.0 copy-start.4
  1.5 0.0 copy-start.5
  1.5 0.0 copy-start.6
  1.6 14.1 %all_to_all.30.parts_ref = bf16[16,8,128]{2,1,0:T(8,128)(2,1)S(1)} all-to-all(bf16[16,8,128]{2,1,0:T(8,128)(2,1)S(1)} %shard_map.185), channel_id=1, replica_groups=mesh['ep_0'=16,'ep_1'=2,'tp_0'=4,'tp_1'=4] {'tp_0','tp_1'}, dimensions={0} | all-to-all | bytes 65536 | tf_op jit(solution)/shard_map/all_to_all | solution.py:312
  15.6 0.0 copy-done
  15.6 0.0 copy-done.1
  15.6 0.0 copy-done.2
  15.7 0.0 copy-done.3
  15.7 0.0 copy-done.4
  15.7 0.0 copy-done.5
  15.7 0.0 copy-start.8
  15.7 0.0 copy-start.9
  15.7 0.0 copy-start.10
  15.7 1.7 %shard_map.186 = (bf16[8,64]{1,0:T(8,128)(2,1)}, bf16[8,64]{1,0:T(8,128)(2,1)}, bf16[16,16,128]{2,1,0:T(8,128)(2,1)S(1)}, bf16[128,8]{1,0:T(8,128)(2,1)S(1)}, bf...) custom-call(bf16[16,8,128]{2,1,0:T(8,128)(2,1)S(1)} %all_to_all.30.parts_ref, ...), custom_call_target="tpu_custom_call" | custom-call | tf_op jit(solution)/shard_map/pallas_call | solution.py:300
  17.5 0.1 shard_map.189.refs_0_
  17.7 2.2 %collective-permute-start = (bf16[6144,128]{1,0:T(8,128)(2,1)S(1)}, bf16[6144,128]{1,0:T(8,128)(2,1)S(1)}, u32[]{:S(2)}, u32[]{:S(2)}) collective-permute-start(bf16[6144,128]{1,0:T(8,128)(2,1)S(1)} %shard_map.189.refs_0_), channel_id=1, source_target_pairs={{0,1},{1,0},{2,3},{3,2},{4,5},{5,4},{6,7},{7,6},{8,9},{9,8},{10,11... | collective-permute-start | bytes 4718600 | tf_op jit(solution)/shard_map/ppermute | solution.py:389
  19.9 20.1 %all_to_all.31.parts_ref = bf16[16,16,128]{2,1,0:T(8,128)(2,1)S(1)} all-to-all(bf16[16,16,128]{2,1,0:T(8,128)(2,1)S(1)} %get-tuple-element.23), channel_id=1, replica_groups=mesh['ep_0'=16,'ep_1'=2,'tp_0'=4,'tp_1'=4] {'tp_0','tp_1'}, dimensions={0} | all-to-all | bytes 131072 | tf_op jit(solution)/shard_map/all_to_all | solution.py:312
  39.9 0.3 shard_map.187
  40.2 31.6 %all_to_all.32.arrived_ref = bf16[32,4,128]{2,1,0:T(4,128)(2,1)S(1)} all-to-all(bf16[32,4,128]{2,1,0:T(4,128)(2,1)S(1)} %get-tuple-element.25), channel_id=1, replica_groups=mesh['ep_0'=16,'ep_1'=2,'tp_0'=4,'tp_1'=4] {'ep_1','ep_0'}, dimensions={0} | all-to-all | bytes 65536 | tf_op jit(solution)/shard_map/all_to_all | solution.py:312
  71.8 0.2 shard_map.188
  72.0 12.3 %all_to_all.33.rows_ref = bf16[16,48,128]{2,1,0:T(8,128)(2,1)S(1)} all-to-all(bf16[16,48,128]{2,1,0:T(8,128)(2,1)S(1)} %shard_map.188), channel_id=1, replica_groups=mesh['ep_0'=16,'ep_1'=2,'tp_0'=4,'tp_1'=4] {'tp_0','tp_1'}, dimensions={0} | all-to-all | bytes 393216 | tf_op jit(solution)/shard_map/all_to_all | solution.py:312
  84.2 0.0 collective-permute-done.refs_1_
  84.2 0.7 shard_map.190
  84.9 9.9 %all_to_all.34.parts_ref = bf16[16,48,128]{2,1,0:T(8,128)(2,1)S(1)} all-to-all(bf16[16,48,128]{2,1,0:T(8,128)(2,1)S(1)} %shard_map.190), channel_id=1, replica_groups=mesh['ep_0'=16,'ep_1'=2,'tp_0'=4,'tp_1'=4] {'tp_0','tp_1'}, dimensions={0} | all-to-all | bytes 393216 | tf_op jit(solution)/shard_map/all_to_all | solution.py:312
  94.8 0.2 shard_map.191
  95.1 17.8 %all_to_all.35.returned_ref = bf16[32,4,128]{2,1,0:T(4,128)(2,1)S(1)} all-to-all(bf16[32,4,128]{2,1,0:T(4,128)(2,1)S(1)} %shard_map.191), channel_id=1, replica_groups=mesh['ep_0'=16,'ep_1'=2,'tp_0'=4,'tp_1'=4] {'ep_1','ep_0'}, dimensions={0} | all-to-all | bytes 65536 | tf_op jit(solution)/shard_map/all_to_all | solution.py:312
  112.8 0.8 shard_map.192
  (7 shorter events, 0.0 us)
Async XLA Ops:
  1.5 14.2 %copy-start = (bf16[8,1,64,1024]{3,2,1,0:T(8,128)(2,1)S(1)}, bf16[8,1,64,1024]{3,2,1,0:T(8,128)(2,1)}, u32[]{:S(2)}) copy-start(bf16[8,1,64,1024]{3,2,1,0:T(8,128)(2,1)} %key_ref.1) | copy-start | bytes 3145732
  1.5 14.2 %copy-start.1 = (bf16[8,1,64,1024]{3,2,1,0:T(8,128)(2,1)S(1)}, bf16[8,1,64,1024]{3,2,1,0:T(8,128)(2,1)}, u32[]{:S(2)}) copy-start(bf16[8,1,64,1024]{3,2,1,0:T(8,128)(2,1)} %value_ref.1) | copy-start | bytes 3145732
  1.5 14.2 %copy-start.2 = (bf16[2048,64]{0,1:T(8,128)(2,1)S(1)}, bf16[2048,64]{0,1:T(8,128)(2,1)}, u32[]{:S(2)}) copy-start(bf16[2048,64]{0,1:T(8,128)(2,1)} %param.19) | copy-start | bytes 786436
  1.5 14.2 %copy-start.3 = (bf16[2048,64]{0,1:T(8,128)(2,1)S(1)}, bf16[2048,64]{0,1:T(8,128)(2,1)}, u32[]{:S(2)}) copy-start(bf16[2048,64]{0,1:T(8,128)(2,1)} %param.20) | copy-start | bytes 786436
  1.5 14.2 %copy-start.4 = (bf16[2048,64]{0,1:T(8,128)(2,1)S(1)}, bf16[2048,64]{0,1:T(8,128)(2,1)}, u32[]{:S(2)}) copy-start(bf16[2048,64]{0,1:T(8,128)(2,1)} %param.21) | copy-start | bytes 786436
  1.5 14.2 %copy-start.5 = (bf16[64,2048]{1,0:T(8,128)(2,1)S(1)}, bf16[64,2048]{1,0:T(8,128)(2,1)}, u32[]{:S(2)}) copy-start(bf16[64,2048]{1,0:T(8,128)(2,1)} %wout_ref.1) | copy-start | bytes 786436
  1.5 14.2 %copy-start.6 = (f32[8,1,1024]{2,1,0:T(1,128)S(1)}, f32[8,1,1024]{2,1,0:T(1,128)}, u32[]{:S(2)}) copy-start(f32[8,1,1024]{2,1,0:T(1,128)} %bias_ref.1) | copy-start | bytes 98308
  15.7 1.8 %copy-start.8 = (bf16[1,2048,128]{2,1,0:T(8,128)(2,1)S(1)}, bf16[1,2048,128]{2,1,0:T(8,128)(2,1)}, u32[]{:S(2)}) copy-start(bf16[1,2048,128]{2,1,0:T(8,128)(2,1)} %gate_ref.1) | copy-start | bytes 1572868
  15.7 1.8 %copy-start.9 = (bf16[1,2048,128]{2,1,0:T(8,128)(2,1)S(1)}, bf16[1,2048,128]{2,1,0:T(8,128)(2,1)}, u32[]{:S(2)}) copy-start(bf16[1,2048,128]{2,1,0:T(8,128)(2,1)} %up_ref.1) | copy-start | bytes 1572868
  15.7 1.8 %copy-start.10 = (bf16[1,128,2048]{2,1,0:T(8,128)(2,1)S(1)}, bf16[1,128,2048]{2,1,0:T(8,128)(2,1)}, u32[]{:S(2)}) copy-start(bf16[1,128,2048]{2,1,0:T(8,128)(2,1)} %down_ref.1) | copy-start | bytes 1572868
  17.7 66.6 %collective-permute-start = (bf16[6144,128]{1,0:T(8,128)(2,1)S(1)}, bf16[6144,128]{1,0:T(8,128)(2,1)S(1)}, u32[]{:S(2)}, u32[]{:S(2)}) collective-permute-start(bf16[6144,128]{1,0:T(8,128)(2,1)S(1)} %shard_map.189.refs_0_), channel_id=1, source_target_pairs={{0,1},{1,0},{2,3},{3,2},{4,5},{5,4},{6,7},{7,6},{8,9},{9,8},{10,11... | collective-permute-start | bytes 4718600 | tf_op jit(solution)/shard_map/ppermute | solution.py:389
  71.8 12.4 %copy-start.7 = (f32[2048]{0:T(1024)S(1)}, f32[2048]{0:T(1024)}, u32[]{:S(2)}) copy-start(f32[2048]{0:T(1024)} %param.28) | copy-start | bytes 24580

commit v10 on v8

--- a/solution.py
+++ b/solution.py
@@ -47,14 +47,18 @@
     return hits, named & (rank == slot % SLOTS)
 
 
-def keys_kernel(normed_ref, wk_ref, wv_ref, new_key_ref, new_value_ref):
-    new_key_ref[...] = project(normed_ref[...], wk_ref)
-    new_value_ref[...] = project(normed_ref[...], wv_ref)
-
-
-def attend_kernel(parts_ref, lengths_ref, gain_ref, mix_ref, experts_ref, share_ref, wq_ref,
-                  key_ref, value_ref, bias_ref, wout_ref, normed_ref, out_ref, placed_ref,
-                  high_ref, low_ref):
+def attend_kernel(far_key_ref, far_wk_ref, far_wv_ref, far_value_ref, far_wout_ref, parts_ref,
+                  lengths_ref, gain_ref, mix_ref, experts_ref, share_ref, wq_ref, bias_ref,
+                  new_key_ref, new_value_ref, out_ref, placed_ref, high_ref, low_ref, fresh_ref,
+                  key_ref, wk_ref, wv_ref, value_ref, wout_ref, sems):
+    far = (far_key_ref, far_wk_ref, far_wv_ref, far_value_ref, far_wout_ref)
+    near = (key_ref, wk_ref, wv_ref, value_ref, wout_ref)
+    fetches = [
+        pltpu.make_async_copy(source, target, sems.at[2 + i])
+        for i, (source, target) in enumerate(zip(far, near))
+    ]
+    for fetch in fetches:
+        fetch.start()
     blocks, rows, lanes = parts_ref.shape
     heads = key_ref.shape[2]
     cache = key_ref.shape[3]
@@ -69,11 +73,11 @@
         axis=1,
     )
     query = project(normed, wq_ref).astype(jnp.float32)
-    normed_ref[...] = normed
     spread = jnp.concatenate([query] * rows, axis=1)
     row = lax.broadcasted_iota(jnp.int32, spread.shape, 0)
     own = lax.broadcasted_iota(jnp.int32, spread.shape, 1) // heads == row
     spread = jnp.where(own, spread, 0.0).astype(jnp.bfloat16)
+    fetches[0].wait()
     keys = key_ref[:, 0].reshape(rows * heads, cache)
     scores = jnp.dot(spread, keys, preferred_element_type=jnp.float32) * heads ** (-0.5)
     scores = scores + bias_ref[:, 0, :]
@@ -83,6 +87,16 @@
     counts = lengths_ref[...].astype(jnp.float32)
     length = jnp.sum(jnp.where(diagonal, counts, 0.0), axis=1, keepdims=True).astype(jnp.int32)
     live = lax.broadcasted_iota(jnp.int32, (rows, cache), 1) < length
+    fetches[1].wait()
+    fetches[2].wait()
+    fresh_ref[0] = project(normed, wk_ref)
+    fresh_ref[1] = project(normed, wv_ref)
+    stores = [
+        pltpu.make_async_copy(fresh_ref.at[i], new_ref, sems.at[i])
+        for i, new_ref in enumerate((new_key_ref, new_value_ref))
+    ]
+    for store in stores:
+        store.start()
     soft = jnp.maximum(scores, 0.0) + jnp.log1p(jnp.exp(-jnp.abs(scores)))
     drop = jnp.where(live, soft, 0.0)
     chunks = cache // lanes
@@ -107,6 +121,7 @@
         running = running + sums[c * rows : (c + 1) * rows]
     after = jnp.concatenate(pieces, axis=1)
     weights = jnp.where(live, jnp.exp(scores - soft - after), 0.0).astype(jnp.bfloat16)
+    fetches[3].wait()
     values = value_ref[:, 0].reshape(rows * heads, cache)
     crossed = lax.dot_general(
         weights, values, (((1,), (1,)), ((), ())), preferred_element_type=jnp.float32
@@ -118,6 +133,7 @@
     square = jnp.sum(folded * folded, axis=1, keepdims=True)
     attended = folded[:, :heads] + folded[:, heads : 2 * heads]
     ready = (attended * mix_ref[...]).astype(jnp.bfloat16)
+    fetches[4].wait()
     branch = jnp.dot(ready, wout_ref[...], preferred_element_type=jnp.float32)
     top = square.astype(jnp.bfloat16).astype(jnp.float32)
     half = lax.broadcasted_iota(jnp.int32, (rows, lanes), 1) < lanes // 2
@@ -136,25 +152,22 @@
     placed_ref[...] = placed.astype(jnp.bfloat16)
     high_ref[...] = high
     low_ref[...] = (weight - high.astype(jnp.float32)).astype(jnp.bfloat16)
+    for store in stores:
+        store.wait()
 
 
 def load_kernel(*refs):
-    count = len(refs) // 2
-    sources, targets, sems = refs[:count], refs[count : 2 * count], refs[2 * count]
+    count = len(refs) // 2 - 1
+    sources, out_ref, targets, sems = refs[:count], refs[count], refs[count + 1 : -1], refs[-1]
+    pairs = [(sources[0], out_ref.at[t]) for t in range(out_ref.shape[0])]
+    pairs += list(zip(sources, targets))
     loads = [
-        pltpu.make_async_copy(source, target, sems.at[i])
-        for i, (source, target) in enumerate(zip(sources, targets))
+        pltpu.make_async_copy(source, target, sems.at[i]) for i, (source, target) in enumerate(pairs)
     ]
     for load in loads:
         load.start()
     for load in loads:
         load.wait()
-
-
-def copies_kernel(row_ref, out_ref):
-    row = row_ref[...]
-    for t in range(out_ref.shape[0]):
-        out_ref[t] = row
 
 
 def join_kernel(gate_ref, up_ref, down_ref, after_ref, out_ref):
@@ -330,27 +343,40 @@
         route_experts.T,
         route_weights.T,
     )
-    near, *small = local(
+    copies, near, *small = local(
         load_kernel,
-        [shape(x.shape, x.dtype) for x in small],
+        [shape((blocks, rows, lanes), bf16)] + [shape(x.shape, x.dtype) for x in small],
         *small,
+        flops=LONG,
         far_in=len(small),
-        scratch=[pltpu.SemaphoreType.DMA((len(small),))],
-    )
-    copies = local(copies_kernel, shape((blocks, rows, lanes), bf16), near, flops=LONG)
-    normed, partial_branch, placed, high, low = local(
+        far_out=1,
+        scratch=[pltpu.SemaphoreType.DMA((blocks + len(small),))],
+    )
+    parts = exchange(copies, TP)
+    new_keys, new_values, partial_branch, placed, high, low = local(
         attend_kernel,
-        [shape((rows, blocks * lanes), bf16), shape((blocks, 2 * rows, lanes), bf16)]
-        + [shape((slots, rows), bf16)] * 3,
-        exchange(copies, TP),
+        [new, new, shape((blocks, 2 * rows, lanes), bf16)] + [shape((slots, rows), bf16)] * 3,
+        key_cache,
+        w_key.T,
+        w_value.T,
+        value_cache,
+        w_out,
+        parts,
         *small,
         w_query.T,
-        key_cache,
-        value_cache,
         key_bias,
-        w_out,
-    )
-    new_keys, new_values = local(keys_kernel, [new, new], normed, w_key.T, w_value.T, flops=SHORT)
+        far_in=5,
+        far_out=2,
+        scratch=[
+            pltpu.VMEM((2, rows, heads), bf16),
+            pltpu.VMEM(key_cache.shape, bf16),
+            pltpu.VMEM(w_key.T.shape, bf16),
+            pltpu.VMEM(w_value.T.shape, bf16),
+            pltpu.VMEM(value_cache.shape, bf16),
+            pltpu.VMEM(w_out.shape, bf16),
+            pltpu.SemaphoreType.DMA((7,)),
+        ],
+    )
     pairs = [(i, i ^ PAIRS[i // blocks]) for i in range(CORES * blocks)]
     branch = exchange(partial_branch, TP)
     joined = local(
@@ -359,7 +385,7 @@
         w_gate,
         w_up,
         w_down,
-        low,
+        near,
         flops=SHORT,
     )
     swapped = lax.ppermute(joined, (EP[0], *TP), pairs)

time: 115 us -> 113 us (0.983)
  blocking collectives: 87.9 us -> 101 us
  waiting for transfers between devices: 11.6 us -> 0.01 us
  starting transfers between devices: 8.37 us -> 4.02 us
    all_to_all x5 -> x6, blocking collectives: 87.9 us -> 101 us  [exchange(): return lax.all_to_all(x, axis, 0, 0, tiled=True)]
    all_to_all x1 -> x0, waiting for transfers between devices: 11.6 us -> none  [exchange(): return lax.all_to_all(x, axis, 0, 0, tiled=True)]
    all_to_all x1 -> x0, starting transfers between devices: 6.18 us -> none  [exchange(): return lax.all_to_all(x, axis, 0, 0, tiled=True)]
    ppermute x1, starting transfers between devices: 2.19 us -> 4.02 us  [layer(): swapped = lax.ppermute(joined, (EP[0], *TP), pairs)]
    pallas_call x10 -> x8, Pallas kernels: 5.94 us -> 6.35 us  [local(): pl.pallas_call(kernel, in_specs=places(len(args), far_in), out_specs=outs...]
  transfers between devices with their start and end apart: 2 -> 1, of which waited for: 1 -> 0; matrix products, arithmetic and copies ran while one was open for 0% -> 0% of each run, Pallas kernels for 1% -> 3%
where the time goes in v10:
time: 113 us; the launch traced here: 112 us
  blocking collectives  101 us (89%)
  Pallas kernels  6.35 us (6%)
  starting transfers between devices  4.02 us (4%)
    all_to_all x6, blocking collectives, exchange(): return lax.all_to_all(x, axis, 0, 0, tiled=True)  101 us
    pallas_call x8, Pallas kernels, local(): pl.pallas_call(kernel, in_specs=places(len(args), far_in), out_specs=outs...  6.35 us
    ppermute x1, starting transfers between devices, layer(): swapped = lax.ppermute(joined, (EP[0], *TP), pairs)  4.02 us
  transfers between devices with their start and end apart: 1, of which 0 were waited for; matrix products, arithmetic and copies ran while one was open for 0% of the time, Pallas kernels for 3%

profile of v10, /device:TPU:1, one launch (start us, length us, event | category | flops | bytes accessed | tf_op | source)
XLA Modules:
  0.0 112.2 jit_solution(17788976717009832427)
XLA Ops:
  0.6 0.0 copy-start.3
  0.6 0.0 copy-start.4
  0.7 0.0 copy-start.5
  0.7 1.5 %shard_map.184 = (bf16[16,8,128]{2,1,0:T(8,128)(2,1)S(1)}, bf16[8,128]{1,0:T(8,128)(2,1)S(1)}, s32[1,8]{1,0:T(1,128)S(1)}, f32[16,128]{1,0:T(8,128)S(1)}, f32[1,...) custom-call(bf16[8,128]{1,0:T(8,128)(2,1)} %refs_0_.1, s32[1,8]{1,0:T(1,128)} %bitcast.16, ...), custom_call_target="tpu_custom_call" | custom-call | flops 40000000000 | tf_op jit(solution)/shard_map/pallas_call | solution.py:295
  2.2 0.0 copy-done.3
  2.2 0.0 copy-done.4
  2.2 0.0 copy-done.5
  2.2 0.0 copy-start
  2.2 0.0 copy-start.1
  2.2 0.1 shard_map.188.refs_0_
  2.4 4.0 %collective-permute-start = (bf16[6144,128]{1,0:T(8,128)(2,1)S(1)}, bf16[6144,128]{1,0:T(8,128)(2,1)S(1)}, u32[]{:S(2)}, u32[]{:S(2)}) collective-permute-start(bf16[6144,128]{1,0:T(8,128)(2,1)S(1)} %shard_map.188.refs_0_), channel_id=1, source_target_pairs={{0,1},{1,0},{2,3},{3,2},{4,5},{5,4},{6,7},{7,6},{8,9},{9,8},{10,11... | collective-permute-start | bytes 4718600 | tf_op jit(solution)/shard_map/ppermute | solution.py:391
  6.4 20.7 %all_to_all.30.parts_ref = bf16[16,8,128]{2,1,0:T(8,128)(2,1)S(1)} all-to-all(bf16[16,8,128]{2,1,0:T(8,128)(2,1)S(1)} %get-tuple-element.18), channel_id=1, replica_groups=mesh['ep_0'=16,'ep_1'=2,'tp_0'=4,'tp_1'=4] {'tp_0','tp_1'}, dimensions={0} | all-to-all | bytes 65536 | tf_op jit(solution)/shard_map/all_to_all | solution.py:307
  27.1 0.0 copy-done
  27.1 0.0 copy-done.1
  27.1 2.6 %shard_map.185 = (bf16[8,64]{1,0:T(8,128)(2,1)}, bf16[8,64]{1,0:T(8,128)(2,1)}, bf16[16,16,128]{2,1,0:T(8,128)(2,1)S(1)}, bf16[128,8]{1,0:T(8,128)(2,1)S(1)}, bf...) custom-call(bf16[8,1,64,1024]{3,2,1,0:T(8,128)(2,1)} %far_key_ref.1, bf16[64,2048]{1,0:T(8,128)(2,1)} %bitcast.11, ...), custom_call_target="tpu_custom_call" | custom-call | tf_op jit(solution)/shard_map/pallas_call | solution.py:295
  29.7 10.9 %all_to_all.31.parts_ref = bf16[16,16,128]{2,1,0:T(8,128)(2,1)S(1)} all-to-all(bf16[16,16,128]{2,1,0:T(8,128)(2,1)S(1)} %get-tuple-element.24), channel_id=1, replica_groups=mesh['ep_0'=16,'ep_1'=2,'tp_0'=4,'tp_1'=4] {'tp_0','tp_1'}, dimensions={0} | all-to-all | bytes 131072 | tf_op jit(solution)/shard_map/all_to_all | solution.py:307
  40.6 0.3 shard_map.186
  40.9 31.2 %all_to_all.32.arrived_ref = bf16[32,4,128]{2,1,0:T(4,128)(2,1)S(1)} all-to-all(bf16[32,4,128]{2,1,0:T(4,128)(2,1)S(1)} %get-tuple-element.27), channel_id=1, replica_groups=mesh['ep_0'=16,'ep_1'=2,'tp_0'=4,'tp_1'=4] {'ep_1','ep_0'}, dimensions={0} | all-to-all | bytes 65536 | tf_op jit(solution)/shard_map/all_to_all | solution.py:307
  72.1 0.0 copy-start.2
  72.1 0.2 shard_map.187
  72.3 10.6 %all_to_all.33.rows_ref = bf16[16,48,128]{2,1,0:T(8,128)(2,1)S(1)} all-to-all(bf16[16,48,128]{2,1,0:T(8,128)(2,1)S(1)} %shard_map.187), channel_id=1, replica_groups=mesh['ep_0'=16,'ep_1'=2,'tp_0'=4,'tp_1'=4] {'tp_0','tp_1'}, dimensions={0} | all-to-all | bytes 393216 | tf_op jit(solution)/shard_map/all_to_all | solution.py:307
  82.9 0.0 collective-permute-done.refs_1_
  82.9 0.0 copy-done.2
  82.9 0.7 shard_map.189
  83.6 9.9 %all_to_all.34.parts_ref = bf16[16,48,128]{2,1,0:T(8,128)(2,1)S(1)} all-to-all(bf16[16,48,128]{2,1,0:T(8,128)(2,1)S(1)} %shard_map.189), channel_id=1, replica_groups=mesh['ep_0'=16,'ep_1'=2,'tp_0'=4,'tp_1'=4] {'tp_0','tp_1'}, dimensions={0} | all-to-all | bytes 393216 | tf_op jit(solution)/shard_map/all_to_all | solution.py:307
  93.5 0.2 shard_map.190
  93.7 17.8 %all_to_all.35.returned_ref = bf16[32,4,128]{2,1,0:T(4,128)(2,1)S(1)} all-to-all(bf16[32,4,128]{2,1,0:T(4,128)(2,1)S(1)} %shard_map.190), channel_id=1, replica_groups=mesh['ep_0'=16,'ep_1'=2,'tp_0'=4,'tp_1'=4] {'ep_1','ep_0'}, dimensions={0} | all-to-all | bytes 65536 | tf_op jit(solution)/shard_map/all_to_all | solution.py:307
  111.5 0.8 shard_map.191
Async XLA Ops:
  0.6 1.5 %copy-start.3 = (bf16[1,2048,128]{2,1,0:T(8,128)(2,1)S(1)}, bf16[1,2048,128]{2,1,0:T(8,128)(2,1)}, u32[]{:S(2)}) copy-start(bf16[1,2048,128]{2,1,0:T(8,128)(2,1)} %gate_ref.1) | copy-start | bytes 1572868
  0.6 1.5 %copy-start.4 = (bf16[1,2048,128]{2,1,0:T(8,128)(2,1)S(1)}, bf16[1,2048,128]{2,1,0:T(8,128)(2,1)}, u32[]{:S(2)}) copy-start(bf16[1,2048,128]{2,1,0:T(8,128)(2,1)} %up_ref.1) | copy-start | bytes 1572868
  0.7 1.5 %copy-start.5 = (bf16[1,128,2048]{2,1,0:T(8,128)(2,1)S(1)}, bf16[1,128,2048]{2,1,0:T(8,128)(2,1)}, u32[]{:S(2)}) copy-start(bf16[1,128,2048]{2,1,0:T(8,128)(2,1)} %down_ref.1) | copy-start | bytes 1572868
  2.2 24.9 %copy-start = (bf16[2048,64]{0,1:T(8,128)(2,1)S(1)}, bf16[2048,64]{0,1:T(8,128)(2,1)}, u32[]{:S(2)}) copy-start(bf16[2048,64]{0,1:T(8,128)(2,1)} %param.19) | copy-start | bytes 786436
  2.2 24.9 %copy-start.1 = (f32[8,1,1024]{2,1,0:T(1,128)S(1)}, f32[8,1,1024]{2,1,0:T(1,128)}, u32[]{:S(2)}) copy-start(f32[8,1,1024]{2,1,0:T(1,128)} %bias_ref.1) | copy-start | bytes 98308
  2.4 80.5 %collective-permute-start = (bf16[6144,128]{1,0:T(8,128)(2,1)S(1)}, bf16[6144,128]{1,0:T(8,128)(2,1)S(1)}, u32[]{:S(2)}, u32[]{:S(2)}) collective-permute-start(bf16[6144,128]{1,0:T(8,128)(2,1)S(1)} %shard_map.188.refs_0_), channel_id=1, source_target_pairs={{0,1},{1,0},{2,3},{3,2},{4,5},{5,4},{6,7},{7,6},{8,9},{9,8},{10,11... | collective-permute-start | bytes 4718600 | tf_op jit(solution)/shard_map/ppermute | solution.py:391
  72.1 10.8 %copy-start.2 = (f32[2048]{0:T(1024)S(1)}, f32[2048]{0:T(1024)}, u32[]{:S(2)}) copy-start(f32[2048]{0:T(1024)} %param.28) | copy-start | bytes 24580

commit v11 on v9

--- a/solution.py
+++ b/solution.py
@@ -10,8 +10,7 @@
 TP = ("tp_0", "tp_1")
 EP = ("ep_1", "ep_0")
 CORES = 2
-PAIRS = (1, 4)
-PIECE = 4
+PAIRS = (4, 1)
 
 eps = 1e-06
 limit = 7.0
@@ -50,7 +49,7 @@
 
 def attend_kernel(parts_ref, lengths_ref, gain_ref, mix_ref, experts_ref, share_ref, wq_ref,
                   wk_ref, wv_ref, key_ref, value_ref, bias_ref, wout_ref, new_key_ref,
-                  new_value_ref, out_ref, placed_ref, high_ref, low_ref, fresh_ref, stage_ref, sems):
+                  new_value_ref, out_ref, placed_ref, high_ref, low_ref, fresh_ref, sems):
     blocks, rows, lanes = parts_ref.shape
     heads = key_ref.shape[2]
     cache = key_ref.shape[3]
@@ -121,26 +120,13 @@
     square = jnp.sum(folded * folded, axis=1, keepdims=True)
     attended = folded[:, :heads] + folded[:, heads : 2 * heads]
     ready = (attended * mix_ref[...]).astype(jnp.bfloat16)
+    branch = jnp.dot(ready, wout_ref[...], preferred_element_type=jnp.float32)
     top = square.astype(jnp.bfloat16).astype(jnp.float32)
     half = lax.broadcasted_iota(jnp.int32, (rows, lanes), 1) < lanes // 2
     tail = jnp.where(half, top, square - top)
-    tail = tail.astype(jnp.bfloat16)
     for t in range(blocks):
-        stage_ref[t, rows:] = tail
-
-    def send(first, last, low, high):
-        store = pltpu.make_async_copy(
-            stage_ref.at[first:last, low:high], out_ref.at[first:last, low:high], sems.at[len(stores)]
-        )
-        store.start()
-        stores.append(store)
-
-    send(0, blocks, rows, 2 * rows)
-    branch = jnp.dot(ready, wout_ref[...], preferred_element_type=jnp.float32)
-    for t in range(blocks):
-        stage_ref[t, :rows] = branch[:, t * lanes : (t + 1) * lanes].astype(jnp.bfloat16)
-        if t % PIECE == PIECE - 1:
-            send(t + 1 - PIECE, t + 1, 0, rows)
+        both = jnp.concatenate([branch[:, t * lanes : (t + 1) * lanes], tail], axis=0)
+        out_ref[t] = both.astype(jnp.bfloat16)
     hits, placed = chosen_slots(experts_ref, placed_ref.shape[0])
     share = share_ref[...]
     share = share / jnp.sum(share, axis=0, keepdims=True)
@@ -368,12 +354,8 @@
         value_cache,
         key_bias,
         w_out,
-        far_out=3,
-        scratch=[
-            pltpu.VMEM((2, rows, heads), bf16),
-            pltpu.VMEM((blocks, 2 * rows, lanes), bf16),
-            pltpu.SemaphoreType.DMA((3 + blocks // PIECE,)),
-        ],
+        far_out=2,
+        scratch=[pltpu.VMEM((2, rows, heads), bf16), pltpu.SemaphoreType.DMA((2,))],
     )
     pairs = [(i, i ^ PAIRS[i // blocks]) for i in range(CORES * blocks)]
     branch = exchange(partial_branch, TP)

time: 114 us -> 112 us (0.982)
  blocking collectives: 106 us -> 104 us
    all_to_all x6, blocking collectives: 106 us -> 104 us  [exchange(): return lax.all_to_all(x, axis, 0, 0, tiled=True)]
where the time goes in v11:
time: 112 us
  blocking collectives  104 us (93%)
  Pallas kernels  4.54 us (4%)
  starting transfers between devices  2.19 us (2%)
    all_to_all x6, blocking collectives, exchange(): return lax.all_to_all(x, axis, 0, 0, tiled=True)  104 us
    pallas_call x9, Pallas kernels, local(): pl.pallas_call(kernel, in_specs=places(len(args), far_in), out_specs=outs...  4.54 us
  transfers between devices with their start and end apart: 1, of which 0 were waited for; matrix products, arithmetic and copies ran while one was open for 0% of the time, Pallas kernels for 0%

profile of v11, /device:TPU:1, one launch (start us, length us, event | category | flops | bytes accessed | tf_op | source)
XLA Modules:
  0.0 111.8 jit_solution(13119204068079280508)
XLA Ops:
  0.6 0.8 shard_map.184
  1.5 0.0 copy-start
  1.5 0.0 copy-start.1
  1.5 0.0 copy-start.2
  1.5 0.0 copy-start.3
  1.5 0.0 copy-start.4
  1.5 0.0 copy-start.5
  1.5 0.0 copy-start.6
  1.6 14.1 %all_to_all.30.parts_ref = bf16[16,8,128]{2,1,0:T(8,128)(2,1)S(1)} all-to-all(bf16[16,8,128]{2,1,0:T(8,128)(2,1)S(1)} %shard_map.185), channel_id=1, replica_groups=mesh['ep_0'=16,'ep_1'=2,'tp_0'=4,'tp_1'=4] {'tp_0','tp_1'}, dimensions={0} | all-to-all | bytes 65536 | tf_op jit(solution)/shard_map/all_to_all | solution.py:298
  15.6 0.0 copy-done
  15.6 0.0 copy-done.1
  15.7 0.0 copy-start.8
  15.7 0.0 copy-start.9
  15.7 0.0 copy-start.10
  15.7 1.5 %shard_map.186 = (bf16[8,64]{1,0:T(8,128)(2,1)}, bf16[8,64]{1,0:T(8,128)(2,1)}, bf16[16,16,128]{2,1,0:T(8,128)(2,1)S(1)}, bf16[128,8]{1,0:T(8,128)(2,1)S(1)}, bf...) custom-call(bf16[16,8,128]{2,1,0:T(8,128)(2,1)S(1)} %all_to_all.30.parts_ref, ...), custom_call_target="tpu_custom_call" | custom-call | tf_op jit(solution)/shard_map/pallas_call | solution.py:286
  17.2 0.0 copy-done.8
  17.2 0.0 copy-done.9
  17.2 0.0 copy-done.10
  17.2 0.1 shard_map.189.refs_0_
  17.4 2.2 %collective-permute-start = (bf16[6144,128]{1,0:T(8,128)(2,1)S(1)}, bf16[6144,128]{1,0:T(8,128)(2,1)S(1)}, u32[]{:S(2)}, u32[]{:S(2)}) collective-permute-start(bf16[6144,128]{1,0:T(8,128)(2,1)S(1)} %shard_map.189.refs_0_), channel_id=1, source_target_pairs={{0,4},{1,5},{2,6},{3,7},{4,0},{5,1},{6,2},{7,3},{8,12},{9,13},{10,... | collective-permute-start | bytes 4718600 | tf_op jit(solution)/shard_map/ppermute | solution.py:371
  19.6 20.9 %all_to_all.31.parts_ref = bf16[16,16,128]{2,1,0:T(8,128)(2,1)S(1)} all-to-all(bf16[16,16,128]{2,1,0:T(8,128)(2,1)S(1)} %get-tuple-element.23), channel_id=1, replica_groups=mesh['ep_0'=16,'ep_1'=2,'tp_0'=4,'tp_1'=4] {'tp_0','tp_1'}, dimensions={0} | all-to-all | bytes 131072 | tf_op jit(solution)/shard_map/all_to_all | solution.py:298
  40.5 0.3 shard_map.187
  40.8 30.1 %all_to_all.32.arrived_ref = bf16[32,4,128]{2,1,0:T(4,128)(2,1)S(1)} all-to-all(bf16[32,4,128]{2,1,0:T(4,128)(2,1)S(1)} %get-tuple-element.25), channel_id=1, replica_groups=mesh['ep_0'=16,'ep_1'=2,'tp_0'=4,'tp_1'=4] {'ep_1','ep_0'}, dimensions={0} | all-to-all | bytes 65536 | tf_op jit(solution)/shard_map/all_to_all | solution.py:298
  70.9 0.2 shard_map.188
  71.0 11.4 %all_to_all.33.rows_ref = bf16[16,48,128]{2,1,0:T(8,128)(2,1)S(1)} all-to-all(bf16[16,48,128]{2,1,0:T(8,128)(2,1)S(1)} %shard_map.188), channel_id=1, replica_groups=mesh['ep_0'=16,'ep_1'=2,'tp_0'=4,'tp_1'=4] {'tp_0','tp_1'}, dimensions={0} | all-to-all | bytes 393216 | tf_op jit(solution)/shard_map/all_to_all | solution.py:298
  82.4 0.0 collective-permute-done.refs_1_
  82.4 0.0 copy-done.7
  82.4 0.7 shard_map.190
  83.2 9.9 %all_to_all.34.parts_ref = bf16[16,48,128]{2,1,0:T(8,128)(2,1)S(1)} all-to-all(bf16[16,48,128]{2,1,0:T(8,128)(2,1)S(1)} %shard_map.190), channel_id=1, replica_groups=mesh['ep_0'=16,'ep_1'=2,'tp_0'=4,'tp_1'=4] {'tp_0','tp_1'}, dimensions={0} | all-to-all | bytes 393216 | tf_op jit(solution)/shard_map/all_to_all | solution.py:298
  93.1 0.2 shard_map.191
  93.3 17.8 %all_to_all.35.returned_ref = bf16[32,4,128]{2,1,0:T(4,128)(2,1)S(1)} all-to-all(bf16[32,4,128]{2,1,0:T(4,128)(2,1)S(1)} %shard_map.191), channel_id=1, replica_groups=mesh['ep_0'=16,'ep_1'=2,'tp_0'=4,'tp_1'=4] {'ep_1','ep_0'}, dimensions={0} | all-to-all | bytes 65536 | tf_op jit(solution)/shard_map/all_to_all | solution.py:298
  111.0 0.8 shard_map.192
  (7 shorter events, 0.0 us)
Async XLA Ops:
  1.5 14.2 %copy-start = (bf16[8,1,64,1024]{3,2,1,0:T(8,128)(2,1)S(1)}, bf16[8,1,64,1024]{3,2,1,0:T(8,128)(2,1)}, u32[]{:S(2)}) copy-start(bf16[8,1,64,1024]{3,2,1,0:T(8,128)(2,1)} %key_ref.1) | copy-start | bytes 3145732
  1.5 14.2 %copy-start.1 = (bf16[8,1,64,1024]{3,2,1,0:T(8,128)(2,1)S(1)}, bf16[8,1,64,1024]{3,2,1,0:T(8,128)(2,1)}, u32[]{:S(2)}) copy-start(bf16[8,1,64,1024]{3,2,1,0:T(8,128)(2,1)} %value_ref.1) | copy-start | bytes 3145732
  1.5 14.2 %copy-start.2 = (bf16[2048,64]{0,1:T(8,128)(2,1)S(1)}, bf16[2048,64]{0,1:T(8,128)(2,1)}, u32[]{:S(2)}) copy-start(bf16[2048,64]{0,1:T(8,128)(2,1)} %param.19) | copy-start | bytes 786436
  1.5 14.2 %copy-start.3 = (bf16[2048,64]{0,1:T(8,128)(2,1)S(1)}, bf16[2048,64]{0,1:T(8,128)(2,1)}, u32[]{:S(2)}) copy-start(bf16[2048,64]{0,1:T(8,128)(2,1)} %param.20) | copy-start | bytes 786436
  1.5 14.2 %copy-start.4 = (bf16[2048,64]{0,1:T(8,128)(2,1)S(1)}, bf16[2048,64]{0,1:T(8,128)(2,1)}, u32[]{:S(2)}) copy-start(bf16[2048,64]{0,1:T(8,128)(2,1)} %param.21) | copy-start | bytes 786436
  1.5 14.2 %copy-start.5 = (bf16[64,2048]{1,0:T(8,128)(2,1)S(1)}, bf16[64,2048]{1,0:T(8,128)(2,1)}, u32[]{:S(2)}) copy-start(bf16[64,2048]{1,0:T(8,128)(2,1)} %wout_ref.1) | copy-start | bytes 786436
  1.5 14.2 %copy-start.6 = (f32[8,1,1024]{2,1,0:T(1,128)S(1)}, f32[8,1,1024]{2,1,0:T(1,128)}, u32[]{:S(2)}) copy-start(f32[8,1,1024]{2,1,0:T(1,128)} %bias_ref.1) | copy-start | bytes 98308
  15.7 1.5 %copy-start.8 = (bf16[1,2048,128]{2,1,0:T(8,128)(2,1)S(1)}, bf16[1,2048,128]{2,1,0:T(8,128)(2,1)}, u32[]{:S(2)}) copy-start(bf16[1,2048,128]{2,1,0:T(8,128)(2,1)} %gate_ref.1) | copy-start | bytes 1572868
  15.7 1.5 %copy-start.9 = (bf16[1,2048,128]{2,1,0:T(8,128)(2,1)S(1)}, bf16[1,2048,128]{2,1,0:T(8,128)(2,1)}, u32[]{:S(2)}) copy-start(bf16[1,2048,128]{2,1,0:T(8,128)(2,1)} %up_ref.1) | copy-start | bytes 1572868
  15.7 1.5 %copy-start.10 = (bf16[1,128,2048]{2,1,0:T(8,128)(2,1)S(1)}, bf16[1,128,2048]{2,1,0:T(8,128)(2,1)}, u32[]{:S(2)}) copy-start(bf16[1,128,2048]{2,1,0:T(8,128)(2,1)} %down_ref.1) | copy-start | bytes 1572868
  17.4 65.1 %collective-permute-start = (bf16[6144,128]{1,0:T(8,128)(2,1)S(1)}, bf16[6144,128]{1,0:T(8,128)(2,1)S(1)}, u32[]{:S(2)}, u32[]{:S(2)}) collective-permute-start(bf16[6144,128]{1,0:T(8,128)(2,1)S(1)} %shard_map.189.refs_0_), channel_id=1, source_target_pairs={{0,4},{1,5},{2,6},{3,7},{4,0},{5,1},{6,2},{7,3},{8,12},{9,13},{10,... | collective-permute-start | bytes 4718600 | tf_op jit(solution)/shard_map/ppermute | solution.py:371
  70.9 11.6 %copy-start.7 = (f32[2048]{0:T(1024)S(1)}, f32[2048]{0:T(1024)}, u32[]{:S(2)}) copy-start(f32[2048]{0:T(1024)} %param.28) | copy-start | bytes 24580
